TPU v7x, 512 devices: a whole 4x4x16 slice. The times are simulated.
512 devices in a mesh: sp: 32 (over z, core), tp: 16 (over y, x).
Axes of the slice: x: 4, y: 4, z: 16, core: 2. Of those that a mesh axis runs over, the one named last changes fastest.
Arguments:
- wide_queries: bfloat16 [2048, 2560], P('sp', 'tp'), may hold values from -512 to 512
- narrow_queries: bfloat16 [2048, 1536], P('sp', 'tp'), may hold values from -512 to 512
- kv_latent: bfloat16 [2048, 512], P('sp'), may hold values from -6 to 6
- rope_key: bfloat16 [2048, 32], P('sp'), may hold values from -4 to 4
- latent_gain: float32 [512], replicated, may hold values from 0.1 to 1.9
- wide_kv_weight: bfloat16 [512, 4096], P(None, 'tp'), may hold values from -0.25 to 0.25
- narrow_kv_weight: bfloat16 [512, 2048], P(None, 'tp'), may hold values from -0.25 to 0.25
- wide_out_weight: bfloat16 [2048, 2048], P('tp'), may hold values from -0.4375 to 0.4375
- narrow_out_weight: bfloat16 [1024, 2048], P('tp'), may hold values from -0.4375 to 0.4375
- residual: bfloat16 [2048, 2048], P('sp'), may hold values from -6 to 6
- norm_gain: float32 [2048], replicated, may hold values from 0.1 to 1.9
- route_ids: int32 [2048, 2], P('sp'), may hold values from 0 to 63, all different within a row; in each aligned block of 64 rows (0 to 63, 64 to 127, ...) at most 3 rows name the same one
- route_weights: float32 [2048, 2], P('sp'), may hold values from 0.3 to 1.3
- expert_gate: bfloat16 [64, 2048, 1024], P('sp', None, 'tp'), may hold values from -0.125 to 0.125
- expert_up: bfloat16 [64, 2048, 1024], P('sp', None, 'tp'), may hold values from -0.125 to 0.125
- expert_down: bfloat16 [64, 1024, 2048], P('sp', 'tp'), may hold values from -0.1875 to 0.1875
- shared_gate: bfloat16 [2048, 1024], P(None, 'tp'), may hold values from -0.125 to 0.125
- shared_up: bfloat16 [2048, 1024], P(None, 'tp'), may hold values from -0.125 to 0.125
- shared_down: bfloat16 [1024, 2048], P('tp'), may hold values from -0.1875 to 0.1875
Outputs:
- mixed_out: bfloat16 [2048, 2048], P('sp', 'tp')
Inputs may be any that keep to these rules, and one draw needn't show every extreme that they name: `route_ids`: in the rows of one index of sp (aligned blocks of 64 rows) no expert is named by more than 3 rows, and some expert by exactly that many; each row names 2 different experts.
All inputs are finite; a program needn't handle non-finite values.
Results may differ from a plain program's by a relative error of at most 0.018.
Values may be sent and summed in bfloat16 or wider, within the bound.
No kernel may reach another device: no remote copies, remote signals or barrier semaphores. Data moves between devices by JAX's collectives and lax.ppermute only.
A program may use at most 64 MiB of HBM per device.

v0:
```python
import jax
import jax.numpy as jnp
from jax import lax
from jax.sharding import Mesh
from jax.sharding import PartitionSpec as P

D_MODEL = 2048
WIDE_NOPE = 128
WIDE_VALUE = 128
NARROW_NOPE = 64
NARROW_VALUE = 64
ROPE_DIM = 32
SP = ("sp_0", "sp_1")


THETA = 10000.0
EPS = 1e-06
FLOOR = -1e30


def from_everyone(shard, axis):
    copies = jnp.broadcast_to(shard, (lax.axis_size(axis), *shard.shape))
    return lax.all_to_all(copies, axis, split_axis=0, concat_axis=0, tiled=True)


def in_order(pieces, dim):
    pieces = jnp.moveaxis(pieces, 0, dim)
    shape = pieces.shape
    return pieces.reshape(*shape[:dim], shape[dim] * shape[dim + 1], *shape[dim + 2 :])


def gather_axes(shard, axes, dim):
    far, near = axes
    pieces = from_everyone(from_everyone(shard, far), near)
    return in_order(pieces.swapaxes(0, 1).reshape(-1, *shard.shape), dim)


def in_one_piece(arrays, axis, dim, along):
    ends, at = ([], 0)
    for a in arrays[:-1]:
        at += a.shape[along]
        ends.append(at)
    both = jnp.concatenate(arrays, axis=along)
    return tuple(jnp.split(gather_axes(both, axis, dim), ends, axis=along))


def cut_along(shard, dim, count):
    before, after = (shard.shape[:dim], shard.shape[dim + 1 :])
    return jnp.moveaxis(shard.reshape(*before, count, -1, *after), dim, 0)


def summed_on_arrival(shard, axis, dim):
    pieces = cut_along(shard, dim, lax.axis_size(axis))
    arrived = lax.all_to_all(pieces, axis, split_axis=0, concat_axis=0, tiled=True)
    return arrived.astype(jnp.float32).sum(axis=0)


def padded_to(lines, count):
    spare = -len(lines) % count
    return jnp.pad(lines, [(0, spare)] + [(0, 0)] * (lines.ndim - 1))


def gather_directly(shard, axis, dim):
    return in_order(from_everyone(shard, axis), dim)


def sum_by_parts(shard, axes):
    lines = shard.reshape(-1, shard.shape[-1])
    own = summed_on_arrival(padded_to(lines, lax.axis_size(axes)), axes, 0)
    whole = gather_directly(own.astype(jnp.bfloat16), axes, 0)
    return whole[: len(lines)].reshape(shard.shape).astype(jnp.float32)


def rounded(values):
    return lax.optimization_barrier(values.astype(jnp.bfloat16)).astype(jnp.float32)


def rotate(values, positions):
    half_width = values.shape[-1] // 2
    frequency = THETA ** (-2.0 * jnp.arange(half_width, dtype=jnp.float32) / values.shape[-1])
    angles = positions.astype(jnp.float32)[:, None] * frequency[None, :]
    if values.ndim == 3:
        angles = angles[:, None, :]
    cosine = jnp.cos(angles)
    sine_part = jnp.sin(angles)
    as_float = values.astype(jnp.float32)
    first_half = as_float[..., :half_width]
    second_half = as_float[..., half_width:]
    return jnp.concatenate(
        [
            first_half * cosine - second_half * sine_part,
            second_half * cosine + first_half * sine_part,
        ],
        axis=-1,
    ).astype(jnp.bfloat16)


def rms_scale(values, gain):
    as_float = values.astype(jnp.float32)
    scaled = as_float * lax.rsqrt(jnp.mean(as_float * as_float, axis=-1, keepdims=True) + EPS)
    return (scaled * gain).astype(jnp.bfloat16)


def fresh_state(head_count, query_count, value_width):
    return (
        jnp.full((head_count, query_count), FLOOR, jnp.float32),
        jnp.zeros((head_count, query_count), jnp.float32),
        jnp.zeros((head_count, query_count, value_width), jnp.float32),
    )


def update(carry_part, queries, nope_width, kv_rows, rot_rows, query_pos, key_pos):
    row_peak, row_total, summed = carry_part
    head_count = queries.shape[1]
    key_value = kv_rows.reshape(kv_rows.shape[0], head_count, -1)
    values = key_value[..., nope_width:]
    shared_rot = rot_rows[:, None, :]
    whole_keys = jnp.concatenate([key_value[..., :nope_width], shared_rot], axis=-1)
    scores = jnp.einsum("qhd,khd->hqk", queries, whole_keys, preferred_element_type=jnp.float32)
    scores = scores * queries.shape[-1] ** (-0.5)
    allowed = (query_pos[:, None] >= key_pos[None, :])[None]
    newest = jnp.maximum(row_peak, jnp.max(jnp.where(allowed, scores, FLOOR), axis=-1))
    weights = jnp.where(allowed, jnp.exp(scores - newest[..., None]), 0.0)
    row_total = jnp.sum(weights, axis=-1)
    summed = jnp.einsum(
        "hqk,khv->hqv", weights.astype(jnp.bfloat16), values, preferred_element_type=jnp.float32
    )
    return (newest, row_total, summed)


def local(
    wide_queries,
    narrow_queries,
    kv_latent,
    rope_key,
    latent_gain,
    wide_kv_weight,
    narrow_kv_weight,
    wide_out_weight,
    narrow_out_weight,
    residual,
    norm_gain,
    route_ids,
    route_weights,
    expert_gate,
    expert_up,
    expert_down,
    shared_gate,
    shared_up,
    shared_down,
):
    tok_rows = residual.shape[0]
    positions = lax.axis_index(SP) * tok_rows + jnp.arange(tok_rows, dtype=jnp.int32)
    wide_count = wide_out_weight.shape[0] // WIDE_VALUE
    narrow_count = narrow_out_weight.shape[0] // NARROW_VALUE
    wide_q = wide_queries.reshape(tok_rows, wide_count, WIDE_NOPE + ROPE_DIM)
    wide_q = jnp.concatenate(
        [wide_q[..., :WIDE_NOPE], rotate(wide_q[..., WIDE_NOPE:], positions)], axis=-1
    )
    narrow_q = narrow_queries.reshape(tok_rows, narrow_count, NARROW_NOPE + ROPE_DIM)
    narrow_q = jnp.concatenate(
        [narrow_q[..., :NARROW_NOPE], rotate(narrow_q[..., NARROW_NOPE:], positions)], axis=-1
    )
    key_rot = rotate(rope_key, positions)
    latent = rms_scale(kv_latent, latent_gain)
    initial = (
        fresh_state(wide_count, tok_rows, WIDE_VALUE),
        fresh_state(narrow_count, tok_rows, NARROW_VALUE),
    )
    wide_kv = jnp.dot(latent, wide_kv_weight, preferred_element_type=jnp.float32).astype(
        jnp.bfloat16
    )
    narrow_kv = jnp.dot(latent, narrow_kv_weight, preferred_element_type=jnp.float32).astype(
        jnp.bfloat16
    )
    pieces = in_one_piece((wide_kv, narrow_kv, key_rot), ("sp_0", "sp_1"), 0, 1)
    rot_rows = pieces[2]
    key_pos = jnp.arange(rot_rows.shape[0], dtype=jnp.int32)
    final_state = (
        update(initial[0], wide_q, WIDE_NOPE, pieces[0], rot_rows, positions, key_pos),
        update(initial[1], narrow_q, NARROW_NOPE, pieces[1], rot_rows, positions, key_pos),
    )
    wide_state, narrow_state = final_state
    wide_att = (wide_state[2] / wide_state[1][..., None]).astype(jnp.bfloat16)
    narrow_att = (narrow_state[2] / narrow_state[1][..., None]).astype(jnp.bfloat16)
    partial_proj = jnp.einsum(
        "hqv,hvd->qd",
        wide_att,
        wide_out_weight.reshape(wide_count, WIDE_VALUE, D_MODEL),
        preferred_element_type=jnp.float32,
    )
    partial_proj = partial_proj + jnp.einsum(
        "hqv,hvd->qd",
        narrow_att,
        narrow_out_weight.reshape(narrow_count, NARROW_VALUE, D_MODEL),
        preferred_element_type=jnp.float32,
    )
    proj_sum = sum_by_parts(rounded(partial_proj).astype(jnp.bfloat16), "tp")
    stream = (residual.astype(jnp.float32) + rounded(proj_sum)).astype(jnp.bfloat16)
    normed = rms_scale(stream, norm_gain)
    shared_hidden = (
        jax.nn.silu(jnp.dot(normed, shared_gate, preferred_element_type=jnp.float32))
        * jnp.dot(normed, shared_up, preferred_element_type=jnp.float32)
    ).astype(jnp.bfloat16)
    shared_part = jnp.dot(shared_hidden, shared_down, preferred_element_type=jnp.float32)
    shared_out = rounded(summed_on_arrival(rounded(shared_part).astype(jnp.bfloat16), "tp", 1))
    top_count = route_ids.shape[1]
    local_experts = expert_gate.shape[0]
    sp_count = lax.axis_size(SP)
    expert_total = sp_count * local_experts
    capacity = max(2, 3 * tok_rows * top_count // (2 * expert_total))
    flat_ids = route_ids.reshape(-1)
    one_hot = (flat_ids[:, None] == jnp.arange(expert_total, dtype=jnp.int32)[None, :]).astype(
        jnp.int32
    )
    earlier = jnp.cumsum(one_hot, axis=0) - one_hot
    slot_index = flat_ids * capacity + jnp.sum(earlier * one_hot, axis=1)
    copy_token = jnp.arange(tok_rows * top_count, dtype=jnp.int32) // top_count
    source_row = jnp.zeros((expert_total * capacity,), jnp.int32).at[slot_index].set(copy_token)
    filled = jnp.zeros((expert_total * capacity,), jnp.bfloat16).at[slot_index].set(1.0)
    column_width = D_MODEL // lax.axis_size("tp")
    column_start = lax.axis_index("tp") * column_width
    own_normed = lax.dynamic_slice_in_dim(normed, column_start, column_width, 1)
    outgoing = (own_normed[source_row] * filled[:, None]).reshape(
        sp_count, local_experts, capacity, column_width
    )
    arrived = gather_directly(
        lax.all_to_all(outgoing, SP, split_axis=0, concat_axis=0, tiled=True), "tp", 3
    )
    gate_value = jnp.einsum(
        "sejd,edf->sejf", arrived, expert_gate, preferred_element_type=jnp.float32
    )
    up_value = jnp.einsum("sejd,edf->sejf", arrived, expert_up, preferred_element_type=jnp.float32)
    hidden_units = (jax.nn.silu(gate_value) * up_value).astype(jnp.bfloat16)
    down_part = jnp.einsum(
        "sejf,efd->sejd", hidden_units, expert_down, preferred_element_type=jnp.float32
    )
    expert_result = summed_on_arrival(rounded(down_part).astype(jnp.bfloat16), "tp", 3).astype(
        jnp.bfloat16
    )
    returned = lax.all_to_all(expert_result, SP, split_axis=0, concat_axis=0, tiled=True)
    back_rows = returned.reshape(expert_total * capacity, column_width)[slot_index]
    routed = jnp.sum(
        back_rows.astype(jnp.float32).reshape(tok_rows, top_count, column_width)
        * route_weights[:, :, None],
        axis=1,
    )
    own_stream = lax.dynamic_slice_in_dim(stream, column_start, column_width, 1).astype(jnp.float32)
    return (own_stream + shared_out + routed).astype(jnp.bfloat16)


def solution(mesh):
    torus = Mesh(mesh.devices.reshape(16, 2, mesh.shape["tp"]), ("sp_0", "sp_1", "tp"))
    return jax.shard_map(
        local,
        mesh=torus,
        in_specs=(
            P(SP, "tp"),
            P(SP, "tp"),
            P(SP, None),
            P(SP, None),
            P(),
            P(None, "tp"),
            P(None, "tp"),
            P("tp", None),
            P("tp", None),
            P(SP, None),
            P(),
            P(SP, None),
            P(SP, None),
            P(SP, None, "tp"),
            P(SP, None, "tp"),
            P(SP, "tp", None),
            P(None, "tp"),
            P(None, "tp"),
            P("tp", None),
        ),
        out_specs=P(SP, "tp"),
        check_vma=False,
    )
```

profile of v0, /device:TPU:1, one launch (start us, length us, event | category | flops | bytes accessed | tf_op | source)
XLA Modules:
  0.0 202.4 jit_solution(16078023920893661811)
XLA Ops:
  0.0 1.0 fusion.45
  1.1 0.7 convert_element_type.138
  2.1 1.2 convolution_convert_fusion.3
  3.3 1.2 convolution_convert_fusion.2
  4.6 1.1 broadcast_in_dim.25
  5.7 15.7 %all-to-all-start = ((bf16[16,64,416]{2,1,0:T(8,128)(2,1)}), bf16[16,64,416]{2,1,0:T(8,128)(2,1)S(1)}, u32[]{:S(2)}, u32[]{:S(2)}) async-start(bf16[16,64,416]{2,1,0:T(8,128)(2,1)} %broadcast_in_dim.25), calls=%async_computation | async-start | bytes 2097152 | tf_op jit(solution)/shard_map/all_to_all | solution.py:23
  22.5 43.9 %all-to-all-done = bf16[16,64,416]{2,1,0:T(8,128)(2,1)S(1)} async-done(((bf16[16,64,416]{2,1,0:T(8,128)(2,1)}), bf16[16,64,416]{2,1,0:T(8,128)(2,1)S(1)}, u32[]{:S(2)}, u32[]{:S(2)}) %all-to-all-start) | async-done | bytes 852000 | tf_op jit(solution)/shard_map/all_to_all | solution.py:23
  66.7 10.9 %all_to_all.45 = bf16[2,16,64,416]{3,2,1,0:T(8,128)(2,1)S(1)} all-to-all(bf16[2,16,64,416]{3,2,1,0:T(8,128)(2,1)S(1)} %broadcast_in_dim.26), channel_id=1, replica_groups=mesh['sp_0'=16,'sp_1'=2,'tp'=16] {'sp_1'}, dimensions={0} | all-to-all | bytes 3407872 | tf_op jit(solution)/shard_map/all_to_all | solution.py:23
  79.6 2.3 %fusion.7 = f32[64,2048]{1,0:T(8,128)} fusion(bf16[128,2048]{1,0:T(8,128)(2,1)} %param.26, bf16[2048,1,256]{2,0,1:T(8,128)(2,1)S(1)} %slice_bitcast_fusion, f32[64,2048]{1,0:T(8,128)S(1)} %convolution_multiply_fusion.1, f32[64]{0:T(128)S(1)} %broadcast_maximum_fusion.1, s32[64]{0:T(128)S(1)} %get-tuple-element.20, f32[64]{0:T(128)S(1)} %get-tuple-element.6), kind=kOutput, calls=%fused_computation.23 | convolution fusion | flops 67649536 | bytes 2098688 | tf_op jit(solution)/shard_map/hqv,hvd->qd/dot_general | solution.py:186
  81.9 1.7 fusion.1
  83.6 0.8 reshape.332
  84.4 6.7 %all-to-all-start.2 = ((bf16[16,4,2048]{2,1,0:T(4,128)(2,1)}), bf16[16,4,2048]{2,1,0:T(4,128)(2,1)S(1)}, u32[]{:S(2)}, u32[]{:S(2)}) async-start(bf16[16,4,2048]{2,1,0:T(4,128)(2,1)} %reshape.332), calls=%async_computation.2 | async-start | bytes 524288 | tf_op jit(solution)/shard_map/all_to_all | solution.py:54
  91.4 1.0 scatter_custom_fusion
  92.4 1.3 scatter_custom_fusion.1
  93.9 5.4 %all-to-all-done.2 = bf16[16,4,2048]{2,1,0:T(4,128)(2,1)S(1)} async-done(((bf16[16,4,2048]{2,1,0:T(4,128)(2,1)}), bf16[16,4,2048]{2,1,0:T(4,128)(2,1)S(1)}, u32[]{:S(2)}, u32[]{:S(2)}) %all-to-all-start.2) | async-done | bytes 262176 | tf_op jit(solution)/shard_map/all_to_all | solution.py:54
  99.4 0.8 broadcast_in_dim.30
  100.2 3.5 %all-to-all-start.3 = ((bf16[16,4,2048]{2,1,0:T(4,128)(2,1)}), bf16[16,4,2048]{2,1,0:T(4,128)(2,1)S(1)}, u32[]{:S(2)}, u32[]{:S(2)}) async-start(bf16[16,4,2048]{2,1,0:T(4,128)(2,1)} %broadcast_in_dim.30), calls=%async_computation.3 | async-start | bytes 524288 | tf_op jit(solution)/shard_map/all_to_all | solution.py:23
  103.8 7.5 %all-to-all-done.3 = bf16[16,4,2048]{2,1,0:T(4,128)(2,1)S(1)} async-done(((bf16[16,4,2048]{2,1,0:T(4,128)(2,1)}), bf16[16,4,2048]{2,1,0:T(4,128)(2,1)S(1)}, u32[]{:S(2)}, u32[]{:S(2)}) %all-to-all-start.3) | async-done | bytes 262176 | tf_op jit(solution)/shard_map/all_to_all | solution.py:23
  111.7 0.8 gather_fusion
  112.7 22.8 %all_to_all.46 = bf16[32,2,3,128]{3,1,2,0:T(2,128)(2,1)S(1)} all-to-all(bf16[32,2,3,128]{3,1,2,0:T(2,128)(2,1)S(1)} %copy.51), channel_id=1, replica_groups=mesh['sp_0'=16,'sp_1'=2,'tp'=16] {'sp_0','sp_1'}, dimensions={0} | all-to-all | bytes 98304 | tf_op jit(solution)/shard_map/all_to_all | solution.py:228
  135.7 15.1 %all_to_all.47 = bf16[16,32,2,3,128]{4,1,3,2,0:T(8,128)(2,1)S(1)} all-to-all(bf16[16,32,2,3,128]{4,1,3,2,0:T(8,128)(2,1)S(1)} %broadcast_in_dim.34), channel_id=1, replica_groups=mesh['sp_0'=16,'sp_1'=2,'tp'=16] {'tp'}, dimensions={0} | all-to-all | bytes 1572864 | tf_op jit(solution)/shard_map/all_to_all | solution.py:23
  151.2 0.7 fusion
  152.0 1.1 bitcast_bitcast_fusion
  153.0 3.6 %all-to-all-start.7 = ((bf16[16,32,2,3,128]{4,1,3,2,0:T(8,128)(2,1)}), bf16[16,32,2,3,128]{4,1,3,2,0:T(8,128)(2,1)S(1)}, u32[]{:S(2)}, u32[]{:S(2)}) async-start(bf16[16,32,2,3,128]{4,1,3,2,0:T(8,128)(2,1)} %bitcast_bitcast_fusion), calls=%async_computation.7 | async-start | bytes 1572864 | tf_op jit(solution)/shard_map/all_to_all | solution.py:54
  157.4 0.8 bitcast_bitcast_fusion.1
  158.2 10.2 %all-to-all-done.7 = bf16[16,32,2,3,128]{4,1,3,2,0:T(8,128)(2,1)S(1)} async-done(((bf16[16,32,2,3,128]{4,1,3,2,0:T(8,128)(2,1)}), bf16[16,32,2,3,128]{4,1,3,2,0:T(8,128)(2,1)S(1)}, u32[]{:S(2)}, u32[]{:S(2)}) %all-to-all-start.7) | async-done | bytes 786464 | tf_op jit(solution)/shard_map/all_to_all | solution.py:54
  168.4 3.5 %all-to-all-start.4 = ((bf16[16,64,128]{2,1,0:T(8,128)(2,1)}), bf16[16,64,128]{2,1,0:T(8,128)(2,1)S(1)}, u32[]{:S(2)}, u32[]{:S(2)}) async-start(bf16[16,64,128]{2,1,0:T(8,128)(2,1)} %bitcast_bitcast_fusion.1), calls=%async_computation.4 | async-start | bytes 524288 | tf_op jit(solution)/shard_map/all_to_all | solution.py:54
  172.0 0.7 copy.56
  172.7 6.7 %all-to-all-done.4 = bf16[16,64,128]{2,1,0:T(8,128)(2,1)S(1)} async-done(((bf16[16,64,128]{2,1,0:T(8,128)(2,1)}), bf16[16,64,128]{2,1,0:T(8,128)(2,1)S(1)}, u32[]{:S(2)}, u32[]{:S(2)}) %all-to-all-start.4) | async-done | bytes 262176 | tf_op jit(solution)/shard_map/all_to_all | solution.py:54
  179.4 9.0 %all-to-all-start.8 = ((bf16[32,2,3,128]{3,1,2,0:T(2,128)(2,1)}), bf16[32,2,3,128]{3,1,2,0:T(2,128)(2,1)S(1)}, u32[]{:S(2)}, u32[]{:S(2)}) async-start(bf16[32,2,3,128]{3,1,2,0:T(2,128)(2,1)} %copy.56), calls=%async_computation.8 | async-start | bytes 98304 | tf_op jit(solution)/shard_map/all_to_all | solution.py:241
  188.6 12.2 %all-to-all-done.8 = bf16[32,2,3,128]{3,1,2,0:T(2,128)(2,1)S(1)} async-done(((bf16[32,2,3,128]{3,1,2,0:T(2,128)(2,1)}), bf16[32,2,3,128]{3,1,2,0:T(2,128)(2,1)S(1)}, u32[]{:S(2)}, u32[]{:S(2)}) %all-to-all-start.8) | async-done | bytes 49184 | tf_op jit(solution)/shard_map/all_to_all | solution.py:241
  200.9 0.7 gather_fusion.1
  (86 shorter events, 7.1 us)
Async XLA Ops:
  0.0 151.2 %copy-start = (bf16[2,64,2048]{2,1,0:T(8,128)(2,1)S(1)}, bf16[2,64,2048]{2,1,0:T(8,128)(2,1)}, u32[]{:S(2)}) copy-start(bf16[2,64,2048]{2,1,0:T(8,128)(2,1)} %param.34) | copy-start | bytes 1572868
  0.0 21.4 %copy-start.8 = (bf16[64,96]{1,0:T(8,128)(2,1)S(1)}, bf16[64,96]{1,0:T(8,128)(2,1)}, u32[]{:S(2)}) copy-start(bf16[64,96]{1,0:T(8,128)(2,1)} %param.20) | copy-start | bytes 36868
  0.0 21.5 %copy-start.10 = (s32[64,2]{0,1:T(2,128)S(1)}, s32[64,2]{0,1:T(2,128)}, u32[]{:S(2)}) copy-start(s32[64,2]{0,1:T(2,128)} %param.30) | copy-start | bytes 1540
  1.0 20.7 %copy-start.7 = (bf16[64,160]{1,0:T(8,128)(2,1)S(1)}, bf16[64,160]{1,0:T(8,128)(2,1)}, u32[]{:S(2)}) copy-start(bf16[64,160]{1,0:T(8,128)(2,1)} %param.19) | copy-start | bytes 61444
  5.7 60.8 %all-to-all-start = ((bf16[16,64,416]{2,1,0:T(8,128)(2,1)}), bf16[16,64,416]{2,1,0:T(8,128)(2,1)S(1)}, u32[]{:S(2)}, u32[]{:S(2)}) async-start(bf16[16,64,416]{2,1,0:T(8,128)(2,1)} %broadcast_in_dim.25), calls=%async_computation | async-start | bytes 2097152 | tf_op jit(solution)/shard_map/all_to_all | solution.py:23
  79.2 2.7 %copy-start.2 = (bf16[64,2048]{1,0:T(8,128)(2,1)S(1)}, bf16[64,2048]{1,0:T(8,128)(2,1)}, u32[]{:S(2)}) copy-start(bf16[64,2048]{1,0:T(8,128)(2,1)} %param.27) | copy-start | bytes 786436
  81.9 29.4 %copy-start.4 = (bf16[64,2048]{1,0:T(8,128)(2,1)S(1)}, bf16[64,2048]{1,0:T(8,128)(2,1)}, u32[]{:S(2)}) copy-start(bf16[64,2048]{1,0:T(8,128)(2,1)} %param.28) | copy-start | bytes 786436
  83.6 27.9 %copy-start.9 = (f32[2048]{0:T(1024)S(1)}, f32[2048]{0:T(1024)}, u32[]{:S(2)}) copy-start(f32[2048]{0:T(1024)} %param.29) | copy-start | bytes 24580
  84.4 14.9 %all-to-all-start.2 = ((bf16[16,4,2048]{2,1,0:T(4,128)(2,1)}), bf16[16,4,2048]{2,1,0:T(4,128)(2,1)S(1)}, u32[]{:S(2)}, u32[]{:S(2)}) async-start(bf16[16,4,2048]{2,1,0:T(4,128)(2,1)} %reshape.332), calls=%async_computation.2 | async-start | bytes 524288 | tf_op jit(solution)/shard_map/all_to_all | solution.py:54
  100.2 11.0 %all-to-all-start.3 = ((bf16[16,4,2048]{2,1,0:T(4,128)(2,1)}), bf16[16,4,2048]{2,1,0:T(4,128)(2,1)S(1)}, u32[]{:S(2)}, u32[]{:S(2)}) async-start(bf16[16,4,2048]{2,1,0:T(4,128)(2,1)} %broadcast_in_dim.30), calls=%async_computation.3 | async-start | bytes 524288 | tf_op jit(solution)/shard_map/all_to_all | solution.py:23
  111.5 39.3 %copy-start.12 = (bf16[2,2048,64]{1,2,0:T(8,128)(2,1)S(1)}, bf16[2,2048,64]{1,2,0:T(8,128)(2,1)}, u32[]{:S(2)}) copy-start(bf16[2,2048,64]{1,2,0:T(8,128)(2,1)} %param.32) | copy-start | bytes 1572868
  135.5 15.7 %copy-start.1 = (bf16[2,2048,64]{1,2,0:T(8,128)(2,1)S(1)}, bf16[2,2048,64]{1,2,0:T(8,128)(2,1)}, u32[]{:S(2)}) copy-start(bf16[2,2048,64]{1,2,0:T(8,128)(2,1)} %param.33) | copy-start | bytes 1572868
  151.9 4.7 %copy-start.3 = (bf16[2048,64]{0,1:T(8,128)(2,1)S(1)}, bf16[2048,64]{0,1:T(8,128)(2,1)}, u32[]{:S(2)}) copy-start(bf16[2048,64]{0,1:T(8,128)(2,1)} %param.35) | copy-start | bytes 786436
  151.9 5.0 %copy-start.5 = (bf16[64,2048]{1,0:T(8,128)(2,1)S(1)}, bf16[64,2048]{1,0:T(8,128)(2,1)}, u32[]{:S(2)}) copy-start(bf16[64,2048]{1,0:T(8,128)(2,1)} %param.37) | copy-start | bytes 786436
  151.9 5.0 %copy-start.6 = (bf16[2048,64]{0,1:T(8,128)(2,1)S(1)}, bf16[2048,64]{0,1:T(8,128)(2,1)}, u32[]{:S(2)}) copy-start(bf16[2048,64]{0,1:T(8,128)(2,1)} %param.36) | copy-start | bytes 786436
  153.0 15.3 %all-to-all-start.7 = ((bf16[16,32,2,3,128]{4,1,3,2,0:T(8,128)(2,1)}), bf16[16,32,2,3,128]{4,1,3,2,0:T(8,128)(2,1)S(1)}, u32[]{:S(2)}, u32[]{:S(2)}) async-start(bf16[16,32,2,3,128]{4,1,3,2,0:T(8,128)(2,1)} %bitcast_bitcast_fusion), calls=%async_computation.7 | async-start | bytes 1572864 | tf_op jit(solution)/shard_map/all_to_all | solution.py:54
  156.7 31.8 %copy-start.11 = (f32[64,2]{0,1:T(2,128)S(1)}, f32[64,2]{0,1:T(2,128)}, u32[]{:S(2)}) copy-start(f32[64,2]{0,1:T(2,128)} %param.31) | copy-start | bytes 1540
  168.4 11.0 %all-to-all-start.4 = ((bf16[16,64,128]{2,1,0:T(8,128)(2,1)}), bf16[16,64,128]{2,1,0:T(8,128)(2,1)S(1)}, u32[]{:S(2)}, u32[]{:S(2)}) async-start(bf16[16,64,128]{2,1,0:T(8,128)(2,1)} %bitcast_bitcast_fusion.1), calls=%async_computation.4 | async-start | bytes 524288 | tf_op jit(solution)/shard_map/all_to_all | solution.py:54
  179.4 21.4 %all-to-all-start.8 = ((bf16[32,2,3,128]{3,1,2,0:T(2,128)(2,1)}), bf16[32,2,3,128]{3,1,2,0:T(2,128)(2,1)S(1)}, u32[]{:S(2)}, u32[]{:S(2)}) async-start(bf16[32,2,3,128]{3,1,2,0:T(2,128)(2,1)} %copy.56), calls=%async_computation.8 | async-start | bytes 98304 | tf_op jit(solution)/shard_map/all_to_all | solution.py:241
where the time goes:
time: 203 us; the launch traced here: 202 us
  waiting for transfers between devices  85.9 us (42%)
  blocking collectives  48.9 us (24%)
  starting transfers between devices  42.2 us (21%)
  local copies, waits for them, and re-layouts  11.3 us (6%)
  matrix products  9.18 us (5%)
  other arithmetic  4.43 us (2%)
    all_to_all x2, waiting for transfers between devices, from_everyone(): return lax.all_to_all(copies, axis, split_axis=0, concat_axis=0, tiled=True)  51.4 us
    all_to_all x2, blocking collectives, from_everyone(): return lax.all_to_all(copies, axis, split_axis=0, concat_axis=0, tiled=True)  26.1 us
    all_to_all x1, blocking collectives, local(): lax.all_to_all(outgoing, SP, split_axis=0, concat_axis=0, tiled=True)  22.8 us
    all_to_all x3, waiting for transfers between devices, summed_on_arrival(): lax.all_to_all(pieces, axis, split_axis=0, concat_axis=0, tiled=True)  22.2 us
    all_to_all x2, starting transfers between devices, from_everyone(): return lax.all_to_all(copies, axis, split_axis=0, concat_axis=0, tiled=True)  19.3 us
    all_to_all x3, starting transfers between devices, summed_on_arrival(): lax.all_to_all(pieces, axis, split_axis=0, concat_axis=0, tiled=True)  13.9 us
    all_to_all x1, waiting for transfers between devices, local(): lax.all_to_all(expert_result, SP, split_axis=0, concat_axis=0, tiled=True)  12.2 us
    all_to_all x1, starting transfers between devices, local(): lax.all_to_all(expert_result, SP, split_axis=0, concat_axis=0, tiled=True)  9.03 us
  transfers between devices with their start and end apart: 6, of which 6 were waited for; matrix products, arithmetic and copies ran while one was open for 3% of the time, Pallas kernels for 0%

commit v1 on v0

v1 whole, which is shorter than its diff:
```python
import functools

import jax
import jax.numpy as jnp
from jax import lax
from jax.experimental import pallas as pl
from jax.experimental.pallas import tpu as pltpu
from jax.sharding import Mesh
from jax.sharding import PartitionSpec as P

D_MODEL = 2048
THETA = 10000.0
EPS = 1e-06
FLOOR = -1e30
SP = ("z", "c")
N_SP = 32
N_TP = 16
TOK = 64
SLOTS = 192
F32 = jnp.float32
BF = jnp.bfloat16

LANE_POS, LANE_HI, LANE_LO, LANE_FLAG = 64, 65, 66, 67


def iota(shape, dim):
    return lax.broadcasted_iota(jnp.int32, shape, dim)


def div6(v):
    return (v * 10923) >> 16


def div3(v):
    return (v * 21846) >> 16


def dot(a, b):
    return jnp.dot(a, b, preferred_element_type=F32)


def dot_nt(a, b):
    return lax.dot_general(a, b, (((1,), (1,)), ((), ())), preferred_element_type=F32)


def dot_tn(a, b):
    return lax.dot_general(a, b, (((0,), (0,)), ((), ())), preferred_element_type=F32)


def picks(mask):
    return jnp.where(mask, 1.0, 0.0).astype(BF)


def lane_value(block, lane):
    return jnp.sum(jnp.where(iota(block.shape, 1) == lane, block, 0.0), axis=1, keepdims=True)


def slot_rows(arrived):
    row, col = iota((SLOTS, 256), 0), iota((SLOTS, 256), 1)
    source = div6(row)
    return picks(col == source * 8 + (row - source * 6))


def pack_kernel(tp_ref, q_ref, rope_ref, lat_ref, gain_ref, res_ref, ids_ref, idst_ref, w_ref, cos_ref, sin_ref, out_ref, sel_ref):
    t = tp_ref[0]
    cos, sin = cos_ref[...], sin_ref[...]
    src, dst = iota((128, 128), 0), iota((128, 128), 1)
    swap = picks(src == dst + jnp.where((dst & 16) == 0, 16, -16))

    def turned(block):
        return (block.astype(F32) * cos + dot(block, swap) * sin).astype(BF)

    q_nope = q_ref[:, :128]
    q_rest = turned(q_ref[:, 128:])
    rope = turned(rope_ref[...])
    lat = lat_ref[...].astype(F32)
    scaled = lat * lax.rsqrt(jnp.mean(lat * lat, axis=1, keepdims=True) + EPS)
    normed = (scaled * gain_ref[...]).astype(BF)
    res = res_ref[:, pl.ds(pl.multiple_of(t * 128, 128), 128)]

    earlier = iota((TOK, TOK), 0) < iota((TOK, TOK), 1)
    row, tok = iota((256, TOK), 0), iota((256, TOK), 1)
    dest, place = row >> 3, row & 7
    lane = iota((TOK, 128), 1)
    local_pos = iota((TOK, 128), 0).astype(F32)
    selects, sides = [], []
    for k in range(2):
        named = idst_ref[k : k + 1, :]
        same = jnp.where(((ids_ref[:, 0:1] == named) | (ids_ref[:, 1:2] == named)) & earlier, 1, 0)
        slot = named * 3 + jnp.sum(same, axis=0, keepdims=True)
        selects.append(picks((slot == dest * 6 + place) & (place < 6)))
        w = w_ref[:, k : k + 1]
        w_hi = w.astype(BF).astype(F32)
        side = jnp.where(lane == LANE_POS, local_pos, 0.0)
        side = jnp.where(lane == LANE_HI, w_hi, side)
        side = jnp.where(lane == LANE_LO, w - w_hi, side)
        side = jnp.where(lane == LANE_FLAG, 1.0 - k, side)
        sides.append(side.astype(BF))
    either = selects[0] + selects[1]
    sel_ref[...] = either
    first = (dest & 1) * 32 + t * 2
    token_row = picks((place >= 6) & (tok == first + place - 6))
    rope_row = picks((place < 2) & (tok == first + place))
    lat_part = dot(token_row, normed)
    out_ref[:, :128] = (dot(either, q_nope) + lat_part[:, :128]).astype(BF)
    out_ref[:, 128:256] = (dot(either, q_rest) + lat_part[:, 128:256]).astype(BF)
    out_ref[:, 256:384] = (dot(either, res) + lat_part[:, 256:384]).astype(BF)
    side = dot(selects[0], sides[0]) + dot(selects[1], sides[1]) + dot(rope_row, rope)
    out_ref[:, 384:] = (side + lat_part[:, 384:]).astype(BF)


def spread_kernel(arr_ref, out_ref):
    row, col = iota((TOK, 256), 0), iota((TOK, 256), 1)
    base = (row >> 1) * 8 + (row & 1)
    lat = dot(picks(col == base + 6), arr_ref[...]).astype(BF)
    side = arr_ref[:, 384:]
    packed = jnp.zeros((16, 128), F32)
    for b in range(4):
        near, far = iota((16, 256), 0) + 16 * b, iota((16, 256), 1)
        here = dot(picks(far == (near >> 1) * 8 + (near & 1)), side).astype(BF)
        src, dst = iota((128, 128), 0), iota((128, 128), 1)
        packed = packed + dot(here, picks((src < 32) & (dst == src + 32 * b)))
    packed = packed.astype(BF)
    for copy in range(N_TP):
        for f in range(4):
            out_ref[copy, f * TOK : (f + 1) * TOK, :] = lat[:, f * 128 : (f + 1) * 128]
        out_ref[copy, 4 * TOK :, :] = packed


def keys_kernel(lat_ref, wide_ref, narrow_ref, out_ref):
    rows = N_TP * TOK
    wide = jnp.zeros((rows, 256), F32)
    narrow = jnp.zeros((rows, 128), F32)
    for f in range(4):
        part = lat_ref[:, f * TOK : (f + 1) * TOK, :].reshape(rows, 128)
        wide = wide + dot(part, wide_ref[f * 128 : (f + 1) * 128, :])
        narrow = narrow + dot(part, narrow_ref[f * 128 : (f + 1) * 128, :])
    wide, narrow = wide.astype(BF), narrow.astype(BF)
    packed = lat_ref[:, 4 * TOK :, :].reshape(256, 128)
    src, dst = iota((128, 128), 0), iota((128, 128), 1)
    pieces = []
    for b in range(4):
        moved = dot(packed, picks((dst >= 96) & (src == dst - 96 + 32 * b)))
        pieces.append(moved.astype(BF).reshape(N_TP, 16, 128))
    rope = jnp.concatenate(pieces, axis=1).reshape(rows, 128)
    out_ref[0] = wide[:, :128]
    out_ref[1] = wide[:, 128:]
    shifted = dot(narrow, picks((src < 64) & (dst == src + 32)))
    out_ref[2] = (shifted + rope.astype(F32)).astype(BF)
    out_ref[3] = dot(narrow, picks((src >= 64) & (dst == src - 64))).astype(BF)


def attend_kernel(core_ref, arr_ref, own_ref, other_ref, wide_out_ref, narrow_out_ref, out_ref):
    core = core_ref[0]
    pick = slot_rows(arr_ref)
    q = dot(pick, arr_ref[:, :256]).astype(BF)
    side = dot(pick, arr_ref[:, 384:])
    row_pos = div6(iota((SLOTS, 1), 0)) * TOK + lane_value(side, LANE_POS).astype(jnp.int32)
    src, dst = iota((128, 128), 0), iota((128, 128), 1)
    q_rest = q[:, 128:]
    wide_q = jnp.concatenate([q[:, :128], dot(q_rest, picks((src < 32) & (dst == src + 96))).astype(BF)], axis=1)
    narrow_q = jnp.where(iota((SLOTS, 128), 1) >= 32, q_rest.astype(F32), 0.0).astype(BF)
    rows = N_TP * TOK
    n = iota((1, rows), 1)
    near = ((n & 63) >> 1) * TOK + (n >> 6) * 2 + (n & 1)
    wide_scores, narrow_scores, masks = [], [], []
    for half, ref in ((core, own_ref), (1 - core, other_ref)):
        allowed = near + half * 32 <= row_pos
        keys = jnp.concatenate([ref[0], ref[2]], axis=1)
        wide = dot_nt(wide_q, keys) * (160 ** -0.5)
        narrow = dot_nt(narrow_q, ref[2]) * (96 ** -0.5)
        wide_scores.append(jnp.where(allowed, wide, FLOOR))
        narrow_scores.append(jnp.where(allowed, narrow, FLOOR))

    def mixed(scores, at):
        peak = jnp.maximum(*[jnp.max(s, axis=1, keepdims=True) for s in scores])
        total, summed = 0.0, 0.0
        for s, ref in zip(scores, (own_ref, other_ref)):
            e = jnp.exp(s - peak)
            total = total + jnp.sum(e, axis=1, keepdims=True)
            summed = summed + dot(e.astype(BF), ref[at])
        return (summed / total).astype(BF)

    wide_att = mixed(wide_scores, 1)
    narrow_att = mixed(narrow_scores, 3)[:, :64]
    for piece in range(N_TP):
        cols = slice(piece * 128, (piece + 1) * 128)
        out_ref[piece] = (dot(wide_att, wide_out_ref[:, cols]) + dot(narrow_att, narrow_out_ref[:, cols])).astype(BF)


def stream_kernel(part_ref, arr_ref, out_ref):
    total = jnp.zeros((SLOTS, 128), F32)
    for piece in range(N_TP):
        total = total + part_ref[piece].astype(F32)
    res = dot(slot_rows(arr_ref), arr_ref[:, 256:384])
    stream = (res + total.astype(BF).astype(F32)).astype(BF)
    for copy in range(N_TP):
        out_ref[copy] = stream


def expert_kernel(x_ref, arr_ref, gain_ref, eg_ref, eu_ref, ed_ref, sg_ref, su_ref, sd_ref, out_ref):
    squares = jnp.zeros((SLOTS, 128), F32)
    for piece in range(N_TP):
        x = x_ref[piece].astype(F32)
        squares = squares + x * x
    scale = lax.rsqrt(jnp.sum(squares, axis=1, keepdims=True) * (1.0 / D_MODEL) + EPS)
    zero = jnp.zeros((SLOTS, 64), F32)
    gates, ups = [zero] * 3, [zero] * 3
    for piece in range(N_TP):
        cols = slice(piece * 128, (piece + 1) * 128)
        x = (x_ref[piece].astype(F32) * scale * gain_ref[:, cols]).astype(BF)
        for e in range(2):
            gates[e] = gates[e] + dot(x, eg_ref[e, cols, :])
            ups[e] = ups[e] + dot(x, eu_ref[e, cols, :])
        gates[2] = gates[2] + dot(x, sg_ref[cols, :])
        ups[2] = ups[2] + dot(x, su_ref[cols, :])
    hidden = [((g / (1.0 + jnp.exp(-g))) * u).astype(BF) for g, u in zip(gates, ups)]
    side = dot(slot_rows(arr_ref), arr_ref[:, 384:])
    weight = lane_value(side, LANE_HI) + lane_value(side, LANE_LO)
    flag = lane_value(side, LANE_FLAG)
    row = iota((SLOTS, 1), 0)
    second = div3(row) & 1
    first_hidden = jnp.where(second == 0, hidden[0].astype(F32), 0.0).astype(BF)
    second_hidden = jnp.where(second == 1, hidden[1].astype(F32), 0.0).astype(BF)
    for piece in range(N_TP):
        cols = slice(piece * 128, (piece + 1) * 128)
        routed = dot(first_hidden, ed_ref[0, :, cols]) + dot(second_hidden, ed_ref[1, :, cols])
        shared = dot(hidden[2], sd_ref[:, cols])
        out_ref[piece] = (weight * routed + flag * shared).astype(BF)


def give_back_kernel(part_ref, stream_ref, arr_ref, out_ref):
    total = jnp.zeros((SLOTS, 128), F32)
    for piece in range(N_TP):
        total = total + part_ref[piece].astype(F32)
    pick = slot_rows(arr_ref)
    flag = lane_value(dot(pick, arr_ref[:, 384:]), LANE_FLAG)
    total = (total + flag * stream_ref[...].astype(F32)).astype(BF)
    out_ref[...] = dot_tn(pick, total).astype(BF)


def finish_kernel(sel_ref, back_ref, out_ref):
    out_ref[...] = dot_tn(sel_ref[...], back_ref[...]).astype(BF)


VMEM = pl.BlockSpec(memory_space=pltpu.VMEM)
SMEM = pl.BlockSpec(memory_space=pltpu.SMEM)


def run(kernel, outs, *args, scalars=0):
    shapes = [jax.ShapeDtypeStruct(s, BF) for s in outs]
    got = pl.pallas_call(
        kernel,
        out_shape=shapes,
        in_specs=[SMEM] * scalars + [VMEM] * (len(args) - scalars),
        out_specs=[VMEM] * len(outs),
        name=kernel.__name__,
    )(*args)
    return got[0] if len(outs) == 1 else got


def swap_all(values, axes):
    return lax.all_to_all(values, axes, split_axis=0, concat_axis=0, tiled=True)


def local(
    wide_queries,
    narrow_queries,
    kv_latent,
    rope_key,
    latent_gain,
    wide_kv_weight,
    narrow_kv_weight,
    wide_out_weight,
    narrow_out_weight,
    residual,
    norm_gain,
    route_ids,
    route_weights,
    expert_gate,
    expert_up,
    expert_down,
    shared_gate,
    shared_up,
    shared_down,
):
    t = lax.axis_index("tp").astype(jnp.int32)[None]
    core = lax.axis_index("c").astype(jnp.int32)[None]
    lane = jnp.arange(128, dtype=jnp.int32)
    frequency = THETA ** (-2.0 * (lane % 16).astype(F32) / 32)
    positions = lax.axis_index(SP) * TOK + jnp.arange(TOK, dtype=jnp.int32)
    angles = positions.astype(F32)[:, None] * frequency[None, :]
    turning = ((lane < 32) | (lane >= 96))[None, :]
    cos = jnp.where(turning, jnp.cos(angles), 1.0)
    sign = jnp.where((lane & 16) == 0, -1.0, 1.0)[None, :]
    sin = jnp.where(turning, jnp.sin(angles) * sign, 0.0)
    queries = jnp.concatenate([wide_queries, narrow_queries], axis=1)
    rope = jnp.pad(rope_key, ((0, 0), (0, 96)))
    payload, chosen = run(
        pack_kernel, [(256, 512), (256, TOK)],
        t, queries, rope, kv_latent, latent_gain[None, :], residual, route_ids, route_ids.T, route_weights, cos, sin,
        scalars=1,
    )
    arrived = swap_all(payload.reshape(N_SP, 8, 512), SP).reshape(256, 512)
    latents = swap_all(run(spread_kernel, [(N_TP, 272, 128)], arrived), "tp")
    own = run(keys_kernel, [(4, N_TP * TOK, 128)], latents, wide_kv_weight, narrow_kv_weight)
    other = lax.ppermute(own, "c", [(0, 1), (1, 0)])
    partial = run(
        attend_kernel, [(N_TP, SLOTS, 128)], core, arrived, own, other, wide_out_weight, narrow_out_weight, scalars=1
    )
    copies = run(stream_kernel, [(N_TP, SLOTS, 128)], swap_all(partial, "tp"), arrived)
    rows = swap_all(copies, "tp")
    partial = run(
        expert_kernel, [(N_TP, SLOTS, 128)],
        rows, arrived, norm_gain[None, :], expert_gate, expert_up, expert_down, shared_gate, shared_up, shared_down,
    )
    back = run(give_back_kernel, [(256, 128)], swap_all(partial, "tp"), copies[0], arrived)
    back = swap_all(back.reshape(N_SP, 8, 128), SP).reshape(256, 128)
    return run(finish_kernel, [(TOK, 128)], chosen, back)


def solution(mesh):
    torus = Mesh(mesh.devices.reshape(16, 2, mesh.shape["tp"]), ("z", "c", "tp"))
    return jax.shard_map(
        local,
        mesh=torus,
        in_specs=(
            P(SP, "tp"),
            P(SP, "tp"),
            P(SP, None),
            P(SP, None),
            P(),
            P(None, "tp"),
            P(None, "tp"),
            P("tp", None),
            P("tp", None),
            P(SP, None),
            P(),
            P(SP, None),
            P(SP, None),
            P(SP, None, "tp"),
            P(SP, None, "tp"),
            P(SP, "tp", None),
            P(None, "tp"),
            P(None, "tp"),
            P("tp", None),
        ),
        out_specs=P(SP, "tp"),
        check_vma=False,
    )
```

time: 203 us -> 177 us (0.87)
  waiting for transfers between devices: 85.9 us -> 21.9 us
  blocking collectives: 48.9 us -> 101 us
  starting transfers between devices: 42.2 us -> 11.7 us
  Pallas kernels: 0 us -> 25.3 us
  matrix products: 9.18 us -> 0 us
  other arithmetic: 4.43 us -> 2.32 us
    all_to_all x6 -> x2, waiting for transfers between devices: 85.9 us -> 19.4 us  [swap_all(): return lax.all_to_all(values, axes, split_axis=0, concat_axis=0, tiled=True)]
    all_to_all x3 -> x4, blocking collectives: 48.9 us -> 101 us  [swap_all(): return lax.all_to_all(values, axes, split_axis=0, concat_axis=0, tiled=True)]
    all_to_all x6 -> x2, starting transfers between devices: 42.2 us -> 7.93 us  [swap_all(): return lax.all_to_all(values, axes, split_axis=0, concat_axis=0, tiled=True)]
    pallas_call x0 -> x8, Pallas kernels: none -> 25.3 us  [run(): pl.pallas_call(kernel, out_shape=shapes, in_specs=[SMEM] * scalars + [VME...]
    unnamed x30 -> x21, local copies, waits for them, and re-layouts: 0.47 us -> 11.1 us
    dot_general x10 -> x0, matrix products: 9.18 us -> none  [the longest x1 2.31 us: local(): jnp.einsum('hqv,hvd->qd', wide_att, wide_out_weight.reshape(wide_count, W...]
    ppermute x0 -> x1, starting transfers between devices: none -> 3.79 us  [local(): other = lax.ppermute(own, 'c', [(0, 1), (1, 0)])]
    ppermute x0 -> x1, waiting for transfers between devices: none -> 2.48 us  [local(): other = lax.ppermute(own, 'c', [(0, 1), (1, 0)])]
  transfers between devices with their start and end apart: 6 -> 3, of which waited for: 6 -> 3; matrix products, arithmetic and copies ran while one was open for 3% -> 4% of each run, Pallas kernels for 0% -> 0%
where the time goes in v1:
time: 177 us; the launch traced here: 176 us
  blocking collectives  101 us (57%)
  Pallas kernels  25.3 us (14%)
  waiting for transfers between devices  21.9 us (12%)
  local copies, waits for them, and re-layouts  13.1 us (7%)
  starting transfers between devices  11.7 us (7%)
  other arithmetic  2.32 us (1%)
    all_to_all x4, blocking collectives, swap_all(): return lax.all_to_all(values, axes, split_axis=0, concat_axis=0, tiled=True)  101 us
    pallas_call x8, Pallas kernels, run(): pl.pallas_call(kernel, out_shape=shapes, in_specs=[SMEM] * scalars + [VME...  25.3 us
    all_to_all x2, waiting for transfers between devices, swap_all(): return lax.all_to_all(values, axes, split_axis=0, concat_axis=0, tiled=True)  19.4 us
    unnamed x21, local copies, waits for them, and re-layouts  11.1 us
    all_to_all x2, starting transfers between devices, swap_all(): return lax.all_to_all(values, axes, split_axis=0, concat_axis=0, tiled=True)  7.93 us
    ppermute x1, starting transfers between devices, local(): other = lax.ppermute(own, 'c', [(0, 1), (1, 0)])  3.79 us
  transfers between devices with their start and end apart: 3, of which 3 were waited for; matrix products, arithmetic and copies ran while one was open for 4% of the time, Pallas kernels for 0%

profile of v1, /device:TPU:1, one launch (start us, length us, event | category | flops | bytes accessed | tf_op | source)
XLA Modules:
  0.0 175.5 jit_solution(10611449787006958960)
XLA Ops:
  0.0 0.8 copy.20
  0.8 1.4 copy.21.ids_ref
  2.2 1.4 copy.22.w_ref
  3.6 1.5 pad_maximum_fusion.q_ref
  5.0 0.6 pad.4.rope_ref
  5.7 0.8 fusion.2
  6.5 2.2 %pack_kernel.1 = (bf16[256,512]{1,0:T(8,128)(2,1)}, bf16[256,64]{1,0:T(8,128)(2,1)}) custom-call(s32[1]{0:T(128)} %bitcast.tp_ref, bf16[64,256]{1,0:T(8,128)(2,1)} %pad_maximum_fusion.q_ref, bf16[64,128]{1,0:T(8,128)(2,1)} %pad.4.rope_ref, bf16[64,512]{1,0:T(8,128)(2,1)} %lat_ref.1, f32[1,512]{1,0:T(1,128)} %bitcast.21, bf16[64,2048]{1,0:T(8,128)(2,1)} %res_ref.1, ...), custom_call_target="tpu_custom_call" | custom-call | tf_op jit(solution)/shard_map/pack_kernel/pallas_call | solution.py:252
  8.7 39.1 %all_to_all.30 = bf16[32,8,512]{2,1,0:T(8,128)(2,1)} all-to-all(bf16[32,8,512]{2,1,0:T(8,128)(2,1)} %bitcast.17), channel_id=1, replica_groups=mesh['z'=16,'c'=2,'tp'=16] {'z','c'}, dimensions={0} | all-to-all | bytes 524288 | tf_op jit(solution)/shard_map/all_to_all | solution.py:263
  47.8 2.5 %spread_kernel.1 = bf16[16,272,128]{2,1,0:T(8,128)(2,1)} custom-call(bf16[256,512]{1,0:T(8,128)(2,1)} %bitcast.11), custom_call_target="tpu_custom_call" | custom-call | tf_op jit(solution)/shard_map/spread_kernel/pallas_call | solution.py:252
  50.4 23.8 %all_to_all.31.lat_ref = bf16[16,272,128]{2,1,0:T(8,128)(2,1)} all-to-all(bf16[16,272,128]{2,1,0:T(8,128)(2,1)} %spread_kernel.1), channel_id=1, replica_groups=mesh['z'=16,'c'=2,'tp'=16] {'tp'}, dimensions={0} | all-to-all | bytes 2228224 | tf_op jit(solution)/shard_map/all_to_all | solution.py:263
  74.2 3.5 %keys_kernel.1.own_ref = bf16[4,1024,128]{2,1,0:T(8,128)(2,1)} custom-call(bf16[16,272,128]{2,1,0:T(8,128)(2,1)} %all_to_all.31.lat_ref, bf16[512,256]{1,0:T(8,128)(2,1)} %wide_ref.1, bf16[512,128]{1,0:T(8,128)(2,1)} %narrow_ref.1), custom_call_target="tpu_custom_call" | custom-call | tf_op jit(solution)/shard_map/keys_kernel/pallas_call | solution.py:252
  77.7 3.8 %collective-permute-start = (bf16[4,1024,128]{2,1,0:T(8,128)(2,1)}, bf16[4,1024,128]{2,1,0:T(8,128)(2,1)S(1)}, u32[]{:S(2)}, u32[]{:S(2)}) collective-permute-start(bf16[4,1024,128]{2,1,0:T(8,128)(2,1)} %keys_kernel.1.own_ref), channel_id=1, source_target_pairs={{0,16},{16,0},{1,17},{17,1},{2,18},{18,2},{3,19},{19,3},{4,20},{20... | collective-permute-start | bytes 3145736 | tf_op jit(solution)/shard_map/ppermute | solution.py:307
  81.5 2.5 %collective-permute-done.other_ref = bf16[4,1024,128]{2,1,0:T(8,128)(2,1)S(1)} collective-permute-done((bf16[4,1024,128]{2,1,0:T(8,128)(2,1)}, bf16[4,1024,128]{2,1,0:T(8,128)(2,1)S(1)}, u32[]{:S(2)}, u32[]{:S(2)}) %collective-permute-start) | collective-permute-done | bytes 1048608 | tf_op jit(solution)/shard_map/ppermute | solution.py:307
  84.0 1.0 copy-done.2
  84.9 5.1 %attend_kernel.1 = bf16[16,192,128]{2,1,0:T(8,128)(2,1)} custom-call(s32[1]{0:T(128)} %bitcast.3.core_ref, bf16[256,512]{1,0:T(8,128)(2,1)} %bitcast.12, bf16[4,1024,128]{2,1,0:T(8,128)(2,1)} %keys_kernel.1.own_ref, bf16[4,1024,128]{2,1,0:T(8,128)(2,1)} %copy-done.2, bf16[128,2048]{1,0:T(8,128)(2,1)} %wide_out_ref.1, bf16[64,2048]{1,0:T(8,128)(2,1)} %narrow_out_ref.1), custom_call_target="tpu_custom_call" | custom-call | tf_op jit(solution)/shard_map/attend_kernel/pallas_call | solution.py:252
  90.1 18.4 %all_to_all.32.part_ref = bf16[16,192,128]{2,1,0:T(8,128)(2,1)} all-to-all(bf16[16,192,128]{2,1,0:T(8,128)(2,1)} %attend_kernel.1), channel_id=1, replica_groups=mesh['z'=16,'c'=2,'tp'=16] {'tp'}, dimensions={0} | all-to-all | bytes 1572864 | tf_op jit(solution)/shard_map/all_to_all | solution.py:263
  108.5 2.3 %stream_kernel.1 = bf16[16,192,128]{2,1,0:T(8,128)(2,1)} custom-call(bf16[16,192,128]{2,1,0:T(8,128)(2,1)} %all_to_all.32.part_ref, bf16[256,512]{1,0:T(8,128)(2,1)} %bitcast.13), custom_call_target="tpu_custom_call" | custom-call | tf_op jit(solution)/shard_map/stream_kernel/pallas_call | solution.py:252
  110.8 3.7 %all-to-all-start.3 = ((bf16[16,192,128]{2,1,0:T(8,128)(2,1)}), bf16[16,192,128]{2,1,0:T(8,128)(2,1)S(1)}, u32[]{:S(2)}, u32[]{:S(2)}) async-start(bf16[16,192,128]{2,1,0:T(8,128)(2,1)} %stream_kernel.1), calls=%async_computation.3 | async-start | bytes 1572864 | tf_op jit(solution)/shard_map/all_to_all | solution.py:263
  114.5 1.3 copy.23.eg_ref
  115.9 1.3 copy.24.eu_ref
  117.2 1.0 copy.25.sg_ref
  118.3 1.0 copy.26.su_ref
  119.3 8.2 %all-to-all-done.3.x_ref = bf16[16,192,128]{2,1,0:T(8,128)(2,1)S(1)} async-done(((bf16[16,192,128]{2,1,0:T(8,128)(2,1)}), bf16[16,192,128]{2,1,0:T(8,128)(2,1)S(1)}, u32[]{:S(2)}, u32[]{:S(2)}) %all-to-all-start.3) | async-done | bytes 786464 | tf_op jit(solution)/shard_map/all_to_all | solution.py:263
  127.5 0.9 copy-done.1
  128.3 5.6 %expert_kernel.1 = bf16[16,192,128]{2,1,0:T(8,128)(2,1)} custom-call(bf16[16,192,128]{2,1,0:T(8,128)(2,1)} %copy-done.1, bf16[256,512]{1,0:T(8,128)(2,1)} %bitcast.14, f32[1,2048]{1,0:T(1,128)} %bitcast.19, bf16[2,2048,64]{2,1,0:T(8,128)(2,1)} %copy.23.eg_ref, bf16[2,2048,64]{2,1,0:T(8,128)(2,1)} %copy.24.eu_ref, bf16[2,64,2048]{2,1,0:T(8,128)(2,1)} %ed_ref.1, ...), custom_call_target="tpu_custom_call" | custom-call | tf_op jit(solution)/shard_map/expert_kernel/pallas_call | solution.py:252
  133.9 4.2 %all-to-all-start.4 = ((bf16[16,192,128]{2,1,0:T(8,128)(2,1)}), bf16[16,192,128]{2,1,0:T(8,128)(2,1)S(1)}, u32[]{:S(2)}, u32[]{:S(2)}) async-start(bf16[16,192,128]{2,1,0:T(8,128)(2,1)} %expert_kernel.1), calls=%async_computation.4 | async-start | bytes 1572864 | tf_op jit(solution)/shard_map/all_to_all | solution.py:263
  138.1 1.4 slice_bitcast_fusion.stream_ref
  139.5 11.3 %all-to-all-done.4.part_ref = bf16[16,192,128]{2,1,0:T(8,128)(2,1)S(1)} async-done(((bf16[16,192,128]{2,1,0:T(8,128)(2,1)}), bf16[16,192,128]{2,1,0:T(8,128)(2,1)S(1)}, u32[]{:S(2)}, u32[]{:S(2)}) %all-to-all-start.4) | async-done | bytes 786464 | tf_op jit(solution)/shard_map/all_to_all | solution.py:263
  150.8 0.9 copy-done
  151.7 2.3 %give_back_kernel.1 = bf16[256,128]{1,0:T(8,128)(2,1)} custom-call(bf16[16,192,128]{2,1,0:T(8,128)(2,1)} %copy-done, bf16[192,128]{1,0:T(8,128)(2,1)} %slice_bitcast_fusion.stream_ref, bf16[256,512]{1,0:T(8,128)(2,1)} %bitcast.15), custom_call_target="tpu_custom_call" | custom-call | tf_op jit(solution)/shard_map/give_back_kernel/pallas_call | solution.py:252
  154.0 19.8 %all_to_all.33 = bf16[32,8,128]{2,1,0:T(8,128)(2,1)} all-to-all(bf16[32,8,128]{2,1,0:T(8,128)(2,1)} %bitcast.16), channel_id=1, replica_groups=mesh['z'=16,'c'=2,'tp'=16] {'z','c'}, dimensions={0} | all-to-all | bytes 131072 | tf_op jit(solution)/shard_map/all_to_all | solution.py:263
  173.8 1.7 finish_kernel.1
  (14 shorter events, 0.0 us)
Async XLA Ops:
  77.7 6.3 %collective-permute-start = (bf16[4,1024,128]{2,1,0:T(8,128)(2,1)}, bf16[4,1024,128]{2,1,0:T(8,128)(2,1)S(1)}, u32[]{:S(2)}, u32[]{:S(2)}) collective-permute-start(bf16[4,1024,128]{2,1,0:T(8,128)(2,1)} %keys_kernel.1.own_ref), channel_id=1, source_target_pairs={{0,16},{16,0},{1,17},{17,1},{2,18},{18,2},{3,19},{19,3},{4,20},{20... | collective-permute-start | bytes 3145736 | tf_op jit(solution)/shard_map/ppermute | solution.py:307
  84.0 1.0 copy-start.2
  110.8 3.8 %copy-start.3 = (bf16[2,2048,64]{1,2,0:T(8,128)(2,1)S(1)}, bf16[2,2048,64]{1,2,0:T(8,128)(2,1)}, u32[]{:S(2)}) copy-start(bf16[2,2048,64]{1,2,0:T(8,128)(2,1)} %param.32) | copy-start | bytes 1572868
  110.8 16.7 %all-to-all-start.3 = ((bf16[16,192,128]{2,1,0:T(8,128)(2,1)}), bf16[16,192,128]{2,1,0:T(8,128)(2,1)S(1)}, u32[]{:S(2)}, u32[]{:S(2)}) async-start(bf16[16,192,128]{2,1,0:T(8,128)(2,1)} %stream_kernel.1), calls=%async_computation.3 | async-start | bytes 1572864 | tf_op jit(solution)/shard_map/all_to_all | solution.py:263
  114.5 1.3 copy-start.4
  115.9 1.3 copy-start.5
  115.9 2.4 %copy-start.6 = (bf16[2048,64]{0,1:T(8,128)(2,1)S(1)}, bf16[2048,64]{0,1:T(8,128)(2,1)}, u32[]{:S(2)}) copy-start(bf16[2048,64]{0,1:T(8,128)(2,1)} %param.36) | copy-start | bytes 786436
  127.5 0.9 copy-start.1
  133.9 16.9 %all-to-all-start.4 = ((bf16[16,192,128]{2,1,0:T(8,128)(2,1)}), bf16[16,192,128]{2,1,0:T(8,128)(2,1)S(1)}, u32[]{:S(2)}, u32[]{:S(2)}) async-start(bf16[16,192,128]{2,1,0:T(8,128)(2,1)} %expert_kernel.1), calls=%async_computation.4 | async-start | bytes 1572864 | tf_op jit(solution)/shard_map/all_to_all | solution.py:263
  150.8 0.9 copy-start

commit v2 on v1

v2 whole, which is shorter than its diff:
```python
import functools

import jax
import jax.numpy as jnp
from jax import lax
from jax.experimental import pallas as pl
from jax.experimental.pallas import tpu as pltpu
from jax.sharding import Mesh
from jax.sharding import PartitionSpec as P

D_MODEL = 2048
THETA = 10000.0
EPS = 1e-06
FLOOR = -1e30
SP = ("z", "c")
N_SP = 32
N_TP = 16
TOK = 64
SLOTS = 192
F32 = jnp.float32
BF = jnp.bfloat16

LANE_POS, LANE_HI, LANE_LO, LANE_FLAG = 64, 65, 66, 67


def iota(shape, dim):
    return lax.broadcasted_iota(jnp.int32, shape, dim)


def div6(v):
    return (v * 10923) >> 16


def div3(v):
    return (v * 21846) >> 16


def dot(a, b):
    return jnp.dot(a, b, preferred_element_type=F32)


def dot_nt(a, b):
    return lax.dot_general(a, b, (((1,), (1,)), ((), ())), preferred_element_type=F32)


def dot_tn(a, b):
    return lax.dot_general(a, b, (((0,), (0,)), ((), ())), preferred_element_type=F32)


def exact_tn(a, b):
    return lax.dot_general(
        a, b, (((0,), (0,)), ((), ())), precision=lax.Precision.HIGHEST, preferred_element_type=F32
    )


def picks(mask):
    return jnp.where(mask, 1.0, 0.0).astype(BF)


def lane_value(block, lane):
    return jnp.sum(jnp.where(iota(block.shape, 1) == lane, block, 0.0), axis=1, keepdims=True)


def slot_rows():
    row, col = iota((SLOTS, 256), 0), iota((SLOTS, 256), 1)
    source = div6(row)
    return picks(col == source * 8 + (row - source * 6))


def pack_kernel(tp_ref, wide_ref, narrow_ref, rope_ref, lat_ref, gain_ref, res_ref, ids_ref, w_ref, cos_ref, sin_ref, out_ref, sel_ref):
    t = tp_ref[0]
    src, dst = iota((16, 128), 0), iota((16, 128), 1)
    turning = (dst < 32) | (dst >= 96)
    spread = jnp.where(turning & ((dst & 15) == src), 1.0, 0.0)
    cos = exact_tn(cos_ref[...], spread) + jnp.where((iota((TOK, 128), 1) >= 32) & (iota((TOK, 128), 1) < 96), 1.0, 0.0)
    sin = exact_tn(sin_ref[...], jnp.where((dst & 16) == 0, -spread, spread))
    src, dst = iota((128, 128), 0), iota((128, 128), 1)
    swap = picks(src == dst + jnp.where((dst & 16) == 0, 16, -16))

    def turned(block):
        return (block.astype(F32) * cos + dot(block, swap) * sin).astype(BF)

    first, after = picks(src == dst), picks(src + 32 == dst)
    q_rest = turned((dot(wide_ref[:, 128:], first[:32]) + dot(narrow_ref[...], after[:96])).astype(BF))
    rope = turned(dot_tn(rope_ref[...], first[:32]).astype(BF))
    lat = lat_ref[...].astype(F32)
    scaled = lat * lax.rsqrt(jnp.mean(lat * lat, axis=1, keepdims=True) + EPS)
    normed = (scaled * gain_ref[...]).astype(BF)
    res = res_ref[:, pl.ds(pl.multiple_of(t * 128, 128), 128)]

    before = picks(iota((TOK, TOK), 0) < iota((TOK, TOK), 1))
    named = [jnp.where(ids_ref[k : k + 1, :] == iota((TOK, TOK), 0), 1.0, 0.0) for k in range(2)]
    rank = dot((named[0] + named[1]).astype(BF), before)
    row, tok = iota((256, TOK), 0), iota((256, TOK), 1)
    dest, place = row >> 3, row & 7
    selects, high, low = [], 0.0, 0.0
    for k in range(2):
        slot = ids_ref[k : k + 1, :] * 3 + jnp.sum(named[k] * rank, axis=0, keepdims=True).astype(jnp.int32)
        mask = (slot == dest * 6 + place) & (place < 6)
        selects.append(picks(mask))
        w = w_ref[k : k + 1, :]
        w_hi = w.astype(BF).astype(F32)
        high = high + jnp.where(mask, w_hi, 0.0)
        low = low + jnp.where(mask, w - w_hi, 0.0)
    either = selects[0] + selects[1]
    sel_ref[...] = either
    start = (dest & 1) * 32 + t * 2
    token_row = picks((place >= 6) & (tok == start + place - 6))
    rope_row = picks((place < 2) & (tok == start + place))
    lat_part = dot(token_row, normed)
    out_ref[:, :128] = (dot(either, wide_ref[:, :128]) + lat_part[:, :128]).astype(BF)
    out_ref[:, 128:256] = (dot(either, q_rest) + lat_part[:, 128:256]).astype(BF)
    out_ref[:, 256:384] = (dot(either, res) + lat_part[:, 256:384]).astype(BF)
    lane, token = iota((TOK, 128), 1), iota((TOK, 128), 0).astype(F32)
    side = dot(either, jnp.where(lane == LANE_POS, token, 0.0).astype(BF))
    side = side + dot(high.astype(BF), picks(lane == LANE_HI)) + dot(low.astype(BF), picks(lane == LANE_LO))
    side = side + dot(selects[0], picks(lane == LANE_FLAG)) + dot(rope_row, rope)
    out_ref[:, 384:] = (side + lat_part[:, 384:]).astype(BF)


def slots_kernel(arr_ref, out_ref):
    out_ref[...] = dot(slot_rows(), arr_ref[...]).astype(BF)


def spread_kernel(arr_ref, out_ref):
    row, col = iota((TOK, 256), 0), iota((TOK, 256), 1)
    base = (row >> 1) * 8 + (row & 1)
    lat = dot(picks(col == base + 6), arr_ref[...]).astype(BF)
    side = arr_ref[:, 384:]
    packed = jnp.zeros((16, 128), F32)
    for b in range(4):
        near, far = iota((16, 256), 0) + 16 * b, iota((16, 256), 1)
        here = dot(picks(far == (near >> 1) * 8 + (near & 1)), side).astype(BF)
        src, dst = iota((128, 128), 0), iota((128, 128), 1)
        packed = packed + dot(here, picks((src < 32) & (dst == src + 32 * b)))
    packed = packed.astype(BF)
    for copy in range(N_TP):
        for f in range(4):
            out_ref[copy, f * TOK : (f + 1) * TOK, :] = lat[:, f * 128 : (f + 1) * 128]
        out_ref[copy, 4 * TOK :, :] = packed


def keys_kernel(lat_ref, wide_ref, narrow_ref, out_ref):
    rows = N_TP * TOK
    wide = jnp.zeros((rows, 256), F32)
    narrow = jnp.zeros((rows, 128), F32)
    for f in range(4):
        part = lat_ref[:, f * TOK : (f + 1) * TOK, :].reshape(rows, 128)
        wide = wide + dot(part, wide_ref[f * 128 : (f + 1) * 128, :])
        narrow = narrow + dot(part, narrow_ref[f * 128 : (f + 1) * 128, :])
    wide, narrow = wide.astype(BF), narrow.astype(BF)
    packed = lat_ref[:, 4 * TOK :, :].reshape(256, 128)
    src, dst = iota((128, 128), 0), iota((128, 128), 1)
    pieces = []
    for b in range(4):
        moved = dot(packed, picks((dst >= 96) & (src == dst - 96 + 32 * b)))
        pieces.append(moved.astype(BF).reshape(N_TP, 16, 128))
    rope = jnp.concatenate(pieces, axis=1).reshape(rows, 128)
    out_ref[0] = wide[:, :128]
    out_ref[1] = wide[:, 128:]
    shifted = dot(narrow, picks((src < 64) & (dst == src + 32)))
    out_ref[2] = (shifted + rope.astype(F32)).astype(BF)
    out_ref[3] = dot(narrow, picks((src >= 64) & (dst == src - 64))).astype(BF)


def attend_kernel(core_ref, slot_ref, own_ref, other_ref, wide_out_ref, narrow_out_ref, out_ref):
    core = core_ref[0]
    q = slot_ref[:, :256]
    side = slot_ref[:, 384:].astype(F32)
    row_pos = div6(iota((SLOTS, 1), 0)) * TOK + lane_value(side, LANE_POS).astype(jnp.int32)
    src, dst = iota((128, 128), 0), iota((128, 128), 1)
    q_rest = q[:, 128:]
    wide_q = jnp.concatenate([q[:, :128], dot(q_rest, picks((src < 32) & (dst == src + 96))).astype(BF)], axis=1)
    narrow_q = jnp.where(iota((SLOTS, 128), 1) >= 32, q_rest.astype(F32), 0.0).astype(BF)
    rows = N_TP * TOK
    n = iota((1, rows), 1)
    near = ((n & 63) >> 1) * TOK + (n >> 6) * 2 + (n & 1)
    wide_scores, narrow_scores, masks = [], [], []
    for half, ref in ((core, own_ref), (1 - core, other_ref)):
        allowed = near + half * 32 <= row_pos
        keys = jnp.concatenate([ref[0], ref[2]], axis=1)
        wide = dot_nt(wide_q, keys) * (160 ** -0.5)
        narrow = dot_nt(narrow_q, ref[2]) * (96 ** -0.5)
        wide_scores.append(jnp.where(allowed, wide, FLOOR))
        narrow_scores.append(jnp.where(allowed, narrow, FLOOR))

    def mixed(scores, at):
        peak = jnp.maximum(*[jnp.max(s, axis=1, keepdims=True) for s in scores])
        total, summed = 0.0, 0.0
        for s, ref in zip(scores, (own_ref, other_ref)):
            e = jnp.exp(s - peak)
            total = total + jnp.sum(e, axis=1, keepdims=True)
            summed = summed + dot(e.astype(BF), ref[at])
        return (summed / total).astype(BF)

    wide_att = mixed(wide_scores, 1)
    narrow_att = mixed(narrow_scores, 3)[:, :64]
    for piece in range(N_TP):
        cols = slice(piece * 128, (piece + 1) * 128)
        out_ref[piece] = (dot(wide_att, wide_out_ref[:, cols]) + dot(narrow_att, narrow_out_ref[:, cols])).astype(BF)


def stream_kernel(part_ref, slot_ref, out_ref):
    total = jnp.zeros((SLOTS, 128), F32)
    for piece in range(N_TP):
        total = total + part_ref[piece].astype(F32)
    stream = (slot_ref[:, 256:384].astype(F32) + total.astype(BF).astype(F32)).astype(BF)
    for copy in range(N_TP):
        out_ref[copy] = stream


def expert_kernel(x_ref, slot_ref, gain_ref, eg_ref, eu_ref, ed_ref, sg_ref, su_ref, sd_ref, out_ref):
    squares = jnp.zeros((SLOTS, 128), F32)
    for piece in range(N_TP):
        x = x_ref[piece].astype(F32)
        squares = squares + x * x
    scale = lax.rsqrt(jnp.sum(squares, axis=1, keepdims=True) * (1.0 / D_MODEL) + EPS)
    into = jnp.zeros((SLOTS, 384), F32)
    for pair in range(N_TP // 2):
        cols = slice(pair * 256, (pair + 1) * 256)
        x = jnp.concatenate([x_ref[2 * pair], x_ref[2 * pair + 1]], axis=1).astype(F32)
        x = (x * scale * gain_ref[:, cols]).astype(BF)
        weights = [eg_ref[0, :, cols], eg_ref[1, :, cols], sg_ref[:, cols], eu_ref[0, :, cols], eu_ref[1, :, cols], su_ref[:, cols]]
        into = into + dot_nt(x, jnp.concatenate(weights, axis=0))
    gate, up = into[:, :192], into[:, 192:]
    hidden = (gate / (1.0 + jnp.exp(-gate))) * up
    side = slot_ref[:, 384:].astype(F32)
    weight = lane_value(side, LANE_HI) + lane_value(side, LANE_LO)
    flag = lane_value(side, LANE_FLAG)
    owner = div3(iota((SLOTS, 128), 0)) & 1
    routed_hidden = jnp.where(owner == (iota((SLOTS, 128), 1) >> 6), hidden[:, :128], 0.0).astype(BF)
    shared_hidden = hidden[:, 128:].astype(BF)
    for piece in range(N_TP // 2):
        cols = slice(piece * 256, (piece + 1) * 256)
        routed = dot(routed_hidden, ed_ref[:, cols])
        shared = dot(shared_hidden, sd_ref[:, cols])
        both = (weight * routed + flag * shared).astype(BF)
        out_ref[2 * piece] = both[:, :128]
        out_ref[2 * piece + 1] = both[:, 128:]


def give_back_kernel(part_ref, stream_ref, slot_ref, out_ref):
    total = jnp.zeros((SLOTS, 128), F32)
    for piece in range(N_TP):
        total = total + part_ref[piece].astype(F32)
    flag = lane_value(slot_ref[:, 384:].astype(F32), LANE_FLAG)
    total = (total + flag * stream_ref[0].astype(F32)).astype(BF)
    out_ref[...] = dot_tn(slot_rows(), total).astype(BF)


def finish_kernel(sel_ref, back_ref, out_ref):
    out_ref[...] = dot_tn(sel_ref[...], back_ref[...]).astype(BF)


VMEM = pl.BlockSpec(memory_space=pltpu.VMEM)
SMEM = pl.BlockSpec(memory_space=pltpu.SMEM)


def run(kernel, outs, *args, scalars=0, plain=0, spread=True):
    placed = [pltpu.with_memory_space_constraint(a, pltpu.VMEM) for a in args[max(scalars, plain) :]]
    args = [*args[: max(scalars, plain)], *placed]
    return pl.pallas_call(
        kernel,
        out_shape=[pltpu.VMEM(shape, BF) for shape in outs] if spread else jax.ShapeDtypeStruct(outs[0], BF),
        in_specs=[SMEM] * scalars + [VMEM] * (len(args) - scalars),
        out_specs=[VMEM] * len(outs) if spread else VMEM,
        compiler_params=pltpu.CompilerParams(vmem_limit_bytes=24 << 20),
        name=kernel.__name__,
    )(*args)


def swap_all(values, axes):
    return lax.all_to_all(values, axes, split_axis=0, concat_axis=0, tiled=True)


def local(
    wide_queries,
    narrow_queries,
    kv_latent,
    rope_key,
    latent_gain,
    wide_kv_weight,
    narrow_kv_weight,
    wide_out_weight,
    narrow_out_weight,
    residual,
    norm_gain,
    route_ids,
    route_weights,
    expert_gate,
    expert_up,
    expert_down,
    shared_gate,
    shared_up,
    shared_down,
):
    t = lax.axis_index("tp").astype(jnp.int32)[None]
    core = lax.axis_index("c").astype(jnp.int32)[None]
    frequency = THETA ** (-2.0 * jnp.arange(16, dtype=F32) / 32)
    positions = lax.axis_index(SP) * TOK + jnp.arange(TOK, dtype=jnp.int32)
    angles = frequency[:, None] * positions.astype(F32)[None, :]
    payload, chosen = run(
        pack_kernel, [(256, 512), (256, TOK)],
        t, wide_queries, narrow_queries, rope_key.T, kv_latent, latent_gain[None, :], residual,
        route_ids.T, route_weights.T, jnp.cos(angles), jnp.sin(angles),
        scalars=1,
        plain=9,
    )
    arrived = swap_all(payload.reshape(N_SP, 8, 512), SP).reshape(256, 512)
    (spread,) = run(spread_kernel, [(N_TP, 272, 128)], arrived)
    latents = swap_all(spread, "tp")
    (slots,) = run(slots_kernel, [(SLOTS, 512)], arrived)
    (own,) = run(keys_kernel, [(4, N_TP * TOK, 128)], latents, wide_kv_weight, narrow_kv_weight)
    other = lax.ppermute(own, "c", [(0, 1), (1, 0)])
    (partial,) = run(
        attend_kernel, [(N_TP, SLOTS, 128)], core, slots, own, other, wide_out_weight, narrow_out_weight, scalars=1
    )
    (copies,) = run(stream_kernel, [(N_TP, SLOTS, 128)], swap_all(partial, "tp"), slots)
    rows = swap_all(copies, "tp")
    (partial,) = run(
        expert_kernel, [(N_TP, SLOTS, 128)],
        rows, slots, norm_gain[None, :],
        expert_gate.swapaxes(1, 2), expert_up.swapaxes(1, 2), expert_down.reshape(128, D_MODEL),
        shared_gate.T, shared_up.T, shared_down,
    )
    (back,) = run(give_back_kernel, [(256, 128)], swap_all(partial, "tp"), copies, slots)
    back = swap_all(back.reshape(N_SP, 8, 128), SP).reshape(256, 128)
    return run(finish_kernel, [(TOK, 128)], chosen, back, spread=False)


def solution(mesh):
    torus = Mesh(mesh.devices.reshape(16, 2, mesh.shape["tp"]), ("z", "c", "tp"))
    return jax.shard_map(
        local,
        mesh=torus,
        in_specs=(
            P(SP, "tp"),
            P(SP, "tp"),
            P(SP, None),
            P(SP, None),
            P(),
            P(None, "tp"),
            P(None, "tp"),
            P("tp", None),
            P("tp", None),
            P(SP, None),
            P(),
            P(SP, None),
            P(SP, None),
            P(SP, None, "tp"),
            P(SP, None, "tp"),
            P(SP, "tp", None),
            P(None, "tp"),
            P(None, "tp"),
            P("tp", None),
        ),
        out_specs=P(SP, "tp"),
        check_vma=False,
    )
```

time: 177 us -> 150 us (0.85)
  blocking collectives: 101 us -> 129 us
  waiting for transfers between devices: 21.9 us -> 2.05 us
  Pallas kernels: 25.3 us -> 7.81 us
  starting transfers between devices: 11.7 us -> 3.8 us
  local copies, waits for them, and re-layouts: 13.1 us -> 6.05 us
  other arithmetic: 2.32 us -> 0.13 us
    all_to_all x4 -> x6, blocking collectives: 101 us -> 129 us  [swap_all(): return lax.all_to_all(values, axes, split_axis=0, concat_axis=0, tiled=True)]
    all_to_all x2 -> x0, waiting for transfers between devices: 19.4 us -> none  [swap_all(): return lax.all_to_all(values, axes, split_axis=0, concat_axis=0, tiled=True)]
    pallas_call x8 -> x9, Pallas kernels: 25.3 us -> 7.81 us  [run(): pl.pallas_call(kernel, out_shape=[pltpu.VMEM(shape, BF) for shape in outs...]
    all_to_all x2 -> x0, starting transfers between devices: 7.93 us -> none  [swap_all(): return lax.all_to_all(values, axes, split_axis=0, concat_axis=0, tiled=True)]
    unnamed x21 -> x38, local copies, waits for them, and re-layouts: 11.1 us -> 6.05 us
  transfers between devices with their start and end apart: 3 -> 1, of which waited for: 3 -> 1; matrix products, arithmetic and copies ran while one was open for 4% -> 0% of each run, Pallas kernels for 0% -> 0%
where the time goes in v2:
time: 150 us; the launch traced here: 149 us
  blocking collectives  129 us (86%)
  Pallas kernels  7.81 us (5%)
  local copies, waits for them, and re-layouts  6.05 us (4%)
  starting transfers between devices  3.8 us (3%)
  waiting for transfers between devices  2.05 us (1%)
    all_to_all x6, blocking collectives, swap_all(): return lax.all_to_all(values, axes, split_axis=0, concat_axis=0, tiled=True)  129 us
    pallas_call x9, Pallas kernels, run(): pl.pallas_call(kernel, out_shape=[pltpu.VMEM(shape, BF) for shape in outs...  7.81 us
    unnamed x38, local copies, waits for them, and re-layouts  6.05 us
    ppermute x1, starting transfers between devices, local(): other = lax.ppermute(own, 'c', [(0, 1), (1, 0)])  3.8 us
  transfers between devices with their start and end apart: 1, of which 1 were waited for; matrix products, arithmetic and copies ran while one was open for 0% of the time, Pallas kernels for 0%

profile of v2, /device:TPU:1, one launch (start us, length us, event | category | flops | bytes accessed | tf_op | source)
XLA Modules:
  0.0 149.2 jit_solution(3665375120354142355)
XLA Ops:
  0.0 0.1 multiply_sine_fusion
  0.2 0.0 copy-start.9
  0.2 0.9 copy-done.9
  1.1 0.8 copy-done.11
  1.9 0.8 copy-done.12
  2.7 0.7 copy-done.13
  3.4 0.7 copy-done.15
  4.1 0.7 copy-done.16
  4.8 0.7 copy-done.17
  5.5 0.7 copy-done.18
  6.2 0.8 pack_kernel.1
  7.0 38.8 %all_to_all.30 = bf16[32,8,512]{2,1,0:T(8,128)(2,1)S(1)} all-to-all(bf16[32,8,512]{2,1,0:T(8,128)(2,1)S(1)} %bitcast.24), channel_id=1, replica_groups=mesh['z'=16,'c'=2,'tp'=16] {'z','c'}, dimensions={0} | all-to-all | bytes 524288 | tf_op jit(solution)/shard_map/all_to_all | solution.py:273
  45.8 0.6 spread_kernel.1
  46.4 0.0 copy-start.10
  46.4 23.6 %all_to_all.31.lat_ref = bf16[16,272,128]{2,1,0:T(8,128)(2,1)S(1)} all-to-all(bf16[16,272,128]{2,1,0:T(8,128)(2,1)S(1)} %spread_kernel.1), channel_id=1, replica_groups=mesh['z'=16,'c'=2,'tp'=16] {'tp'}, dimensions={0} | all-to-all | bytes 2228224 | tf_op jit(solution)/shard_map/all_to_all | solution.py:273
  70.0 1.2 keys_kernel.1.own_ref
  71.2 3.8 %collective-permute-start = (bf16[4,1024,128]{2,1,0:T(8,128)(2,1)S(1)}, bf16[4,1024,128]{2,1,0:T(8,128)(2,1)S(1)}, u32[]{:S(2)}, u32[]{:S(2)}) collective-permute-start(bf16[4,1024,128]{2,1,0:T(8,128)(2,1)S(1)} %keys_kernel.1.own_ref), channel_id=1, source_target_pairs={{0,16},{16,0},{1,17},{17,1},{2,18},{18,2},{3,19},{19,3},{4,20},{20... | collective-permute-start | bytes 3145736 | tf_op jit(solution)/shard_map/ppermute | solution.py:314
  75.0 0.2 slots_kernel.1.slot_ref
  75.2 2.1 %collective-permute-done.other_ref = bf16[4,1024,128]{2,1,0:T(8,128)(2,1)S(1)} collective-permute-done((bf16[4,1024,128]{2,1,0:T(8,128)(2,1)S(1)}, bf16[4,1024,128]{2,1,0:T(8,128)(2,1)S(1)}, u32[]{:S(2)}, u32[]{:S(2)}) %collective-permute-start) | collective-permute-done | bytes 1048608 | tf_op jit(solution)/shard_map/ppermute | solution.py:314
  77.3 2.3 %attend_kernel.1 = bf16[16,192,128]{2,1,0:T(8,128)(2,1)S(1)} custom-call(s32[1]{0:T(128)} %bitcast.5.core_ref, bf16[192,512]{1,0:T(8,128)(2,1)S(1)} %slots_kernel.1.slot_ref, bf16[4,1024,128]{2,1,0:T(8,128)(2,1)S(1)} %keys_kernel.1.own_ref, bf16[4,1024,128]{2,1,0:T(8,128)(2,1)S(1)} %collective-permute-done.other_ref, bf16[128,2048]{1,0:T(8,128)(2,1)S(1)} %copy-done, ...), custom_call_target="tpu_custom_call" | custom-call | tf_op jit(solution)/shard_map/attend_kernel/pallas_call | solution.py:262
  79.6 16.7 %all_to_all.32.part_ref = bf16[16,192,128]{2,1,0:T(8,128)(2,1)S(1)} all-to-all(bf16[16,192,128]{2,1,0:T(8,128)(2,1)S(1)} %attend_kernel.1), channel_id=1, replica_groups=mesh['z'=16,'c'=2,'tp'=16] {'tp'}, dimensions={0} | all-to-all | bytes 1572864 | tf_op jit(solution)/shard_map/all_to_all | solution.py:273
  96.3 0.1 stream_kernel.1.stream_ref
  96.4 0.0 copy-start.1
  96.4 0.0 copy-start.2
  96.4 0.0 copy-start.3
  96.4 0.0 copy-start.14
  96.5 16.5 %all_to_all.33.x_ref = bf16[16,192,128]{2,1,0:T(8,128)(2,1)S(1)} all-to-all(bf16[16,192,128]{2,1,0:T(8,128)(2,1)S(1)} %stream_kernel.1.stream_ref), channel_id=1, replica_groups=mesh['z'=16,'c'=2,'tp'=16] {'tp'}, dimensions={0} | all-to-all | bytes 1572864 | tf_op jit(solution)/shard_map/all_to_all | solution.py:273
  113.0 1.5 %expert_kernel.1 = bf16[16,192,128]{2,1,0:T(8,128)(2,1)S(1)} custom-call(bf16[16,192,128]{2,1,0:T(8,128)(2,1)S(1)} %all_to_all.33.x_ref, bf16[192,512]{1,0:T(8,128)(2,1)S(1)} %slots_kernel.1.slot_ref, f32[1,2048]{1,0:T(1,128)S(1)} %bitcast.26, bf16[2,64,2048]{2,1,0:T(8,128)(2,1)S(1)} %bitcast.18, bf16[2,64,2048]{2,1,0:T(8,128)(2,1)S(1)} %bitcast.19, ...), custom_call_target="tpu_custom_call" | custom-call | tf_op jit(solution)/shard_map/expert_kernel/pallas_call | solution.py:262
  114.5 14.8 %all_to_all.34.part_ref = bf16[16,192,128]{2,1,0:T(8,128)(2,1)S(1)} all-to-all(bf16[16,192,128]{2,1,0:T(8,128)(2,1)S(1)} %expert_kernel.1), channel_id=1, replica_groups=mesh['z'=16,'c'=2,'tp'=16] {'tp'}, dimensions={0} | all-to-all | bytes 1572864 | tf_op jit(solution)/shard_map/all_to_all | solution.py:273
  129.3 0.3 give_back_kernel.1
  129.6 18.8 %all_to_all.35 = bf16[32,8,128]{2,1,0:T(8,128)(2,1)S(1)} all-to-all(bf16[32,8,128]{2,1,0:T(8,128)(2,1)S(1)} %bitcast.23), channel_id=1, replica_groups=mesh['z'=16,'c'=2,'tp'=16] {'z','c'}, dimensions={0} | all-to-all | bytes 131072 | tf_op jit(solution)/shard_map/all_to_all | solution.py:273
  148.4 0.8 finish_kernel.1
  (26 shorter events, 0.1 us)
Async XLA Ops:
  0.2 1.0 copy-start.9
  1.1 0.8 copy-start.11
  1.9 0.8 copy-start.12
  2.7 0.7 copy-start.13
  3.4 0.7 copy-start.15
  4.1 0.7 copy-start.16
  4.8 0.7 copy-start.17
  5.5 0.7 copy-start.18
  46.4 23.7 %copy-start.4 = (bf16[512,256]{1,0:T(8,128)(2,1)S(1)}, bf16[512,256]{1,0:T(8,128)(2,1)}, u32[]{:S(2)}) copy-start(bf16[512,256]{1,0:T(8,128)(2,1)} %wide_ref.3) | copy-start | bytes 786436
  46.4 23.7 %copy-start.10 = (bf16[512,128]{1,0:T(8,128)(2,1)S(1)}, bf16[512,128]{1,0:T(8,128)(2,1)}, u32[]{:S(2)}) copy-start(bf16[512,128]{1,0:T(8,128)(2,1)} %narrow_ref.3) | copy-start | bytes 393220
  70.0 7.3 %copy-start = (bf16[128,2048]{1,0:T(8,128)(2,1)S(1)}, bf16[128,2048]{1,0:T(8,128)(2,1)}, u32[]{:S(2)}) copy-start(bf16[128,2048]{1,0:T(8,128)(2,1)} %wide_out_ref.1) | copy-start | bytes 1572868
  70.0 7.3 %copy-start.5 = (bf16[64,2048]{1,0:T(8,128)(2,1)S(1)}, bf16[64,2048]{1,0:T(8,128)(2,1)}, u32[]{:S(2)}) copy-start(bf16[64,2048]{1,0:T(8,128)(2,1)} %narrow_out_ref.1) | copy-start | bytes 786436
  71.2 6.1 %collective-permute-start = (bf16[4,1024,128]{2,1,0:T(8,128)(2,1)S(1)}, bf16[4,1024,128]{2,1,0:T(8,128)(2,1)S(1)}, u32[]{:S(2)}, u32[]{:S(2)}) collective-permute-start(bf16[4,1024,128]{2,1,0:T(8,128)(2,1)S(1)} %keys_kernel.1.own_ref), channel_id=1, source_target_pairs={{0,16},{16,0},{1,17},{17,1},{2,18},{18,2},{3,19},{19,3},{4,20},{20... | collective-permute-start | bytes 3145736 | tf_op jit(solution)/shard_map/ppermute | solution.py:314
  96.2 16.7 %copy-start.6 = (bf16[2048,64]{0,1:T(8,128)(2,1)S(1)}, bf16[2048,64]{0,1:T(8,128)(2,1)}, u32[]{:S(2)}) copy-start(bf16[2048,64]{0,1:T(8,128)(2,1)} %param.35) | copy-start | bytes 786436
  96.3 16.7 %copy-start.7 = (bf16[2048,64]{0,1:T(8,128)(2,1)S(1)}, bf16[2048,64]{0,1:T(8,128)(2,1)}, u32[]{:S(2)}) copy-start(bf16[2048,64]{0,1:T(8,128)(2,1)} %param.36) | copy-start | bytes 786436
  96.3 16.7 %copy-start.8 = (bf16[64,2048]{1,0:T(8,128)(2,1)S(1)}, bf16[64,2048]{1,0:T(8,128)(2,1)}, u32[]{:S(2)}) copy-start(bf16[64,2048]{1,0:T(8,128)(2,1)} %sd_ref.1) | copy-start | bytes 786436
  96.4 16.5 %copy-start.1 = (bf16[2,2048,64]{1,2,0:T(8,128)(2,1)S(1)}, bf16[2,2048,64]{1,2,0:T(8,128)(2,1)}, u32[]{:S(2)}) copy-start(bf16[2,2048,64]{1,2,0:T(8,128)(2,1)} %param.32) | copy-start | bytes 1572868
  96.4 16.5 %copy-start.2 = (bf16[2,2048,64]{1,2,0:T(8,128)(2,1)S(1)}, bf16[2,2048,64]{1,2,0:T(8,128)(2,1)}, u32[]{:S(2)}) copy-start(bf16[2,2048,64]{1,2,0:T(8,128)(2,1)} %param.33) | copy-start | bytes 1572868
  96.4 16.5 %copy-start.3 = (bf16[2,64,2048]{2,1,0:T(8,128)(2,1)S(1)}, bf16[2,64,2048]{2,1,0:T(8,128)(2,1)}, u32[]{:S(2)}) copy-start(bf16[2,64,2048]{2,1,0:T(8,128)(2,1)} %param.34) | copy-start | bytes 1572868
  96.4 16.5 %copy-start.14 = (f32[2048]{0:T(1024)S(1)}, f32[2048]{0:T(1024)}, u32[]{:S(2)}) copy-start(f32[2048]{0:T(1024)} %param.29) | copy-start | bytes 24580

commit v3 on v2

--- a/solution.py
+++ b/solution.py
@@ -163,8 +163,7 @@
     out_ref[3] = dot(narrow, picks((src >= 64) & (dst == src - 64))).astype(BF)
 
 
-def attend_kernel(core_ref, slot_ref, own_ref, other_ref, wide_out_ref, narrow_out_ref, out_ref):
-    core = core_ref[0]
+def half_attention(half, slot_ref, kv_ref):
     q = slot_ref[:, :256]
     side = slot_ref[:, 384:].astype(F32)
     row_pos = div6(iota((SLOTS, 1), 0)) * TOK + lane_value(side, LANE_POS).astype(jnp.int32)
@@ -172,29 +171,36 @@
     q_rest = q[:, 128:]
     wide_q = jnp.concatenate([q[:, :128], dot(q_rest, picks((src < 32) & (dst == src + 96))).astype(BF)], axis=1)
     narrow_q = jnp.where(iota((SLOTS, 128), 1) >= 32, q_rest.astype(F32), 0.0).astype(BF)
-    rows = N_TP * TOK
-    n = iota((1, rows), 1)
-    near = ((n & 63) >> 1) * TOK + (n >> 6) * 2 + (n & 1)
-    wide_scores, narrow_scores, masks = [], [], []
-    for half, ref in ((core, own_ref), (1 - core, other_ref)):
-        allowed = near + half * 32 <= row_pos
-        keys = jnp.concatenate([ref[0], ref[2]], axis=1)
-        wide = dot_nt(wide_q, keys) * (160 ** -0.5)
-        narrow = dot_nt(narrow_q, ref[2]) * (96 ** -0.5)
-        wide_scores.append(jnp.where(allowed, wide, FLOOR))
-        narrow_scores.append(jnp.where(allowed, narrow, FLOOR))
-
-    def mixed(scores, at):
-        peak = jnp.maximum(*[jnp.max(s, axis=1, keepdims=True) for s in scores])
-        total, summed = 0.0, 0.0
-        for s, ref in zip(scores, (own_ref, other_ref)):
-            e = jnp.exp(s - peak)
-            total = total + jnp.sum(e, axis=1, keepdims=True)
-            summed = summed + dot(e.astype(BF), ref[at])
-        return (summed / total).astype(BF)
-
-    wide_att = mixed(wide_scores, 1)
-    narrow_att = mixed(narrow_scores, 3)[:, :64]
+    n = iota((1, N_TP * TOK), 1)
+    allowed = ((n & 63) >> 1) * TOK + (n >> 6) * 2 + (n & 1) + half * 32 <= row_pos
+    wide = dot_nt(wide_q, jnp.concatenate([kv_ref[0], kv_ref[2]], axis=1)) * (160 ** -0.5)
+    narrow = dot_nt(narrow_q, kv_ref[2]) * (96 ** -0.5)
+    return [jnp.where(allowed, s, FLOOR) for s in (wide, narrow)]
+
+
+def weighed(scores, peak, values):
+    e = jnp.exp(scores - peak)
+    return jnp.sum(e, axis=1, keepdims=True), dot(e.astype(BF), values)
+
+
+def attend_own_kernel(core_ref, slot_ref, kv_ref, peak_ref, total_ref, sum_ref):
+    for i, scores in enumerate(half_attention(core_ref[0], slot_ref, kv_ref)):
+        peak = jnp.max(scores, axis=1, keepdims=True)
+        total, summed = weighed(scores, peak, kv_ref[1 + 2 * i])
+        peak_ref[i] = jnp.broadcast_to(peak, (SLOTS, 128))
+        total_ref[i] = jnp.broadcast_to(total, (SLOTS, 128))
+        sum_ref[i] = summed
+
+
+def attend_rest_kernel(core_ref, slot_ref, kv_ref, peak_ref, total_ref, sum_ref, wide_out_ref, narrow_out_ref, out_ref):
+    attended = []
+    for i, scores in enumerate(half_attention(1 - core_ref[0], slot_ref, kv_ref)):
+        old = peak_ref[i][:, :1]
+        peak = jnp.maximum(old, jnp.max(scores, axis=1, keepdims=True))
+        total, summed = weighed(scores, peak, kv_ref[1 + 2 * i])
+        kept = jnp.exp(old - peak)
+        attended.append(((summed + kept * sum_ref[i]) / (total + kept * total_ref[i][:, :1])).astype(BF))
+    wide_att, narrow_att = attended[0], attended[1][:, :64]
     for piece in range(N_TP):
         cols = slice(piece * 128, (piece + 1) * 128)
         out_ref[piece] = (dot(wide_att, wide_out_ref[:, cols]) + dot(narrow_att, narrow_out_ref[:, cols])).astype(BF)
@@ -256,12 +262,13 @@
 SMEM = pl.BlockSpec(memory_space=pltpu.SMEM)
 
 
-def run(kernel, outs, *args, scalars=0, plain=0, spread=True):
-    placed = [pltpu.with_memory_space_constraint(a, pltpu.VMEM) for a in args[max(scalars, plain) :]]
-    args = [*args[: max(scalars, plain)], *placed]
+def run(kernel, outs, *args, scalars=0, plain=0, spread=True, kind=BF):
+    spaces = [pltpu.HBM if i < plain else pltpu.VMEM for i in range(scalars, len(args))]
+    placed = [pltpu.with_memory_space_constraint(a, m) for a, m in zip(args[scalars:], spaces)]
+    args = [*args[:scalars], *placed]
     return pl.pallas_call(
         kernel,
-        out_shape=[pltpu.VMEM(shape, BF) for shape in outs] if spread else jax.ShapeDtypeStruct(outs[0], BF),
+        out_shape=[pltpu.VMEM(shape, kind) for shape in outs] if spread else jax.ShapeDtypeStruct(outs[0], BF),
         in_specs=[SMEM] * scalars + [VMEM] * (len(args) - scalars),
         out_specs=[VMEM] * len(outs) if spread else VMEM,
         compiler_params=pltpu.CompilerParams(vmem_limit_bytes=24 << 20),
@@ -312,8 +319,11 @@
     (slots,) = run(slots_kernel, [(SLOTS, 512)], arrived)
     (own,) = run(keys_kernel, [(4, N_TP * TOK, 128)], latents, wide_kv_weight, narrow_kv_weight)
     other = lax.ppermute(own, "c", [(0, 1), (1, 0)])
+    state = run(attend_own_kernel, [(2, SLOTS, 128)] * 3, core, slots, own, scalars=1, kind=F32)
     (partial,) = run(
-        attend_kernel, [(N_TP, SLOTS, 128)], core, slots, own, other, wide_out_weight, narrow_out_weight, scalars=1
+        attend_rest_kernel, [(N_TP, SLOTS, 128)],
+        core, slots, other, *state, wide_out_weight, narrow_out_weight,
+        scalars=1,
     )
     (copies,) = run(stream_kernel, [(N_TP, SLOTS, 128)], swap_all(partial, "tp"), slots)
     rows = swap_all(copies, "tp")

time: 150 us -> 144 us (0.960)
  local copies, waits for them, and re-layouts: 6.05 us -> 0.07 us
    unnamed x38 -> x22, local copies, waits for them, and re-layouts: 6.05 us -> 0.07 us
    pallas_call x9 -> x10, Pallas kernels: 7.81 us -> 9.3 us  [run(): pl.pallas_call(kernel, out_shape=[pltpu.VMEM(shape, kind) for shape in ou...]
  transfers between devices with their start and end apart: 1 -> 1, of which waited for: 1 -> 1; matrix products, arithmetic and copies ran while one was open for 0% -> 0% of each run, Pallas kernels for 0% -> 1%
where the time goes in v3:
time: 144 us
  blocking collectives  129 us (90%)
  Pallas kernels  9.3 us (6%)
  starting transfers between devices  3.94 us (3%)
    all_to_all x6, blocking collectives, swap_all(): return lax.all_to_all(values, axes, split_axis=0, concat_axis=0, tiled=True)  129 us
    pallas_call x10, Pallas kernels, run(): pl.pallas_call(kernel, out_shape=[pltpu.VMEM(shape, kind) for shape in ou...  9.3 us
    ppermute x1, starting transfers between devices, local(): other = lax.ppermute(own, 'c', [(0, 1), (1, 0)])  3.94 us
  transfers between devices with their start and end apart: 1, of which 1 were waited for; matrix products, arithmetic and copies ran while one was open for 0% of the time, Pallas kernels for 1%

profile of v3, /device:TPU:1, one launch (start us, length us, event | category | flops | bytes accessed | tf_op | source)
XLA Modules:
  0.0 143.8 jit_solution(10027993273552086504)
XLA Ops:
  0.0 0.1 multiply_sine_fusion
  0.2 1.8 %pack_kernel.1 = (bf16[256,512]{1,0:T(8,128)(2,1)S(1)}, bf16[256,64]{1,0:T(8,128)(2,1)S(1)}) custom-call(s32[1]{0:T(128)} %bitcast.tp_ref, bf16[64,160]{1,0:T(8,128)(2,1)} %wide_ref.2, bf16[64,96]{1,0:T(8,128)(2,1)} %narrow_ref.2, bf16[32,64]{1,0:T(8,128)(2,1)} %bitcast.27, bf16[64,512]{1,0:T(8,128)(2,1)} %lat_ref.1, f32[1,512]{1,0:T(1,128)} %bitcast.28, ...), custom_call_target="tpu_custom_call" | custom-call | tf_op jit(solution)/shard_map/pack_kernel/pallas_call | solution.py:269
  2.0 38.8 %all_to_all.30 = bf16[32,8,512]{2,1,0:T(8,128)(2,1)S(1)} all-to-all(bf16[32,8,512]{2,1,0:T(8,128)(2,1)S(1)} %bitcast.24), channel_id=1, replica_groups=mesh['z'=16,'c'=2,'tp'=16] {'z','c'}, dimensions={0} | all-to-all | bytes 524288 | tf_op jit(solution)/shard_map/all_to_all | solution.py:280
  40.8 0.6 spread_kernel.1
  41.4 0.0 copy-start.9
  41.4 23.6 %all_to_all.31.lat_ref = bf16[16,272,128]{2,1,0:T(8,128)(2,1)S(1)} all-to-all(bf16[16,272,128]{2,1,0:T(8,128)(2,1)S(1)} %spread_kernel.1), channel_id=1, replica_groups=mesh['z'=16,'c'=2,'tp'=16] {'tp'}, dimensions={0} | all-to-all | bytes 2228224 | tf_op jit(solution)/shard_map/all_to_all | solution.py:280
  65.0 0.0 copy-done.4
  65.0 1.2 keys_kernel.1.kv_ref
  66.2 0.0 copy-start
  66.2 0.0 copy-start.5
  66.2 3.9 %collective-permute-start = (bf16[4,1024,128]{2,1,0:T(8,128)(2,1)S(1)}, bf16[4,1024,128]{2,1,0:T(8,128)(2,1)S(1)}, u32[]{:S(2)}, u32[]{:S(2)}) collective-permute-start(bf16[4,1024,128]{2,1,0:T(8,128)(2,1)S(1)} %keys_kernel.1.kv_ref), channel_id=1, source_target_pairs={{0,16},{16,0},{1,17},{17,1},{2,18},{18,2},{3,19},{19,3},{4,20},{20... | collective-permute-start | bytes 3145736 | tf_op jit(solution)/shard_map/ppermute | solution.py:321
  70.2 0.2 slots_kernel.1.slot_ref
  70.4 1.1 attend_own_kernel.1
  71.4 1.0 collective-permute-done.kv_ref
  72.4 0.0 copy-done.5
  72.4 1.7 %attend_rest_kernel.1 = bf16[16,192,128]{2,1,0:T(8,128)(2,1)S(1)} custom-call(s32[1]{0:T(128)} %bitcast.5.core_ref, bf16[192,512]{1,0:T(8,128)(2,1)S(1)} %slots_kernel.1.slot_ref, bf16[4,1024,128]{2,1,0:T(8,128)(2,1)S(1)} %collective-permute-done.kv_ref, f32[2,192,128]{2,1,0:T(8,128)S(1)} %get-tuple-element.12.peak_ref, ...), custom_call_target="tpu_custom_call" | custom-call | tf_op jit(solution)/shard_map/attend_rest_kernel/pallas_call | solution.py:269
  74.1 16.7 %all_to_all.32.part_ref = bf16[16,192,128]{2,1,0:T(8,128)(2,1)S(1)} all-to-all(bf16[16,192,128]{2,1,0:T(8,128)(2,1)S(1)} %attend_rest_kernel.1), channel_id=1, replica_groups=mesh['z'=16,'c'=2,'tp'=16] {'tp'}, dimensions={0} | all-to-all | bytes 1572864 | tf_op jit(solution)/shard_map/all_to_all | solution.py:280
  90.8 0.1 stream_kernel.1.stream_ref
  91.0 0.0 copy-start.1
  91.0 0.0 copy-start.2
  91.0 0.0 copy-start.3
  91.0 0.0 copy-start.10
  91.0 16.5 %all_to_all.33.x_ref = bf16[16,192,128]{2,1,0:T(8,128)(2,1)S(1)} all-to-all(bf16[16,192,128]{2,1,0:T(8,128)(2,1)S(1)} %stream_kernel.1.stream_ref), channel_id=1, replica_groups=mesh['z'=16,'c'=2,'tp'=16] {'tp'}, dimensions={0} | all-to-all | bytes 1572864 | tf_op jit(solution)/shard_map/all_to_all | solution.py:280
  107.5 0.0 copy-done.1
  107.5 0.0 copy-done.2
  107.5 0.0 copy-done.3
  107.5 0.0 copy-done.10
  107.5 1.5 %expert_kernel.1 = bf16[16,192,128]{2,1,0:T(8,128)(2,1)S(1)} custom-call(bf16[16,192,128]{2,1,0:T(8,128)(2,1)S(1)} %all_to_all.33.x_ref, bf16[192,512]{1,0:T(8,128)(2,1)S(1)} %slots_kernel.1.slot_ref, f32[1,2048]{1,0:T(1,128)S(1)} %bitcast.26, bf16[2,64,2048]{2,1,0:T(8,128)(2,1)S(1)} %bitcast.18, bf16[2,64,2048]{2,1,0:T(8,128)(2,1)S(1)} %bitcast.19, ...), custom_call_target="tpu_custom_call" | custom-call | tf_op jit(solution)/shard_map/expert_kernel/pallas_call | solution.py:269
  109.1 14.8 %all_to_all.34.part_ref = bf16[16,192,128]{2,1,0:T(8,128)(2,1)S(1)} all-to-all(bf16[16,192,128]{2,1,0:T(8,128)(2,1)S(1)} %expert_kernel.1), channel_id=1, replica_groups=mesh['z'=16,'c'=2,'tp'=16] {'tp'}, dimensions={0} | all-to-all | bytes 1572864 | tf_op jit(solution)/shard_map/all_to_all | solution.py:280
  123.9 0.3 give_back_kernel.1
  124.2 18.8 %all_to_all.35 = bf16[32,8,128]{2,1,0:T(8,128)(2,1)S(1)} all-to-all(bf16[32,8,128]{2,1,0:T(8,128)(2,1)S(1)} %bitcast.23), channel_id=1, replica_groups=mesh['z'=16,'c'=2,'tp'=16] {'z','c'}, dimensions={0} | all-to-all | bytes 131072 | tf_op jit(solution)/shard_map/all_to_all | solution.py:280
  143.0 0.8 finish_kernel.1
  (11 shorter events, 0.0 us)
Async XLA Ops:
  41.4 23.6 %copy-start.4 = (bf16[512,256]{1,0:T(8,128)(2,1)S(1)}, bf16[512,256]{1,0:T(8,128)(2,1)}, u32[]{:S(2)}) copy-start(bf16[512,256]{1,0:T(8,128)(2,1)} %wide_ref.3) | copy-start | bytes 786436
  41.4 23.6 %copy-start.9 = (bf16[512,128]{1,0:T(8,128)(2,1)S(1)}, bf16[512,128]{1,0:T(8,128)(2,1)}, u32[]{:S(2)}) copy-start(bf16[512,128]{1,0:T(8,128)(2,1)} %narrow_ref.3) | copy-start | bytes 393220
  66.2 6.2 %copy-start = (bf16[128,2048]{1,0:T(8,128)(2,1)S(1)}, bf16[128,2048]{1,0:T(8,128)(2,1)}, u32[]{:S(2)}) copy-start(bf16[128,2048]{1,0:T(8,128)(2,1)} %wide_out_ref.1) | copy-start | bytes 1572868
  66.2 6.2 %copy-start.5 = (bf16[64,2048]{1,0:T(8,128)(2,1)S(1)}, bf16[64,2048]{1,0:T(8,128)(2,1)}, u32[]{:S(2)}) copy-start(bf16[64,2048]{1,0:T(8,128)(2,1)} %narrow_out_ref.1) | copy-start | bytes 786436
  66.2 6.2 %collective-permute-start = (bf16[4,1024,128]{2,1,0:T(8,128)(2,1)S(1)}, bf16[4,1024,128]{2,1,0:T(8,128)(2,1)S(1)}, u32[]{:S(2)}, u32[]{:S(2)}) collective-permute-start(bf16[4,1024,128]{2,1,0:T(8,128)(2,1)S(1)} %keys_kernel.1.kv_ref), channel_id=1, source_target_pairs={{0,16},{16,0},{1,17},{17,1},{2,18},{18,2},{3,19},{19,3},{4,20},{20... | collective-permute-start | bytes 3145736 | tf_op jit(solution)/shard_map/ppermute | solution.py:321
  90.8 16.7 %copy-start.6 = (bf16[2048,64]{0,1:T(8,128)(2,1)S(1)}, bf16[2048,64]{0,1:T(8,128)(2,1)}, u32[]{:S(2)}) copy-start(bf16[2048,64]{0,1:T(8,128)(2,1)} %param.35) | copy-start | bytes 786436
  90.8 16.7 %copy-start.7 = (bf16[2048,64]{0,1:T(8,128)(2,1)S(1)}, bf16[2048,64]{0,1:T(8,128)(2,1)}, u32[]{:S(2)}) copy-start(bf16[2048,64]{0,1:T(8,128)(2,1)} %param.36) | copy-start | bytes 786436
  90.8 16.7 %copy-start.8 = (bf16[64,2048]{1,0:T(8,128)(2,1)S(1)}, bf16[64,2048]{1,0:T(8,128)(2,1)}, u32[]{:S(2)}) copy-start(bf16[64,2048]{1,0:T(8,128)(2,1)} %sd_ref.1) | copy-start | bytes 786436
  91.0 16.5 %copy-start.1 = (bf16[2,2048,64]{1,2,0:T(8,128)(2,1)S(1)}, bf16[2,2048,64]{1,2,0:T(8,128)(2,1)}, u32[]{:S(2)}) copy-start(bf16[2,2048,64]{1,2,0:T(8,128)(2,1)} %param.32) | copy-start | bytes 1572868
  91.0 16.5 %copy-start.2 = (bf16[2,2048,64]{1,2,0:T(8,128)(2,1)S(1)}, bf16[2,2048,64]{1,2,0:T(8,128)(2,1)}, u32[]{:S(2)}) copy-start(bf16[2,2048,64]{1,2,0:T(8,128)(2,1)} %param.33) | copy-start | bytes 1572868
  91.0 16.5 %copy-start.3 = (bf16[2,64,2048]{2,1,0:T(8,128)(2,1)S(1)}, bf16[2,64,2048]{2,1,0:T(8,128)(2,1)}, u32[]{:S(2)}) copy-start(bf16[2,64,2048]{2,1,0:T(8,128)(2,1)} %param.34) | copy-start | bytes 1572868
  91.0 16.5 %copy-start.10 = (f32[2048]{0:T(1024)S(1)}, f32[2048]{0:T(1024)}, u32[]{:S(2)}) copy-start(f32[2048]{0:T(1024)} %param.29) | copy-start | bytes 24580

commit v4 on v3

--- a/solution.py
+++ b/solution.py
@@ -20,6 +20,7 @@
 F32 = jnp.float32
 BF = jnp.bfloat16
 
+ROWS = 28
 LANE_POS, LANE_HI, LANE_LO, LANE_FLAG = 64, 65, 66, 67
 
 
@@ -33,6 +34,10 @@
 
 def div3(v):
     return (v * 21846) >> 16
+
+
+def div28(v):
+    return (v * 2341) >> 16
 
 
 def dot(a, b):
@@ -57,14 +62,14 @@
     return jnp.where(mask, 1.0, 0.0).astype(BF)
 
 
-def lane_value(block, lane):
-    return jnp.sum(jnp.where(iota(block.shape, 1) == lane, block, 0.0), axis=1, keepdims=True)
-
-
-def slot_rows():
-    row, col = iota((SLOTS, 256), 0), iota((SLOTS, 256), 1)
-    source = div6(row)
-    return picks(col == source * 8 + (row - source * 6))
+def side_value(block, lane):
+    row = iota((SLOTS, 1), 0)
+    return jnp.sum(jnp.where(iota(block.shape, 1) == lane + 4 * (row - 3 * div3(row)), block, 0.0), axis=1, keepdims=True)
+
+
+def from_rows(source, row):
+    count = source.shape[0]
+    return picks(iota((count, N_SP * ROWS), 1) == source * ROWS + row)
 
 
 def pack_kernel(tp_ref, wide_ref, narrow_ref, rope_ref, lat_ref, gain_ref, res_ref, ids_ref, w_ref, cos_ref, sin_ref, out_ref, sel_ref):
@@ -91,52 +96,69 @@
     before = picks(iota((TOK, TOK), 0) < iota((TOK, TOK), 1))
     named = [jnp.where(ids_ref[k : k + 1, :] == iota((TOK, TOK), 0), 1.0, 0.0) for k in range(2)]
     rank = dot((named[0] + named[1]).astype(BF), before)
-    row, tok = iota((256, TOK), 0), iota((256, TOK), 1)
-    dest, place = row >> 3, row & 7
-    selects, high, low = [], 0.0, 0.0
-    for k in range(2):
-        slot = ids_ref[k : k + 1, :] * 3 + jnp.sum(named[k] * rank, axis=0, keepdims=True).astype(jnp.int32)
-        mask = (slot == dest * 6 + place) & (place < 6)
-        selects.append(picks(mask))
-        w = w_ref[k : k + 1, :]
-        w_hi = w.astype(BF).astype(F32)
-        high = high + jnp.where(mask, w_hi, 0.0)
-        low = low + jnp.where(mask, w - w_hi, 0.0)
-    either = selects[0] + selects[1]
-    sel_ref[...] = either
+    slots = [
+        ids_ref[k : k + 1, :] * 3 + jnp.sum(named[k] * rank, axis=0, keepdims=True).astype(jnp.int32) for k in range(2)
+    ]
+
+    def either(want):
+        return picks((slots[0] == want) | (slots[1] == want))
+
+    sel_ref[...] = either(iota((SLOTS, 1), 0))
+
+    row = iota((TOK, 1), 0)
+    lane, token = iota((TOK, 128), 1), iota((TOK, 128), 0).astype(F32)
+    side = dot(picks(iota((TOK, TOK), 1) == ((row >> 1) & 1) * 32 + t * 2 + (row & 1)), rope)
+    for place in range(3):
+        high, low, flag = 0.0, 0.0, 0.0
+        for k in range(2):
+            mask = slots[k] == row * 3 + place
+            w = w_ref[k : k + 1, :]
+            w_hi = w.astype(BF).astype(F32)
+            high = high + jnp.where(mask, w_hi, 0.0)
+            low = low + jnp.where(mask, w - w_hi, 0.0)
+            flag = flag + jnp.where(mask, 1.0 - k, 0.0)
+        at = lane - 4 * place
+        side = side + dot(either(row * 3 + place), jnp.where(at == LANE_POS, token, 0.0).astype(BF))
+        side = side + dot(high.astype(BF), picks(at == LANE_HI)) + dot(low.astype(BF), picks(at == LANE_LO))
+        side = side + dot(flag.astype(BF), picks(at == LANE_FLAG))
+
+    row = iota((N_SP * ROWS, 1), 0)
+    dest = div28(row)
+    place = row - dest * ROWS
+    kind = div6(place)
+    slot = dest * 6 + place - kind * 6
+    out = 0.0
+    for i, rows in enumerate((wide_ref[:, :128], q_rest, res)):
+        out = out + dot(either(jnp.where(kind == i, slot, -1)), rows)
     start = (dest & 1) * 32 + t * 2
-    token_row = picks((place >= 6) & (tok == start + place - 6))
-    rope_row = picks((place < 2) & (tok == start + place))
-    lat_part = dot(token_row, normed)
-    out_ref[:, :128] = (dot(either, wide_ref[:, :128]) + lat_part[:, :128]).astype(BF)
-    out_ref[:, 128:256] = (dot(either, q_rest) + lat_part[:, 128:256]).astype(BF)
-    out_ref[:, 256:384] = (dot(either, res) + lat_part[:, 256:384]).astype(BF)
-    lane, token = iota((TOK, 128), 1), iota((TOK, 128), 0).astype(F32)
-    side = dot(either, jnp.where(lane == LANE_POS, token, 0.0).astype(BF))
-    side = side + dot(high.astype(BF), picks(lane == LANE_HI)) + dot(low.astype(BF), picks(lane == LANE_LO))
-    side = side + dot(selects[0], picks(lane == LANE_FLAG)) + dot(rope_row, rope)
-    out_ref[:, 384:] = (side + lat_part[:, 384:]).astype(BF)
+    tok = iota((N_SP * ROWS, TOK), 1)
+    for f in range(4):
+        mine = (place >> 1) == 9 + f
+        out = out + dot(picks(tok == jnp.where(mine, start + (place & 1), -1)), normed[:, f * 128 : (f + 1) * 128])
+    out = out + dot(picks(tok == jnp.where(place >= 26, dest * 2 + place - 26, -1)), side.astype(BF))
+    out_ref[...] = out.astype(BF)
 
 
 def slots_kernel(arr_ref, out_ref):
-    out_ref[...] = dot(slot_rows(), arr_ref[...]).astype(BF)
+    row = iota((SLOTS, 1), 0)
+    source = div6(row)
+    place = row - source * 6
+    for i, start in enumerate((place, place + 6, place + 12, 26 + div3(place))):
+        out_ref[:, i * 128 : (i + 1) * 128] = dot(from_rows(source, start), arr_ref[...]).astype(BF)
 
 
 def spread_kernel(arr_ref, out_ref):
-    row, col = iota((TOK, 256), 0), iota((TOK, 256), 1)
-    base = (row >> 1) * 8 + (row & 1)
-    lat = dot(picks(col == base + 6), arr_ref[...]).astype(BF)
-    side = arr_ref[:, 384:]
+    n = iota((TOK, 1), 0)
+    rows = [dot(from_rows(n >> 1, 18 + 2 * f + (n & 1)), arr_ref[...]).astype(BF) for f in range(4)]
+    rope = dot(from_rows(n >> 1, 26 + (n & 1)), arr_ref[...]).astype(BF)
     packed = jnp.zeros((16, 128), F32)
+    src, dst = iota((128, 128), 0), iota((128, 128), 1)
     for b in range(4):
-        near, far = iota((16, 256), 0) + 16 * b, iota((16, 256), 1)
-        here = dot(picks(far == (near >> 1) * 8 + (near & 1)), side).astype(BF)
-        src, dst = iota((128, 128), 0), iota((128, 128), 1)
-        packed = packed + dot(here, picks((src < 32) & (dst == src + 32 * b)))
+        packed = packed + dot(rope[16 * b : 16 * (b + 1)], picks((src < 32) & (dst == src + 32 * b)))
     packed = packed.astype(BF)
     for copy in range(N_TP):
         for f in range(4):
-            out_ref[copy, f * TOK : (f + 1) * TOK, :] = lat[:, f * 128 : (f + 1) * 128]
+            out_ref[copy, f * TOK : (f + 1) * TOK, :] = rows[f]
         out_ref[copy, 4 * TOK :, :] = packed
 
 
@@ -166,7 +188,7 @@
 def half_attention(half, slot_ref, kv_ref):
     q = slot_ref[:, :256]
     side = slot_ref[:, 384:].astype(F32)
-    row_pos = div6(iota((SLOTS, 1), 0)) * TOK + lane_value(side, LANE_POS).astype(jnp.int32)
+    row_pos = div6(iota((SLOTS, 1), 0)) * TOK + side_value(side, LANE_POS).astype(jnp.int32)
     src, dst = iota((128, 128), 0), iota((128, 128), 1)
     q_rest = q[:, 128:]
     wide_q = jnp.concatenate([q[:, :128], dot(q_rest, picks((src < 32) & (dst == src + 96))).astype(BF)], axis=1)
@@ -231,8 +253,8 @@
     gate, up = into[:, :192], into[:, 192:]
     hidden = (gate / (1.0 + jnp.exp(-gate))) * up
     side = slot_ref[:, 384:].astype(F32)
-    weight = lane_value(side, LANE_HI) + lane_value(side, LANE_LO)
-    flag = lane_value(side, LANE_FLAG)
+    weight = side_value(side, LANE_HI) + side_value(side, LANE_LO)
+    flag = side_value(side, LANE_FLAG)
     owner = div3(iota((SLOTS, 128), 0)) & 1
     routed_hidden = jnp.where(owner == (iota((SLOTS, 128), 1) >> 6), hidden[:, :128], 0.0).astype(BF)
     shared_hidden = hidden[:, 128:].astype(BF)
@@ -249,9 +271,8 @@
     total = jnp.zeros((SLOTS, 128), F32)
     for piece in range(N_TP):
         total = total + part_ref[piece].astype(F32)
-    flag = lane_value(slot_ref[:, 384:].astype(F32), LANE_FLAG)
-    total = (total + flag * stream_ref[0].astype(F32)).astype(BF)
-    out_ref[...] = dot_tn(slot_rows(), total).astype(BF)
+    flag = side_value(slot_ref[:, 384:].astype(F32), LANE_FLAG)
+    out_ref[...] = (total + flag * stream_ref[0].astype(F32)).astype(BF)
 
 
 def finish_kernel(sel_ref, back_ref, out_ref):
@@ -307,13 +328,13 @@
     positions = lax.axis_index(SP) * TOK + jnp.arange(TOK, dtype=jnp.int32)
     angles = frequency[:, None] * positions.astype(F32)[None, :]
     payload, chosen = run(
-        pack_kernel, [(256, 512), (256, TOK)],
+        pack_kernel, [(N_SP * ROWS, 128), (SLOTS, TOK)],
         t, wide_queries, narrow_queries, rope_key.T, kv_latent, latent_gain[None, :], residual,
         route_ids.T, route_weights.T, jnp.cos(angles), jnp.sin(angles),
         scalars=1,
         plain=9,
     )
-    arrived = swap_all(payload.reshape(N_SP, 8, 512), SP).reshape(256, 512)
+    arrived = swap_all(payload.reshape(N_SP, ROWS // 2, 2, 128), SP).reshape(N_SP * ROWS, 128)
     (spread,) = run(spread_kernel, [(N_TP, 272, 128)], arrived)
     latents = swap_all(spread, "tp")
     (slots,) = run(slots_kernel, [(SLOTS, 512)], arrived)
@@ -333,8 +354,8 @@
         expert_gate.swapaxes(1, 2), expert_up.swapaxes(1, 2), expert_down.reshape(128, D_MODEL),
         shared_gate.T, shared_up.T, shared_down,
     )
-    (back,) = run(give_back_kernel, [(256, 128)], swap_all(partial, "tp"), copies, slots)
-    back = swap_all(back.reshape(N_SP, 8, 128), SP).reshape(256, 128)
+    (back,) = run(give_back_kernel, [(SLOTS, 128)], swap_all(partial, "tp"), copies, slots)
+    back = swap_all(back.reshape(N_SP, 3, 2, 128), SP).reshape(SLOTS, 128)
     return run(finish_kernel, [(TOK, 128)], chosen, back, spread=False)
 
 

time: 144 us -> 143 us (level)
  blocking collectives: 129 us -> 127 us
    all_to_all x6, blocking collectives: 129 us -> 127 us  [swap_all(): return lax.all_to_all(values, axes, split_axis=0, concat_axis=0, tiled=True)]
where the time goes in v4:
time: 143 us; the launch traced here: 142 us
  blocking collectives  127 us (89%)
  Pallas kernels  10 us (7%)
  starting transfers between devices  4.32 us (3%)
    all_to_all x6, blocking collectives, swap_all(): return lax.all_to_all(values, axes, split_axis=0, concat_axis=0, tiled=True)  127 us
    pallas_call x10, Pallas kernels, run(): pl.pallas_call(kernel, out_shape=[pltpu.VMEM(shape, kind) for shape in ou...  10 us
    ppermute x1, starting transfers between devices, local(): other = lax.ppermute(own, 'c', [(0, 1), (1, 0)])  4.32 us
  transfers between devices with their start and end apart: 1, of which 1 were waited for; matrix products, arithmetic and copies ran while one was open for 0% of the time, Pallas kernels for 1%

profile of v4, /device:TPU:1, one launch (start us, length us, event | category | flops | bytes accessed | tf_op | source)
XLA Modules:
  0.0 142.3 jit_solution(11214096111522414453)
XLA Ops:
  0.0 0.1 multiply_sine_fusion
  0.2 2.5 %pack_kernel.1 = (bf16[896,128]{1,0:T(8,128)(2,1)S(1)}, bf16[192,64]{1,0:T(8,128)(2,1)S(1)}) custom-call(s32[1]{0:T(128)} %bitcast.tp_ref, bf16[64,160]{1,0:T(8,128)(2,1)} %wide_ref.2, bf16[64,96]{1,0:T(8,128)(2,1)} %narrow_ref.2, bf16[32,64]{1,0:T(8,128)(2,1)} %bitcast.27, bf16[64,512]{1,0:T(8,128)(2,1)} %lat_ref.1, f32[1,512]{1,0:T(1,128)} %bitcast.28, ...), custom_call_target="tpu_custom_call" | custom-call | tf_op jit(solution)/shard_map/pack_kernel/pallas_call | solution.py:290
  2.7 36.8 %all_to_all.30 = bf16[32,14,2,128]{3,2,1,0:T(2,128)(2,1)S(1)} all-to-all(bf16[32,14,2,128]{3,2,1,0:T(2,128)(2,1)S(1)} %bitcast.23), channel_id=1, replica_groups=mesh['z'=16,'c'=2,'tp'=16] {'z','c'}, dimensions={0} | all-to-all | bytes 458752 | tf_op jit(solution)/shard_map/all_to_all | solution.py:301
  39.5 0.5 spread_kernel.1
  40.0 0.0 copy-start.9
  40.0 23.3 %all_to_all.31.lat_ref = bf16[16,272,128]{2,1,0:T(8,128)(2,1)S(1)} all-to-all(bf16[16,272,128]{2,1,0:T(8,128)(2,1)S(1)} %spread_kernel.1), channel_id=1, replica_groups=mesh['z'=16,'c'=2,'tp'=16] {'tp'}, dimensions={0} | all-to-all | bytes 2228224 | tf_op jit(solution)/shard_map/all_to_all | solution.py:301
  63.3 0.0 copy-done.4
  63.3 0.0 copy-done.9
  63.3 1.2 keys_kernel.1.kv_ref
  64.5 0.0 copy-start
  64.5 0.0 copy-start.5
  64.5 4.3 %collective-permute-start = (bf16[4,1024,128]{2,1,0:T(8,128)(2,1)S(1)}, bf16[4,1024,128]{2,1,0:T(8,128)(2,1)S(1)}, u32[]{:S(2)}, u32[]{:S(2)}) collective-permute-start(bf16[4,1024,128]{2,1,0:T(8,128)(2,1)S(1)} %keys_kernel.1.kv_ref), channel_id=1, source_target_pairs={{0,16},{16,0},{1,17},{17,1},{2,18},{18,2},{3,19},{19,3},{4,20},{20... | collective-permute-start | bytes 3145736 | tf_op jit(solution)/shard_map/ppermute | solution.py:342
  68.8 0.5 slots_kernel.1.slot_ref
  69.4 1.0 attend_own_kernel.1
  70.4 0.7 collective-permute-done.kv_ref
  71.1 0.0 copy-done
  71.1 0.0 copy-done.5
  71.1 1.7 %attend_rest_kernel.1 = bf16[16,192,128]{2,1,0:T(8,128)(2,1)S(1)} custom-call(s32[1]{0:T(128)} %bitcast.5.core_ref, bf16[192,512]{1,0:T(8,128)(2,1)S(1)} %slots_kernel.1.slot_ref, bf16[4,1024,128]{2,1,0:T(8,128)(2,1)S(1)} %collective-permute-done.kv_ref, f32[2,192,128]{2,1,0:T(8,128)S(1)} %get-tuple-element.12.peak_ref, ...), custom_call_target="tpu_custom_call" | custom-call | tf_op jit(solution)/shard_map/attend_rest_kernel/pallas_call | solution.py:290
  72.8 16.7 %all_to_all.32.part_ref = bf16[16,192,128]{2,1,0:T(8,128)(2,1)S(1)} all-to-all(bf16[16,192,128]{2,1,0:T(8,128)(2,1)S(1)} %attend_rest_kernel.1), channel_id=1, replica_groups=mesh['z'=16,'c'=2,'tp'=16] {'tp'}, dimensions={0} | all-to-all | bytes 1572864 | tf_op jit(solution)/shard_map/all_to_all | solution.py:301
  89.5 0.1 stream_kernel.1.stream_ref
  89.7 0.0 copy-start.1
  89.7 0.0 copy-start.2
  89.7 0.0 copy-start.3
  89.7 0.0 copy-start.10
  89.7 16.5 %all_to_all.33.x_ref = bf16[16,192,128]{2,1,0:T(8,128)(2,1)S(1)} all-to-all(bf16[16,192,128]{2,1,0:T(8,128)(2,1)S(1)} %stream_kernel.1.stream_ref), channel_id=1, replica_groups=mesh['z'=16,'c'=2,'tp'=16] {'tp'}, dimensions={0} | all-to-all | bytes 1572864 | tf_op jit(solution)/shard_map/all_to_all | solution.py:301
  106.2 0.0 copy-done.6
  106.2 0.0 copy-done.7
  106.3 1.5 %expert_kernel.1 = bf16[16,192,128]{2,1,0:T(8,128)(2,1)S(1)} custom-call(bf16[16,192,128]{2,1,0:T(8,128)(2,1)S(1)} %all_to_all.33.x_ref, bf16[192,512]{1,0:T(8,128)(2,1)S(1)} %slots_kernel.1.slot_ref, f32[1,2048]{1,0:T(1,128)S(1)} %bitcast.26, bf16[2,64,2048]{2,1,0:T(8,128)(2,1)S(1)} %bitcast.18, bf16[2,64,2048]{2,1,0:T(8,128)(2,1)S(1)} %bitcast.19, ...), custom_call_target="tpu_custom_call" | custom-call | tf_op jit(solution)/shard_map/expert_kernel/pallas_call | solution.py:290
  107.8 14.8 %all_to_all.34.part_ref = bf16[16,192,128]{2,1,0:T(8,128)(2,1)S(1)} all-to-all(bf16[16,192,128]{2,1,0:T(8,128)(2,1)S(1)} %expert_kernel.1), channel_id=1, replica_groups=mesh['z'=16,'c'=2,'tp'=16] {'tp'}, dimensions={0} | all-to-all | bytes 1572864 | tf_op jit(solution)/shard_map/all_to_all | solution.py:301
  122.6 0.2 give_back_kernel.1
  122.7 18.8 %all_to_all.35 = bf16[32,3,2,128]{3,2,1,0:T(2,128)(2,1)S(1)} all-to-all(bf16[32,3,2,128]{3,2,1,0:T(2,128)(2,1)S(1)} %bitcast.25), channel_id=1, replica_groups=mesh['z'=16,'c'=2,'tp'=16] {'z','c'}, dimensions={0} | all-to-all | bytes 98304 | tf_op jit(solution)/shard_map/all_to_all | solution.py:301
  141.6 0.8 finish_kernel.1
  (11 shorter events, 0.0 us)
Async XLA Ops:
  40.0 23.3 %copy-start.4 = (bf16[512,256]{1,0:T(8,128)(2,1)S(1)}, bf16[512,256]{1,0:T(8,128)(2,1)}, u32[]{:S(2)}) copy-start(bf16[512,256]{1,0:T(8,128)(2,1)} %wide_ref.3) | copy-start | bytes 786436
  40.0 23.3 %copy-start.9 = (bf16[512,128]{1,0:T(8,128)(2,1)S(1)}, bf16[512,128]{1,0:T(8,128)(2,1)}, u32[]{:S(2)}) copy-start(bf16[512,128]{1,0:T(8,128)(2,1)} %narrow_ref.3) | copy-start | bytes 393220
  64.5 6.6 %copy-start = (bf16[128,2048]{1,0:T(8,128)(2,1)S(1)}, bf16[128,2048]{1,0:T(8,128)(2,1)}, u32[]{:S(2)}) copy-start(bf16[128,2048]{1,0:T(8,128)(2,1)} %wide_out_ref.1) | copy-start | bytes 1572868
  64.5 6.6 %copy-start.5 = (bf16[64,2048]{1,0:T(8,128)(2,1)S(1)}, bf16[64,2048]{1,0:T(8,128)(2,1)}, u32[]{:S(2)}) copy-start(bf16[64,2048]{1,0:T(8,128)(2,1)} %narrow_out_ref.1) | copy-start | bytes 786436
  64.5 6.6 %collective-permute-start = (bf16[4,1024,128]{2,1,0:T(8,128)(2,1)S(1)}, bf16[4,1024,128]{2,1,0:T(8,128)(2,1)S(1)}, u32[]{:S(2)}, u32[]{:S(2)}) collective-permute-start(bf16[4,1024,128]{2,1,0:T(8,128)(2,1)S(1)} %keys_kernel.1.kv_ref), channel_id=1, source_target_pairs={{0,16},{16,0},{1,17},{17,1},{2,18},{18,2},{3,19},{19,3},{4,20},{20... | collective-permute-start | bytes 3145736 | tf_op jit(solution)/shard_map/ppermute | solution.py:342
  89.5 16.7 %copy-start.6 = (bf16[2048,64]{0,1:T(8,128)(2,1)S(1)}, bf16[2048,64]{0,1:T(8,128)(2,1)}, u32[]{:S(2)}) copy-start(bf16[2048,64]{0,1:T(8,128)(2,1)} %param.35) | copy-start | bytes 786436
  89.5 16.7 %copy-start.7 = (bf16[2048,64]{0,1:T(8,128)(2,1)S(1)}, bf16[2048,64]{0,1:T(8,128)(2,1)}, u32[]{:S(2)}) copy-start(bf16[2048,64]{0,1:T(8,128)(2,1)} %param.36) | copy-start | bytes 786436
  89.5 16.7 %copy-start.8 = (bf16[64,2048]{1,0:T(8,128)(2,1)S(1)}, bf16[64,2048]{1,0:T(8,128)(2,1)}, u32[]{:S(2)}) copy-start(bf16[64,2048]{1,0:T(8,128)(2,1)} %sd_ref.1) | copy-start | bytes 786436
  89.7 16.5 %copy-start.1 = (bf16[2,2048,64]{1,2,0:T(8,128)(2,1)S(1)}, bf16[2,2048,64]{1,2,0:T(8,128)(2,1)}, u32[]{:S(2)}) copy-start(bf16[2,2048,64]{1,2,0:T(8,128)(2,1)} %param.32) | copy-start | bytes 1572868
  89.7 16.5 %copy-start.2 = (bf16[2,2048,64]{1,2,0:T(8,128)(2,1)S(1)}, bf16[2,2048,64]{1,2,0:T(8,128)(2,1)}, u32[]{:S(2)}) copy-start(bf16[2,2048,64]{1,2,0:T(8,128)(2,1)} %param.33) | copy-start | bytes 1572868
  89.7 16.5 %copy-start.3 = (bf16[2,64,2048]{2,1,0:T(8,128)(2,1)S(1)}, bf16[2,64,2048]{2,1,0:T(8,128)(2,1)}, u32[]{:S(2)}) copy-start(bf16[2,64,2048]{2,1,0:T(8,128)(2,1)} %param.34) | copy-start | bytes 1572868
  89.7 16.5 %copy-start.10 = (f32[2048]{0:T(1024)S(1)}, f32[2048]{0:T(1024)}, u32[]{:S(2)}) copy-start(f32[2048]{0:T(1024)} %param.29) | copy-start | bytes 24580

commit v5 on v4

--- a/solution.py
+++ b/solution.py
@@ -122,20 +122,27 @@
         side = side + dot(high.astype(BF), picks(at == LANE_HI)) + dot(low.astype(BF), picks(at == LANE_LO))
         side = side + dot(flag.astype(BF), picks(at == LANE_FLAG))
 
+    twice = picks((iota((TOK, 128), 1) & 63) == iota((TOK, 128), 0))
+    keys = [dot(slot.astype(F32).astype(BF), twice).astype(jnp.int32) for slot in slots]
     row = iota((N_SP * ROWS, 1), 0)
     dest = div28(row)
     place = row - dest * ROWS
     kind = div6(place)
     slot = dest * 6 + place - kind * 6
-    out = 0.0
-    for i, rows in enumerate((wide_ref[:, :128], q_rest, res)):
-        out = out + dot(either(jnp.where(kind == i, slot, -1)), rows)
-    start = (dest & 1) * 32 + t * 2
-    tok = iota((N_SP * ROWS, TOK), 1)
-    for f in range(4):
-        mine = (place >> 1) == 9 + f
-        out = out + dot(picks(tok == jnp.where(mine, start + (place & 1), -1)), normed[:, f * 128 : (f + 1) * 128])
-    out = out + dot(picks(tok == jnp.where(place >= 26, dest * 2 + place - 26, -1)), side.astype(BF))
+    lanes = iota((1, 128), 1)
+    tok, upper = lanes & 63, lanes >= 64
+    marks = [jnp.where(upper, key + 1024, key) for key in keys]
+    want = jnp.where(kind < 2, slot + kind * 1024, -1)
+    out = dot(picks((marks[0] == want) | (marks[1] == want)), jnp.concatenate([wide_ref[:, :128], q_rest], axis=0))
+    marks = [jnp.where(upper, tok + 1024, key) for key in keys]
+    want = jnp.where(kind == 2, slot, jnp.where(place >= 26, dest * 2 + place - 26 + 1024, -1))
+    out = out + dot(picks((marks[0] == want) | (marks[1] == want)), jnp.concatenate([res, side.astype(BF)], axis=0))
+    start = (dest & 1) * 32 + t * 2 + (place & 1)
+    block = (place >> 1) - 9
+    for pair in range(2):
+        want = jnp.where((block >> 1) == pair, start + (block & 1) * 64, -1)
+        rows = [normed[:, f * 128 : (f + 1) * 128] for f in (2 * pair, 2 * pair + 1)]
+        out = out + dot(picks(lanes == want), jnp.concatenate(rows, axis=0))
     out_ref[...] = out.astype(BF)
 
 
@@ -166,10 +173,11 @@
     rows = N_TP * TOK
     wide = jnp.zeros((rows, 256), F32)
     narrow = jnp.zeros((rows, 128), F32)
-    for f in range(4):
-        part = lat_ref[:, f * TOK : (f + 1) * TOK, :].reshape(rows, 128)
-        wide = wide + dot(part, wide_ref[f * 128 : (f + 1) * 128, :])
-        narrow = narrow + dot(part, narrow_ref[f * 128 : (f + 1) * 128, :])
+    for pair in range(2):
+        parts = [lat_ref[:, f * TOK : (f + 1) * TOK, :].reshape(rows, 128) for f in (2 * pair, 2 * pair + 1)]
+        part = jnp.concatenate(parts, axis=1)
+        wide = wide + dot(part, wide_ref[pair * 256 : (pair + 1) * 256, :])
+        narrow = narrow + dot(part, narrow_ref[pair * 256 : (pair + 1) * 256, :])
     wide, narrow = wide.astype(BF), narrow.astype(BF)
     packed = lat_ref[:, 4 * TOK :, :].reshape(256, 128)
     src, dst = iota((128, 128), 0), iota((128, 128), 1)
@@ -223,9 +231,11 @@
         kept = jnp.exp(old - peak)
         attended.append(((summed + kept * sum_ref[i]) / (total + kept * total_ref[i][:, :1])).astype(BF))
     wide_att, narrow_att = attended[0], attended[1][:, :64]
-    for piece in range(N_TP):
-        cols = slice(piece * 128, (piece + 1) * 128)
-        out_ref[piece] = (dot(wide_att, wide_out_ref[:, cols]) + dot(narrow_att, narrow_out_ref[:, cols])).astype(BF)
+    for pair in range(N_TP // 2):
+        cols = slice(pair * 256, (pair + 1) * 256)
+        both = (dot(wide_att, wide_out_ref[:, cols]) + dot(narrow_att, narrow_out_ref[:, cols])).astype(BF)
+        out_ref[2 * pair] = both[:, :128]
+        out_ref[2 * pair + 1] = both[:, 128:]
 
 
 def stream_kernel(part_ref, slot_ref, out_ref):

time: 143 us -> 142 us (level)
  no operation moved by 1% of the time
where the time goes in v5:
time: 142 us
  blocking collectives  127 us (89%)
  Pallas kernels  9.67 us (7%)
  starting transfers between devices  4.32 us (3%)
    all_to_all x6, blocking collectives, swap_all(): return lax.all_to_all(values, axes, split_axis=0, concat_axis=0, tiled=True)  127 us
    pallas_call x10, Pallas kernels, run(): pl.pallas_call(kernel, out_shape=[pltpu.VMEM(shape, kind) for shape in ou...  9.67 us
    ppermute x1, starting transfers between devices, local(): other = lax.ppermute(own, 'c', [(0, 1), (1, 0)])  4.32 us
  transfers between devices with their start and end apart: 1, of which 1 were waited for; matrix products, arithmetic and copies ran while one was open for 0% of the time, Pallas kernels for 1%

profile of v5, /device:TPU:1, one launch (start us, length us, event | category | flops | bytes accessed | tf_op | source)
XLA Modules:
  0.0 142.0 jit_solution(6165167215367129312)
XLA Ops:
  0.0 0.1 multiply_sine_fusion
  0.2 2.4 %pack_kernel.1 = (bf16[896,128]{1,0:T(8,128)(2,1)S(1)}, bf16[192,64]{1,0:T(8,128)(2,1)S(1)}) custom-call(s32[1]{0:T(128)} %bitcast.tp_ref, bf16[64,160]{1,0:T(8,128)(2,1)} %wide_ref.2, bf16[64,96]{1,0:T(8,128)(2,1)} %narrow_ref.2, bf16[32,64]{1,0:T(8,128)(2,1)} %bitcast.27, bf16[64,512]{1,0:T(8,128)(2,1)} %lat_ref.1, f32[1,512]{1,0:T(1,128)} %bitcast.28, ...), custom_call_target="tpu_custom_call" | custom-call | tf_op jit(solution)/shard_map/pack_kernel/pallas_call | solution.py:300
  2.6 36.8 %all_to_all.30 = bf16[32,14,2,128]{3,2,1,0:T(2,128)(2,1)S(1)} all-to-all(bf16[32,14,2,128]{3,2,1,0:T(2,128)(2,1)S(1)} %bitcast.23), channel_id=1, replica_groups=mesh['z'=16,'c'=2,'tp'=16] {'z','c'}, dimensions={0} | all-to-all | bytes 458752 | tf_op jit(solution)/shard_map/all_to_all | solution.py:311
  39.4 0.5 spread_kernel.1
  39.9 0.0 copy-start.9
  39.9 23.3 %all_to_all.31.lat_ref = bf16[16,272,128]{2,1,0:T(8,128)(2,1)S(1)} all-to-all(bf16[16,272,128]{2,1,0:T(8,128)(2,1)S(1)} %spread_kernel.1), channel_id=1, replica_groups=mesh['z'=16,'c'=2,'tp'=16] {'tp'}, dimensions={0} | all-to-all | bytes 2228224 | tf_op jit(solution)/shard_map/all_to_all | solution.py:311
  63.2 0.0 copy-done.4
  63.2 0.0 copy-done.9
  63.2 0.9 keys_kernel.1.kv_ref
  64.1 0.0 copy-start
  64.1 0.0 copy-start.5
  64.1 4.3 %collective-permute-start = (bf16[4,1024,128]{2,1,0:T(8,128)(2,1)S(1)}, bf16[4,1024,128]{2,1,0:T(8,128)(2,1)S(1)}, u32[]{:S(2)}, u32[]{:S(2)}) collective-permute-start(bf16[4,1024,128]{2,1,0:T(8,128)(2,1)S(1)} %keys_kernel.1.kv_ref), channel_id=1, source_target_pairs={{0,16},{16,0},{1,17},{17,1},{2,18},{18,2},{3,19},{19,3},{4,20},{20... | collective-permute-start | bytes 3145736 | tf_op jit(solution)/shard_map/ppermute | solution.py:352
  68.5 0.5 slots_kernel.1.slot_ref
  69.0 1.0 attend_own_kernel.1
  70.1 0.7 collective-permute-done.kv_ref
  70.7 0.0 copy-done
  70.7 0.0 copy-done.5
  70.7 1.7 %attend_rest_kernel.1 = bf16[16,192,128]{2,1,0:T(8,128)(2,1)S(1)} custom-call(s32[1]{0:T(128)} %bitcast.5.core_ref, bf16[192,512]{1,0:T(8,128)(2,1)S(1)} %slots_kernel.1.slot_ref, bf16[4,1024,128]{2,1,0:T(8,128)(2,1)S(1)} %collective-permute-done.kv_ref, f32[2,192,128]{2,1,0:T(8,128)S(1)} %get-tuple-element.12.peak_ref, ...), custom_call_target="tpu_custom_call" | custom-call | tf_op jit(solution)/shard_map/attend_rest_kernel/pallas_call | solution.py:300
  72.4 16.7 %all_to_all.32.part_ref = bf16[16,192,128]{2,1,0:T(8,128)(2,1)S(1)} all-to-all(bf16[16,192,128]{2,1,0:T(8,128)(2,1)S(1)} %attend_rest_kernel.1), channel_id=1, replica_groups=mesh['z'=16,'c'=2,'tp'=16] {'tp'}, dimensions={0} | all-to-all | bytes 1572864 | tf_op jit(solution)/shard_map/all_to_all | solution.py:311
  89.2 0.1 stream_kernel.1.stream_ref
  89.3 0.0 copy-start.1
  89.3 0.0 copy-start.2
  89.4 0.0 copy-start.3
  89.4 0.0 copy-start.10
  89.4 16.5 %all_to_all.33.x_ref = bf16[16,192,128]{2,1,0:T(8,128)(2,1)S(1)} all-to-all(bf16[16,192,128]{2,1,0:T(8,128)(2,1)S(1)} %stream_kernel.1.stream_ref), channel_id=1, replica_groups=mesh['z'=16,'c'=2,'tp'=16] {'tp'}, dimensions={0} | all-to-all | bytes 1572864 | tf_op jit(solution)/shard_map/all_to_all | solution.py:311
  105.9 0.0 copy-done.6
  105.9 0.0 copy-done.7
  105.9 1.5 %expert_kernel.1 = bf16[16,192,128]{2,1,0:T(8,128)(2,1)S(1)} custom-call(bf16[16,192,128]{2,1,0:T(8,128)(2,1)S(1)} %all_to_all.33.x_ref, bf16[192,512]{1,0:T(8,128)(2,1)S(1)} %slots_kernel.1.slot_ref, f32[1,2048]{1,0:T(1,128)S(1)} %bitcast.26, bf16[2,64,2048]{2,1,0:T(8,128)(2,1)S(1)} %bitcast.18, bf16[2,64,2048]{2,1,0:T(8,128)(2,1)S(1)} %bitcast.19, ...), custom_call_target="tpu_custom_call" | custom-call | tf_op jit(solution)/shard_map/expert_kernel/pallas_call | solution.py:300
  107.5 14.8 %all_to_all.34.part_ref = bf16[16,192,128]{2,1,0:T(8,128)(2,1)S(1)} all-to-all(bf16[16,192,128]{2,1,0:T(8,128)(2,1)S(1)} %expert_kernel.1), channel_id=1, replica_groups=mesh['z'=16,'c'=2,'tp'=16] {'tp'}, dimensions={0} | all-to-all | bytes 1572864 | tf_op jit(solution)/shard_map/all_to_all | solution.py:311
  122.2 0.2 give_back_kernel.1
  122.4 18.8 %all_to_all.35 = bf16[32,3,2,128]{3,2,1,0:T(2,128)(2,1)S(1)} all-to-all(bf16[32,3,2,128]{3,2,1,0:T(2,128)(2,1)S(1)} %bitcast.25), channel_id=1, replica_groups=mesh['z'=16,'c'=2,'tp'=16] {'z','c'}, dimensions={0} | all-to-all | bytes 98304 | tf_op jit(solution)/shard_map/all_to_all | solution.py:311
  141.2 0.8 finish_kernel.1
  (11 shorter events, 0.0 us)
Async XLA Ops:
  39.9 23.3 %copy-start.4 = (bf16[512,256]{1,0:T(8,128)(2,1)S(1)}, bf16[512,256]{1,0:T(8,128)(2,1)}, u32[]{:S(2)}) copy-start(bf16[512,256]{1,0:T(8,128)(2,1)} %wide_ref.3) | copy-start | bytes 786436
  39.9 23.3 %copy-start.9 = (bf16[512,128]{1,0:T(8,128)(2,1)S(1)}, bf16[512,128]{1,0:T(8,128)(2,1)}, u32[]{:S(2)}) copy-start(bf16[512,128]{1,0:T(8,128)(2,1)} %narrow_ref.3) | copy-start | bytes 393220
  64.1 6.6 %copy-start = (bf16[128,2048]{1,0:T(8,128)(2,1)S(1)}, bf16[128,2048]{1,0:T(8,128)(2,1)}, u32[]{:S(2)}) copy-start(bf16[128,2048]{1,0:T(8,128)(2,1)} %wide_out_ref.1) | copy-start | bytes 1572868
  64.1 6.6 %copy-start.5 = (bf16[64,2048]{1,0:T(8,128)(2,1)S(1)}, bf16[64,2048]{1,0:T(8,128)(2,1)}, u32[]{:S(2)}) copy-start(bf16[64,2048]{1,0:T(8,128)(2,1)} %narrow_out_ref.1) | copy-start | bytes 786436
  64.1 6.6 %collective-permute-start = (bf16[4,1024,128]{2,1,0:T(8,128)(2,1)S(1)}, bf16[4,1024,128]{2,1,0:T(8,128)(2,1)S(1)}, u32[]{:S(2)}, u32[]{:S(2)}) collective-permute-start(bf16[4,1024,128]{2,1,0:T(8,128)(2,1)S(1)} %keys_kernel.1.kv_ref), channel_id=1, source_target_pairs={{0,16},{16,0},{1,17},{17,1},{2,18},{18,2},{3,19},{19,3},{4,20},{20... | collective-permute-start | bytes 3145736 | tf_op jit(solution)/shard_map/ppermute | solution.py:352
  89.2 16.7 %copy-start.6 = (bf16[2048,64]{0,1:T(8,128)(2,1)S(1)}, bf16[2048,64]{0,1:T(8,128)(2,1)}, u32[]{:S(2)}) copy-start(bf16[2048,64]{0,1:T(8,128)(2,1)} %param.35) | copy-start | bytes 786436
  89.2 16.7 %copy-start.7 = (bf16[2048,64]{0,1:T(8,128)(2,1)S(1)}, bf16[2048,64]{0,1:T(8,128)(2,1)}, u32[]{:S(2)}) copy-start(bf16[2048,64]{0,1:T(8,128)(2,1)} %param.36) | copy-start | bytes 786436
  89.2 16.7 %copy-start.8 = (bf16[64,2048]{1,0:T(8,128)(2,1)S(1)}, bf16[64,2048]{1,0:T(8,128)(2,1)}, u32[]{:S(2)}) copy-start(bf16[64,2048]{1,0:T(8,128)(2,1)} %sd_ref.1) | copy-start | bytes 786436
  89.3 16.5 %copy-start.1 = (bf16[2,2048,64]{1,2,0:T(8,128)(2,1)S(1)}, bf16[2,2048,64]{1,2,0:T(8,128)(2,1)}, u32[]{:S(2)}) copy-start(bf16[2,2048,64]{1,2,0:T(8,128)(2,1)} %param.32) | copy-start | bytes 1572868
  89.3 16.5 %copy-start.2 = (bf16[2,2048,64]{1,2,0:T(8,128)(2,1)S(1)}, bf16[2,2048,64]{1,2,0:T(8,128)(2,1)}, u32[]{:S(2)}) copy-start(bf16[2,2048,64]{1,2,0:T(8,128)(2,1)} %param.33) | copy-start | bytes 1572868
  89.4 16.5 %copy-start.3 = (bf16[2,64,2048]{2,1,0:T(8,128)(2,1)S(1)}, bf16[2,64,2048]{2,1,0:T(8,128)(2,1)}, u32[]{:S(2)}) copy-start(bf16[2,64,2048]{2,1,0:T(8,128)(2,1)} %param.34) | copy-start | bytes 1572868
  89.4 16.5 %copy-start.10 = (f32[2048]{0:T(1024)S(1)}, f32[2048]{0:T(1024)}, u32[]{:S(2)}) copy-start(f32[2048]{0:T(1024)} %param.29) | copy-start | bytes 24580

commit v6 on v5

--- a/solution.py
+++ b/solution.py
@@ -72,8 +72,17 @@
     return picks(iota((count, N_SP * ROWS), 1) == source * ROWS + row)
 
 
-def pack_kernel(tp_ref, wide_ref, narrow_ref, rope_ref, lat_ref, gain_ref, res_ref, ids_ref, w_ref, cos_ref, sin_ref, out_ref, sel_ref):
+def pack_kernel(
+    tp_ref, wide_hbm, narrow_hbm, rope_hbm, lat_hbm, gain_hbm, res_hbm, ids_hbm, w_hbm, cos_ref, sin_ref, out_ref, sel_ref,
+    ids_ref, w_ref, wide_ref, narrow_ref, rope_ref, lat_ref, gain_ref, res_ref, sems,
+):
     t = tp_ref[0]
+    own_columns = res_hbm.at[:, pl.ds(pl.multiple_of(t * 128, 128), 128)]
+    sources = (ids_hbm, w_hbm, wide_hbm, narrow_hbm, rope_hbm, lat_hbm, gain_hbm, own_columns)
+    targets = (ids_ref, w_ref, wide_ref, narrow_ref, rope_ref, lat_ref, gain_ref, res_ref)
+    copies = [pltpu.make_async_copy(a, b, sems.at[i]) for i, (a, b) in enumerate(zip(sources, targets))]
+    for copy in copies:
+        copy.start()
     src, dst = iota((16, 128), 0), iota((16, 128), 1)
     turning = (dst < 32) | (dst >= 96)
     spread = jnp.where(turning & ((dst & 15) == src), 1.0, 0.0)
@@ -81,18 +90,23 @@
     sin = exact_tn(sin_ref[...], jnp.where((dst & 16) == 0, -spread, spread))
     src, dst = iota((128, 128), 0), iota((128, 128), 1)
     swap = picks(src == dst + jnp.where((dst & 16) == 0, 16, -16))
-
-    def turned(block):
-        return (block.astype(F32) * cos + dot(block, swap) * sin).astype(BF)
-
     first, after = picks(src == dst), picks(src + 32 == dst)
-    q_rest = turned((dot(wide_ref[:, 128:], first[:32]) + dot(narrow_ref[...], after[:96])).astype(BF))
-    rope = turned(dot_tn(rope_ref[...], first[:32]).astype(BF))
-    lat = lat_ref[...].astype(F32)
-    scaled = lat * lax.rsqrt(jnp.mean(lat * lat, axis=1, keepdims=True) + EPS)
-    normed = (scaled * gain_ref[...]).astype(BF)
-    res = res_ref[:, pl.ds(pl.multiple_of(t * 128, 128), 128)]
-
+    twice = picks((iota((TOK, 128), 1) & 63) == iota((TOK, 128), 0))
+    row = iota((4 * ROWS, 128), 0)
+    dest = div28(row)
+    place = row - dest * ROWS
+    kind = div6(place)
+    slot = dest * 6 + place - kind * 6
+    lanes = iota((4 * ROWS, 128), 1)
+    start = (dest & 1) * 32 + t * 2 + (place & 1)
+    block = (place >> 1) - 9
+    want_query = jnp.where(kind < 2, slot + kind * 1024, -100000)
+    want_rest = jnp.where(kind == 2, slot, -100000)
+    want_side = jnp.where(place >= 26, dest * 2 + place - 26 + 1024, -100000)
+    lat_masks = [picks(lanes == jnp.where((block >> 1) == pair, start + (block & 1) * 64, -1)) for pair in range(2)]
+
+    copies[0].wait()
+    copies[1].wait()
     before = picks(iota((TOK, TOK), 0) < iota((TOK, TOK), 1))
     named = [jnp.where(ids_ref[k : k + 1, :] == iota((TOK, TOK), 0), 1.0, 0.0) for k in range(2)]
     rank = dot((named[0] + named[1]).astype(BF), before)
@@ -103,47 +117,54 @@
     def either(want):
         return picks((slots[0] == want) | (slots[1] == want))
 
-    sel_ref[...] = either(iota((SLOTS, 1), 0))
-
-    row = iota((TOK, 1), 0)
+    sel_ref[...] = either(iota((SLOTS, TOK), 0))
     lane, token = iota((TOK, 128), 1), iota((TOK, 128), 0).astype(F32)
-    side = dot(picks(iota((TOK, TOK), 1) == ((row >> 1) & 1) * 32 + t * 2 + (row & 1)), rope)
-    for place in range(3):
+    expert = iota((TOK, TOK), 0)
+    side = 0.0
+    for third in range(3):
         high, low, flag = 0.0, 0.0, 0.0
         for k in range(2):
-            mask = slots[k] == row * 3 + place
+            mask = slots[k] == expert * 3 + third
             w = w_ref[k : k + 1, :]
             w_hi = w.astype(BF).astype(F32)
             high = high + jnp.where(mask, w_hi, 0.0)
             low = low + jnp.where(mask, w - w_hi, 0.0)
             flag = flag + jnp.where(mask, 1.0 - k, 0.0)
-        at = lane - 4 * place
-        side = side + dot(either(row * 3 + place), jnp.where(at == LANE_POS, token, 0.0).astype(BF))
+        at = lane - 4 * third
+        side = side + dot(either(expert * 3 + third), jnp.where(at == LANE_POS, token, 0.0).astype(BF))
         side = side + dot(high.astype(BF), picks(at == LANE_HI)) + dot(low.astype(BF), picks(at == LANE_LO))
         side = side + dot(flag.astype(BF), picks(at == LANE_FLAG))
-
-    twice = picks((iota((TOK, 128), 1) & 63) == iota((TOK, 128), 0))
     keys = [dot(slot.astype(F32).astype(BF), twice).astype(jnp.int32) for slot in slots]
-    row = iota((N_SP * ROWS, 1), 0)
-    dest = div28(row)
-    place = row - dest * ROWS
-    kind = div6(place)
-    slot = dest * 6 + place - kind * 6
-    lanes = iota((1, 128), 1)
-    tok, upper = lanes & 63, lanes >= 64
-    marks = [jnp.where(upper, key + 1024, key) for key in keys]
-    want = jnp.where(kind < 2, slot + kind * 1024, -1)
-    out = dot(picks((marks[0] == want) | (marks[1] == want)), jnp.concatenate([wide_ref[:, :128], q_rest], axis=0))
-    marks = [jnp.where(upper, tok + 1024, key) for key in keys]
-    want = jnp.where(kind == 2, slot, jnp.where(place >= 26, dest * 2 + place - 26 + 1024, -1))
-    out = out + dot(picks((marks[0] == want) | (marks[1] == want)), jnp.concatenate([res, side.astype(BF)], axis=0))
-    start = (dest & 1) * 32 + t * 2 + (place & 1)
-    block = (place >> 1) - 9
+    upper = iota((1, 128), 1) >= 64
+    query_keys = [jnp.where(upper, key + 1024, key) for key in keys]
+    rest_keys = [jnp.where(upper, -1, key) for key in keys]
+    side_key = jnp.where(upper, (iota((1, 128), 1) & 63) + 1024, -1)
+
+    for copy in copies[2:]:
+        copy.wait()
+
+    def turned(block):
+        return (block.astype(F32) * cos + dot(block, swap) * sin).astype(BF)
+
+    q_rest = turned((dot(wide_ref[:, 128:], first[:32]) + dot(narrow_ref[...], after[:96])).astype(BF))
+    rope = turned(dot_tn(rope_ref[...], first[:32]).astype(BF))
+    lat = lat_ref[...].astype(F32)
+    scaled = lat * lax.rsqrt(jnp.mean(lat * lat, axis=1, keepdims=True) + EPS)
+    normed = (scaled * gain_ref[...]).astype(BF)
+    side = side + dot(picks(iota((TOK, TOK), 1) == ((expert >> 1) & 1) * 32 + t * 2 + (expert & 1)), rope)
+    lat_part = 0.0
     for pair in range(2):
-        want = jnp.where((block >> 1) == pair, start + (block & 1) * 64, -1)
         rows = [normed[:, f * 128 : (f + 1) * 128] for f in (2 * pair, 2 * pair + 1)]
-        out = out + dot(picks(lanes == want), jnp.concatenate(rows, axis=0))
-    out_ref[...] = out.astype(BF)
+        lat_part = lat_part + dot(lat_masks[pair], jnp.concatenate(rows, axis=0))
+    query_rows = jnp.concatenate([wide_ref[:, :128], q_rest], axis=0)
+    rest_rows = jnp.concatenate([res_ref[...], side.astype(BF)], axis=0)
+    for part in range(N_SP // 4):
+        want = want_query + 24 * part
+        out = dot(picks((query_keys[0] == want) | (query_keys[1] == want)), query_rows)
+        want = want_rest + 24 * part
+        mask = (rest_keys[0] == want) | (rest_keys[1] == want) | (side_key == want_side + 8 * part)
+        out = out + dot(picks(mask), rest_rows)
+        out_ref[part * 4 * ROWS : (part + 1) * 4 * ROWS, :] = (out + lat_part).astype(BF)
 
 
 def slots_kernel(arr_ref, out_ref):
@@ -293,15 +314,19 @@
 SMEM = pl.BlockSpec(memory_space=pltpu.SMEM)
 
 
-def run(kernel, outs, *args, scalars=0, plain=0, spread=True, kind=BF):
+HBM = pl.BlockSpec(memory_space=pltpu.HBM)
+
+
+def run(kernel, outs, *args, scalars=0, plain=0, spread=True, kind=BF, scratch=()):
     spaces = [pltpu.HBM if i < plain else pltpu.VMEM for i in range(scalars, len(args))]
     placed = [pltpu.with_memory_space_constraint(a, m) for a, m in zip(args[scalars:], spaces)]
     args = [*args[:scalars], *placed]
     return pl.pallas_call(
         kernel,
         out_shape=[pltpu.VMEM(shape, kind) for shape in outs] if spread else jax.ShapeDtypeStruct(outs[0], BF),
-        in_specs=[SMEM] * scalars + [VMEM] * (len(args) - scalars),
+        in_specs=[SMEM] * scalars + [HBM if m is pltpu.HBM else VMEM for m in spaces],
         out_specs=[VMEM] * len(outs) if spread else VMEM,
+        scratch_shapes=scratch,
         compiler_params=pltpu.CompilerParams(vmem_limit_bytes=24 << 20),
         name=kernel.__name__,
     )(*args)
@@ -343,6 +368,17 @@
         route_ids.T, route_weights.T, jnp.cos(angles), jnp.sin(angles),
         scalars=1,
         plain=9,
+        scratch=[
+            pltpu.VMEM((2, TOK), jnp.int32),
+            pltpu.VMEM((2, TOK), F32),
+            pltpu.VMEM((TOK, 160), BF),
+            pltpu.VMEM((TOK, 96), BF),
+            pltpu.VMEM((32, TOK), BF),
+            pltpu.VMEM((TOK, 512), BF),
+            pltpu.VMEM((1, 512), F32),
+            pltpu.VMEM((TOK, 128), BF),
+            pltpu.SemaphoreType.DMA((8,)),
+        ],
     )
     arrived = swap_all(payload.reshape(N_SP, ROWS // 2, 2, 128), SP).reshape(N_SP * ROWS, 128)
     (spread,) = run(spread_kernel, [(N_TP, 272, 128)], arrived)

time: 142 us -> 142 us (level)
  no operation moved by 1% of the time
where the time goes in v6:
time: 142 us
  blocking collectives  127 us (89%)
  Pallas kernels  9.28 us (7%)
  starting transfers between devices  4.32 us (3%)
    all_to_all x6, blocking collectives, swap_all(): return lax.all_to_all(values, axes, split_axis=0, concat_axis=0, tiled=True)  127 us
    pallas_call x10, Pallas kernels, run(): pl.pallas_call(kernel, out_shape=[pltpu.VMEM(shape, kind) for shape in ou...  9.28 us
    ppermute x1, starting transfers between devices, local(): other = lax.ppermute(own, 'c', [(0, 1), (1, 0)])  4.32 us
  transfers between devices with their start and end apart: 1, of which 1 were waited for; matrix products, arithmetic and copies ran while one was open for 0% of the time, Pallas kernels for 1%

profile of v6, /device:TPU:1, one launch (start us, length us, event | category | flops | bytes accessed | tf_op | source)
XLA Modules:
  0.0 141.6 jit_solution(8585249285088730656)
XLA Ops:
  0.0 0.1 multiply_sine_fusion
  0.2 2.0 %pack_kernel.1 = (bf16[896,128]{1,0:T(8,128)(2,1)S(1)}, bf16[192,64]{1,0:T(8,128)(2,1)S(1)}) custom-call(s32[1]{0:T(128)} %bitcast.tp_ref, bf16[64,160]{1,0:T(8,128)(2,1)} %wide_hbm.1, bf16[64,96]{1,0:T(8,128)(2,1)} %narrow_hbm.1, bf16[32,64]{1,0:T(8,128)(2,1)} %bitcast.27, bf16[64,512]{1,0:T(8,128)(2,1)} %lat_hbm.1, f32[1,512]{1,0:T(1,128)} %bitcast.28, ...), custom_call_target="tpu_custom_call" | custom-call | tf_op jit(solution)/shard_map/pack_kernel/pallas_call | solution.py:324
  2.2 36.8 %all_to_all.30 = bf16[32,14,2,128]{3,2,1,0:T(2,128)(2,1)S(1)} all-to-all(bf16[32,14,2,128]{3,2,1,0:T(2,128)(2,1)S(1)} %bitcast.23), channel_id=1, replica_groups=mesh['z'=16,'c'=2,'tp'=16] {'z','c'}, dimensions={0} | all-to-all | bytes 458752 | tf_op jit(solution)/shard_map/all_to_all | solution.py:336
  39.0 0.5 spread_kernel.1
  39.5 0.0 copy-start.9
  39.5 23.3 %all_to_all.31.lat_ref = bf16[16,272,128]{2,1,0:T(8,128)(2,1)S(1)} all-to-all(bf16[16,272,128]{2,1,0:T(8,128)(2,1)S(1)} %spread_kernel.1), channel_id=1, replica_groups=mesh['z'=16,'c'=2,'tp'=16] {'tp'}, dimensions={0} | all-to-all | bytes 2228224 | tf_op jit(solution)/shard_map/all_to_all | solution.py:336
  62.8 0.0 copy-done.4
  62.8 0.0 copy-done.9
  62.8 0.9 keys_kernel.1.kv_ref
  63.7 0.0 copy-start
  63.7 0.0 copy-start.5
  63.7 4.3 %collective-permute-start = (bf16[4,1024,128]{2,1,0:T(8,128)(2,1)S(1)}, bf16[4,1024,128]{2,1,0:T(8,128)(2,1)S(1)}, u32[]{:S(2)}, u32[]{:S(2)}) collective-permute-start(bf16[4,1024,128]{2,1,0:T(8,128)(2,1)S(1)} %keys_kernel.1.kv_ref), channel_id=1, source_target_pairs={{0,16},{16,0},{1,17},{17,1},{2,18},{18,2},{3,19},{19,3},{4,20},{20... | collective-permute-start | bytes 3145736 | tf_op jit(solution)/shard_map/ppermute | solution.py:388
  68.1 0.5 slots_kernel.1.slot_ref
  68.6 1.0 attend_own_kernel.1
  69.7 0.7 collective-permute-done.kv_ref
  70.3 0.0 copy-done
  70.3 0.0 copy-done.5
  70.3 1.7 %attend_rest_kernel.1 = bf16[16,192,128]{2,1,0:T(8,128)(2,1)S(1)} custom-call(s32[1]{0:T(128)} %bitcast.5.core_ref, bf16[192,512]{1,0:T(8,128)(2,1)S(1)} %slots_kernel.1.slot_ref, bf16[4,1024,128]{2,1,0:T(8,128)(2,1)S(1)} %collective-permute-done.kv_ref, f32[2,192,128]{2,1,0:T(8,128)S(1)} %get-tuple-element.12.peak_ref, ...), custom_call_target="tpu_custom_call" | custom-call | tf_op jit(solution)/shard_map/attend_rest_kernel/pallas_call | solution.py:324
  72.0 16.7 %all_to_all.32.part_ref = bf16[16,192,128]{2,1,0:T(8,128)(2,1)S(1)} all-to-all(bf16[16,192,128]{2,1,0:T(8,128)(2,1)S(1)} %attend_rest_kernel.1), channel_id=1, replica_groups=mesh['z'=16,'c'=2,'tp'=16] {'tp'}, dimensions={0} | all-to-all | bytes 1572864 | tf_op jit(solution)/shard_map/all_to_all | solution.py:336
  88.8 0.1 stream_kernel.1.stream_ref
  88.9 0.0 copy-start.1
  88.9 0.0 copy-start.2
  89.0 0.0 copy-start.3
  89.0 0.0 copy-start.10
  89.0 16.5 %all_to_all.33.x_ref = bf16[16,192,128]{2,1,0:T(8,128)(2,1)S(1)} all-to-all(bf16[16,192,128]{2,1,0:T(8,128)(2,1)S(1)} %stream_kernel.1.stream_ref), channel_id=1, replica_groups=mesh['z'=16,'c'=2,'tp'=16] {'tp'}, dimensions={0} | all-to-all | bytes 1572864 | tf_op jit(solution)/shard_map/all_to_all | solution.py:336
  105.5 0.0 copy-done.6
  105.5 0.0 copy-done.7
  105.5 1.5 %expert_kernel.1 = bf16[16,192,128]{2,1,0:T(8,128)(2,1)S(1)} custom-call(bf16[16,192,128]{2,1,0:T(8,128)(2,1)S(1)} %all_to_all.33.x_ref, bf16[192,512]{1,0:T(8,128)(2,1)S(1)} %slots_kernel.1.slot_ref, f32[1,2048]{1,0:T(1,128)S(1)} %bitcast.26, bf16[2,64,2048]{2,1,0:T(8,128)(2,1)S(1)} %bitcast.18, bf16[2,64,2048]{2,1,0:T(8,128)(2,1)S(1)} %bitcast.19, ...), custom_call_target="tpu_custom_call" | custom-call | tf_op jit(solution)/shard_map/expert_kernel/pallas_call | solution.py:324
  107.1 14.8 %all_to_all.34.part_ref = bf16[16,192,128]{2,1,0:T(8,128)(2,1)S(1)} all-to-all(bf16[16,192,128]{2,1,0:T(8,128)(2,1)S(1)} %expert_kernel.1), channel_id=1, replica_groups=mesh['z'=16,'c'=2,'tp'=16] {'tp'}, dimensions={0} | all-to-all | bytes 1572864 | tf_op jit(solution)/shard_map/all_to_all | solution.py:336
  121.8 0.2 give_back_kernel.1
  122.0 18.8 %all_to_all.35 = bf16[32,3,2,128]{3,2,1,0:T(2,128)(2,1)S(1)} all-to-all(bf16[32,3,2,128]{3,2,1,0:T(2,128)(2,1)S(1)} %bitcast.25), channel_id=1, replica_groups=mesh['z'=16,'c'=2,'tp'=16] {'z','c'}, dimensions={0} | all-to-all | bytes 98304 | tf_op jit(solution)/shard_map/all_to_all | solution.py:336
  140.8 0.8 finish_kernel.1
  (11 shorter events, 0.0 us)
Async XLA Ops:
  39.5 23.3 %copy-start.4 = (bf16[512,256]{1,0:T(8,128)(2,1)S(1)}, bf16[512,256]{1,0:T(8,128)(2,1)}, u32[]{:S(2)}) copy-start(bf16[512,256]{1,0:T(8,128)(2,1)} %wide_ref.1) | copy-start | bytes 786436
  39.5 23.3 %copy-start.9 = (bf16[512,128]{1,0:T(8,128)(2,1)S(1)}, bf16[512,128]{1,0:T(8,128)(2,1)}, u32[]{:S(2)}) copy-start(bf16[512,128]{1,0:T(8,128)(2,1)} %narrow_ref.1) | copy-start | bytes 393220
  63.7 6.6 %copy-start = (bf16[128,2048]{1,0:T(8,128)(2,1)S(1)}, bf16[128,2048]{1,0:T(8,128)(2,1)}, u32[]{:S(2)}) copy-start(bf16[128,2048]{1,0:T(8,128)(2,1)} %wide_out_ref.1) | copy-start | bytes 1572868
  63.7 6.6 %copy-start.5 = (bf16[64,2048]{1,0:T(8,128)(2,1)S(1)}, bf16[64,2048]{1,0:T(8,128)(2,1)}, u32[]{:S(2)}) copy-start(bf16[64,2048]{1,0:T(8,128)(2,1)} %narrow_out_ref.1) | copy-start | bytes 786436
  63.7 6.6 %collective-permute-start = (bf16[4,1024,128]{2,1,0:T(8,128)(2,1)S(1)}, bf16[4,1024,128]{2,1,0:T(8,128)(2,1)S(1)}, u32[]{:S(2)}, u32[]{:S(2)}) collective-permute-start(bf16[4,1024,128]{2,1,0:T(8,128)(2,1)S(1)} %keys_kernel.1.kv_ref), channel_id=1, source_target_pairs={{0,16},{16,0},{1,17},{17,1},{2,18},{18,2},{3,19},{19,3},{4,20},{20... | collective-permute-start | bytes 3145736 | tf_op jit(solution)/shard_map/ppermute | solution.py:388
  88.8 16.7 %copy-start.6 = (bf16[2048,64]{0,1:T(8,128)(2,1)S(1)}, bf16[2048,64]{0,1:T(8,128)(2,1)}, u32[]{:S(2)}) copy-start(bf16[2048,64]{0,1:T(8,128)(2,1)} %param.35) | copy-start | bytes 786436
  88.8 16.7 %copy-start.7 = (bf16[2048,64]{0,1:T(8,128)(2,1)S(1)}, bf16[2048,64]{0,1:T(8,128)(2,1)}, u32[]{:S(2)}) copy-start(bf16[2048,64]{0,1:T(8,128)(2,1)} %param.36) | copy-start | bytes 786436
  88.8 16.7 %copy-start.8 = (bf16[64,2048]{1,0:T(8,128)(2,1)S(1)}, bf16[64,2048]{1,0:T(8,128)(2,1)}, u32[]{:S(2)}) copy-start(bf16[64,2048]{1,0:T(8,128)(2,1)} %sd_ref.1) | copy-start | bytes 786436
  88.9 16.5 %copy-start.1 = (bf16[2,2048,64]{1,2,0:T(8,128)(2,1)S(1)}, bf16[2,2048,64]{1,2,0:T(8,128)(2,1)}, u32[]{:S(2)}) copy-start(bf16[2,2048,64]{1,2,0:T(8,128)(2,1)} %param.32) | copy-start | bytes 1572868
  88.9 16.5 %copy-start.2 = (bf16[2,2048,64]{1,2,0:T(8,128)(2,1)S(1)}, bf16[2,2048,64]{1,2,0:T(8,128)(2,1)}, u32[]{:S(2)}) copy-start(bf16[2,2048,64]{1,2,0:T(8,128)(2,1)} %param.33) | copy-start | bytes 1572868
  89.0 16.5 %copy-start.3 = (bf16[2,64,2048]{2,1,0:T(8,128)(2,1)S(1)}, bf16[2,64,2048]{2,1,0:T(8,128)(2,1)}, u32[]{:S(2)}) copy-start(bf16[2,64,2048]{2,1,0:T(8,128)(2,1)} %param.34) | copy-start | bytes 1572868
  89.0 16.5 %copy-start.10 = (f32[2048]{0:T(1024)S(1)}, f32[2048]{0:T(1024)}, u32[]{:S(2)}) copy-start(f32[2048]{0:T(1024)} %param.29) | copy-start | bytes 24580

commit v7 on v6

--- a/solution.py
+++ b/solution.py
@@ -12,7 +12,10 @@
 THETA = 10000.0
 EPS = 1e-06
 FLOOR = -1e30
-SP = ("z", "c")
+MESH = ("z3", "z2", "z1", "z0", "c", "y1", "y0", "x1", "x0")
+SP, TP = MESH[:5], MESH[5:]
+SP_ORDER = ("z0", "c", "z3", "z2", "z1")
+TP_ORDER = ("y0", "x0", "y1", "x1")
 N_SP = 32
 N_TP = 16
 TOK = 64
@@ -56,6 +59,22 @@
     return lax.dot_general(
         a, b, (((0,), (0,)), ((), ())), precision=lax.Precision.HIGHEST, preferred_element_type=F32
     )
+
+
+def reordered(peer, order, names):
+    bits = [((peer >> (len(order) - 1 - i)) & 1) << (len(names) - 1 - names.index(axis)) for i, axis in enumerate(order)]
+    return sum(bits[1:], bits[0])
+
+
+def source_of(peer):
+    return reordered(peer, SP_ORDER, SP)
+
+
+TP_PLACES = tuple(reordered(piece, TP_ORDER, TP) for piece in range(N_TP))
+
+
+def columns(piece):
+    return slice(TP_PLACES[piece] * 128, (TP_PLACES[piece] + 1) * 128)
 
 
 def picks(mask):
@@ -93,17 +112,21 @@
     first, after = picks(src == dst), picks(src + 32 == dst)
     twice = picks((iota((TOK, 128), 1) & 63) == iota((TOK, 128), 0))
     row = iota((4 * ROWS, 128), 0)
-    dest = div28(row)
-    place = row - dest * ROWS
+    peer = div28(row)
+    place = row - peer * ROWS
+    dest = source_of(peer)
     kind = div6(place)
     slot = dest * 6 + place - kind * 6
     lanes = iota((4 * ROWS, 128), 1)
-    start = (dest & 1) * 32 + t * 2 + (place & 1)
+    start = t * 2 + (place & 1)
     block = (place >> 1) - 9
     want_query = jnp.where(kind < 2, slot + kind * 1024, -100000)
     want_rest = jnp.where(kind == 2, slot, -100000)
     want_side = jnp.where(place >= 26, dest * 2 + place - 26 + 1024, -100000)
-    lat_masks = [picks(lanes == jnp.where((block >> 1) == pair, start + (block & 1) * 64, -1)) for pair in range(2)]
+    lat_masks = [
+        [picks(lanes == jnp.where((block >> 1) == pair, start + half * 32 + (block & 1) * 64, -1)) for pair in range(2)]
+        for half in range(2)
+    ]
 
     copies[0].wait()
     copies[1].wait()
@@ -117,7 +140,9 @@
     def either(want):
         return picks((slots[0] == want) | (slots[1] == want))
 
-    sel_ref[...] = either(iota((SLOTS, TOK), 0))
+    place = iota((SLOTS, TOK), 0)
+    peer = div6(place)
+    sel_ref[...] = either(source_of(peer) * 6 + place - peer * 6)
     lane, token = iota((TOK, 128), 1), iota((TOK, 128), 0).astype(F32)
     expert = iota((TOK, TOK), 0)
     side = 0.0
@@ -152,19 +177,20 @@
     scaled = lat * lax.rsqrt(jnp.mean(lat * lat, axis=1, keepdims=True) + EPS)
     normed = (scaled * gain_ref[...]).astype(BF)
     side = side + dot(picks(iota((TOK, TOK), 1) == ((expert >> 1) & 1) * 32 + t * 2 + (expert & 1)), rope)
-    lat_part = 0.0
-    for pair in range(2):
-        rows = [normed[:, f * 128 : (f + 1) * 128] for f in (2 * pair, 2 * pair + 1)]
-        lat_part = lat_part + dot(lat_masks[pair], jnp.concatenate(rows, axis=0))
+    lat_rows = [
+        jnp.concatenate([normed[:, f * 128 : (f + 1) * 128] for f in (2 * pair, 2 * pair + 1)], axis=0) for pair in range(2)
+    ]
+    lat_parts = [dot(masks[0], lat_rows[0]) + dot(masks[1], lat_rows[1]) for masks in lat_masks]
     query_rows = jnp.concatenate([wide_ref[:, :128], q_rest], axis=0)
     rest_rows = jnp.concatenate([res_ref[...], side.astype(BF)], axis=0)
     for part in range(N_SP // 4):
-        want = want_query + 24 * part
+        away = source_of(4 * part)
+        want = want_query + 6 * away
         out = dot(picks((query_keys[0] == want) | (query_keys[1] == want)), query_rows)
-        want = want_rest + 24 * part
-        mask = (rest_keys[0] == want) | (rest_keys[1] == want) | (side_key == want_side + 8 * part)
+        want = want_rest + 6 * away
+        mask = (rest_keys[0] == want) | (rest_keys[1] == want) | (side_key == want_side + 2 * away)
         out = out + dot(picks(mask), rest_rows)
-        out_ref[part * 4 * ROWS : (part + 1) * 4 * ROWS, :] = (out + lat_part).astype(BF)
+        out_ref[part * 4 * ROWS : (part + 1) * 4 * ROWS, :] = (out + lat_parts[away & 1]).astype(BF)
 
 
 def slots_kernel(arr_ref, out_ref):
@@ -217,13 +243,14 @@
 def half_attention(half, slot_ref, kv_ref):
     q = slot_ref[:, :256]
     side = slot_ref[:, 384:].astype(F32)
-    row_pos = div6(iota((SLOTS, 1), 0)) * TOK + side_value(side, LANE_POS).astype(jnp.int32)
+    row_pos = source_of(div6(iota((SLOTS, 1), 0))) * TOK + side_value(side, LANE_POS).astype(jnp.int32)
     src, dst = iota((128, 128), 0), iota((128, 128), 1)
     q_rest = q[:, 128:]
     wide_q = jnp.concatenate([q[:, :128], dot(q_rest, picks((src < 32) & (dst == src + 96))).astype(BF)], axis=1)
     narrow_q = jnp.where(iota((SLOTS, 128), 1) >= 32, q_rest.astype(F32), 0.0).astype(BF)
     n = iota((1, N_TP * TOK), 1)
-    allowed = ((n & 63) >> 1) * TOK + (n >> 6) * 2 + (n & 1) + half * 32 <= row_pos
+    source, taken = source_of((n & 63) >> 1), reordered(n >> 6, TP_ORDER, TP)
+    allowed = source * TOK + taken * 2 + (n & 1) + half * 32 <= row_pos
     wide = dot_nt(wide_q, jnp.concatenate([kv_ref[0], kv_ref[2]], axis=1)) * (160 ** -0.5)
     narrow = dot_nt(narrow_q, kv_ref[2]) * (96 ** -0.5)
     return [jnp.where(allowed, s, FLOOR) for s in (wide, narrow)]
@@ -253,8 +280,9 @@
         attended.append(((summed + kept * sum_ref[i]) / (total + kept * total_ref[i][:, :1])).astype(BF))
     wide_att, narrow_att = attended[0], attended[1][:, :64]
     for pair in range(N_TP // 2):
-        cols = slice(pair * 256, (pair + 1) * 256)
-        both = (dot(wide_att, wide_out_ref[:, cols]) + dot(narrow_att, narrow_out_ref[:, cols])).astype(BF)
+        ends = columns(2 * pair), columns(2 * pair + 1)
+        wide, narrow = (jnp.concatenate([ref[:, c] for c in ends], axis=1) for ref in (wide_out_ref, narrow_out_ref))
+        both = (dot(wide_att, wide) + dot(narrow_att, narrow)).astype(BF)
         out_ref[2 * pair] = both[:, :128]
         out_ref[2 * pair + 1] = both[:, 128:]
 
@@ -276,11 +304,14 @@
     scale = lax.rsqrt(jnp.sum(squares, axis=1, keepdims=True) * (1.0 / D_MODEL) + EPS)
     into = jnp.zeros((SLOTS, 384), F32)
     for pair in range(N_TP // 2):
-        cols = slice(pair * 256, (pair + 1) * 256)
+        ends = columns(2 * pair), columns(2 * pair + 1)
         x = jnp.concatenate([x_ref[2 * pair], x_ref[2 * pair + 1]], axis=1).astype(F32)
-        x = (x * scale * gain_ref[:, cols]).astype(BF)
-        weights = [eg_ref[0, :, cols], eg_ref[1, :, cols], sg_ref[:, cols], eu_ref[0, :, cols], eu_ref[1, :, cols], su_ref[:, cols]]
-        into = into + dot_nt(x, jnp.concatenate(weights, axis=0))
+        x = (x * scale * jnp.concatenate([gain_ref[:, c] for c in ends], axis=1)).astype(BF)
+        halves = [
+            jnp.concatenate([eg_ref[0, :, c], eg_ref[1, :, c], sg_ref[:, c], eu_ref[0, :, c], eu_ref[1, :, c], su_ref[:, c]], axis=0)
+            for c in ends
+        ]
+        into = into + dot_nt(x, jnp.concatenate(halves, axis=1))
     gate, up = into[:, :192], into[:, 192:]
     hidden = (gate / (1.0 + jnp.exp(-gate))) * up
     side = slot_ref[:, 384:].astype(F32)
@@ -289,13 +320,12 @@
     owner = div3(iota((SLOTS, 128), 0)) & 1
     routed_hidden = jnp.where(owner == (iota((SLOTS, 128), 1) >> 6), hidden[:, :128], 0.0).astype(BF)
     shared_hidden = hidden[:, 128:].astype(BF)
-    for piece in range(N_TP // 2):
-        cols = slice(piece * 256, (piece + 1) * 256)
-        routed = dot(routed_hidden, ed_ref[:, cols])
-        shared = dot(shared_hidden, sd_ref[:, cols])
-        both = (weight * routed + flag * shared).astype(BF)
-        out_ref[2 * piece] = both[:, :128]
-        out_ref[2 * piece + 1] = both[:, 128:]
+    for pair in range(N_TP // 2):
+        ends = columns(2 * pair), columns(2 * pair + 1)
+        routed_down, shared_down = (jnp.concatenate([ref[:, c] for c in ends], axis=1) for ref in (ed_ref, sd_ref))
+        both = (weight * dot(routed_hidden, routed_down) + flag * dot(shared_hidden, shared_down)).astype(BF)
+        out_ref[2 * pair] = both[:, :128]
+        out_ref[2 * pair + 1] = both[:, 128:]
 
 
 def give_back_kernel(part_ref, stream_ref, slot_ref, out_ref):
@@ -357,7 +387,7 @@
     shared_up,
     shared_down,
 ):
-    t = lax.axis_index("tp").astype(jnp.int32)[None]
+    t = lax.axis_index(TP).astype(jnp.int32)[None]
     core = lax.axis_index("c").astype(jnp.int32)[None]
     frequency = THETA ** (-2.0 * jnp.arange(16, dtype=F32) / 32)
     positions = lax.axis_index(SP) * TOK + jnp.arange(TOK, dtype=jnp.int32)
@@ -380,9 +410,9 @@
             pltpu.SemaphoreType.DMA((8,)),
         ],
     )
-    arrived = swap_all(payload.reshape(N_SP, ROWS // 2, 2, 128), SP).reshape(N_SP * ROWS, 128)
+    arrived = swap_all(payload.reshape(N_SP, ROWS // 2, 2, 128), SP_ORDER).reshape(N_SP * ROWS, 128)
     (spread,) = run(spread_kernel, [(N_TP, 272, 128)], arrived)
-    latents = swap_all(spread, "tp")
+    latents = swap_all(spread, TP_ORDER)
     (slots,) = run(slots_kernel, [(SLOTS, 512)], arrived)
     (own,) = run(keys_kernel, [(4, N_TP * TOK, 128)], latents, wide_kv_weight, narrow_kv_weight)
     other = lax.ppermute(own, "c", [(0, 1), (1, 0)])
@@ -392,45 +422,45 @@
         core, slots, other, *state, wide_out_weight, narrow_out_weight,
         scalars=1,
     )
-    (copies,) = run(stream_kernel, [(N_TP, SLOTS, 128)], swap_all(partial, "tp"), slots)
-    rows = swap_all(copies, "tp")
+    (copies,) = run(stream_kernel, [(N_TP, SLOTS, 128)], swap_all(partial, TP_ORDER), slots)
+    rows = swap_all(copies, TP_ORDER)
     (partial,) = run(
         expert_kernel, [(N_TP, SLOTS, 128)],
         rows, slots, norm_gain[None, :],
         expert_gate.swapaxes(1, 2), expert_up.swapaxes(1, 2), expert_down.reshape(128, D_MODEL),
         shared_gate.T, shared_up.T, shared_down,
     )
-    (back,) = run(give_back_kernel, [(SLOTS, 128)], swap_all(partial, "tp"), copies, slots)
-    back = swap_all(back.reshape(N_SP, 3, 2, 128), SP).reshape(SLOTS, 128)
+    (back,) = run(give_back_kernel, [(SLOTS, 128)], swap_all(partial, TP_ORDER), copies, slots)
+    back = swap_all(back.reshape(N_SP, 3, 2, 128), SP_ORDER).reshape(SLOTS, 128)
     return run(finish_kernel, [(TOK, 128)], chosen, back, spread=False)
 
 
 def solution(mesh):
-    torus = Mesh(mesh.devices.reshape(16, 2, mesh.shape["tp"]), ("z", "c", "tp"))
+    torus = Mesh(mesh.devices.reshape((2,) * len(MESH)), MESH)
     return jax.shard_map(
         local,
         mesh=torus,
         in_specs=(
-            P(SP, "tp"),
-            P(SP, "tp"),
+            P(SP, TP),
+            P(SP, TP),
             P(SP, None),
             P(SP, None),
             P(),
-            P(None, "tp"),
-            P(None, "tp"),
-            P("tp", None),
-            P("tp", None),
+            P(None, TP),
+            P(None, TP),
+            P(TP, None),
+            P(TP, None),
             P(SP, None),
             P(),
             P(SP, None),
             P(SP, None),
-            P(SP, None, "tp"),
-            P(SP, None, "tp"),
-            P(SP, "tp", None),
-            P(None, "tp"),
-            P(None, "tp"),
-            P("tp", None),
+            P(SP, None, TP),
+            P(SP, None, TP),
+            P(SP, TP, None),
+            P(None, TP),
+            P(None, TP),
+            P(TP, None),
         ),
-        out_specs=P(SP, "tp"),
+        out_specs=P(SP, TP),
         check_vma=False,
     )

time: 142 us -> 140 us (0.986)
  blocking collectives: 127 us -> 125 us
    all_to_all x6, blocking collectives: 127 us -> 125 us  [swap_all(): return lax.all_to_all(values, axes, split_axis=0, concat_axis=0, tiled=True)]
where the time goes in v7:
time: 140 us
  blocking collectives  125 us (89%)
  Pallas kernels  9.28 us (7%)
  starting transfers between devices  4.53 us (3%)
    all_to_all x6, blocking collectives, swap_all(): return lax.all_to_all(values, axes, split_axis=0, concat_axis=0, tiled=True)  125 us
    pallas_call x10, Pallas kernels, run(): pl.pallas_call(kernel, out_shape=[pltpu.VMEM(shape, kind) for shape in ou...  9.28 us
    ppermute x1, starting transfers between devices, local(): other = lax.ppermute(own, 'c', [(0, 1), (1, 0)])  4.53 us
  transfers between devices with their start and end apart: 1, of which 1 were waited for; matrix products, arithmetic and copies ran while one was open for 0% of the time, Pallas kernels for 1%

profile of v7, /device:TPU:1, one launch (start us, length us, event | category | flops | bytes accessed | tf_op | source)
XLA Modules:
  0.0 139.9 jit_solution(17301172493284290025)
XLA Ops:
  0.1 0.1 multiply_sine_fusion
  0.2 2.0 %pack_kernel.1 = (bf16[896,128]{1,0:T(8,128)(2,1)S(1)}, bf16[192,64]{1,0:T(8,128)(2,1)S(1)}) custom-call(s32[1]{0:T(128)} %bitcast.tp_ref, bf16[64,160]{1,0:T(8,128)(2,1)} %wide_hbm.1, bf16[64,96]{1,0:T(8,128)(2,1)} %narrow_hbm.1, bf16[32,64]{1,0:T(8,128)(2,1)} %bitcast.27, bf16[64,512]{1,0:T(8,128)(2,1)} %lat_hbm.1, f32[1,512]{1,0:T(1,128)} %bitcast.28, ...), custom_call_target="tpu_custom_call" | custom-call | tf_op jit(solution)/shard_map/pack_kernel/pallas_call | solution.py:354
  2.2 33.7 %all_to_all.30 = bf16[32,14,2,128]{3,2,1,0:T(2,128)(2,1)S(1)} all-to-all(bf16[32,14,2,128]{3,2,1,0:T(2,128)(2,1)S(1)} %bitcast.23), channel_id=1, replica_groups=mesh['z3'=2,'z2'=2,'z1'=2,'z0'=2,'c'=2,'y1'=2,'y0'=2,'x1'=2,'x0'=2] {'z0..., dimensions={0} | all-to-all | bytes 458752 | tf_op jit(solution)/shard_map/all_to_all | solution.py:366
  35.8 0.5 spread_kernel.1
  36.3 0.0 copy-start.9
  36.3 23.2 %all_to_all.31.lat_ref = bf16[16,272,128]{2,1,0:T(8,128)(2,1)S(1)} all-to-all(bf16[16,272,128]{2,1,0:T(8,128)(2,1)S(1)} %spread_kernel.1), channel_id=1, replica_groups=mesh['z3'=2,'z2'=2,'z1'=2,'z0'=2,'c'=2,'y1'=2,'y0'=2,'x1'=2,'x0'=2] {'y0..., dimensions={0} | all-to-all | bytes 2228224 | tf_op jit(solution)/shard_map/all_to_all | solution.py:366
  59.5 0.0 copy-done.4
  59.5 0.0 copy-done.9
  59.5 0.9 keys_kernel.1.kv_ref
  60.5 0.0 copy-start
  60.5 0.0 copy-start.5
  60.5 4.5 %collective-permute-start = (bf16[4,1024,128]{2,1,0:T(8,128)(2,1)S(1)}, bf16[4,1024,128]{2,1,0:T(8,128)(2,1)S(1)}, u32[]{:S(2)}, u32[]{:S(2)}) collective-permute-start(bf16[4,1024,128]{2,1,0:T(8,128)(2,1)S(1)} %keys_kernel.1.kv_ref), channel_id=1, source_target_pairs={{0,16},{16,0},{1,17},{17,1},{2,18},{18,2},{3,19},{19,3},{4,20},{20... | collective-permute-start | bytes 3145736 | tf_op jit(solution)/shard_map/ppermute | solution.py:418
  65.0 0.5 slots_kernel.1.slot_ref
  65.5 1.1 attend_own_kernel.1
  66.6 0.7 collective-permute-done.kv_ref
  67.3 0.0 copy-done
  67.3 0.0 copy-done.5
  67.3 1.7 %attend_rest_kernel.1 = bf16[16,192,128]{2,1,0:T(8,128)(2,1)S(1)} custom-call(s32[1]{0:T(128)} %bitcast.5.core_ref, bf16[192,512]{1,0:T(8,128)(2,1)S(1)} %slots_kernel.1.slot_ref, bf16[4,1024,128]{2,1,0:T(8,128)(2,1)S(1)} %collective-permute-done.kv_ref, f32[2,192,128]{2,1,0:T(8,128)S(1)} %get-tuple-element.12.peak_ref, ...), custom_call_target="tpu_custom_call" | custom-call | tf_op jit(solution)/shard_map/attend_rest_kernel/pallas_call | solution.py:354
  69.0 15.9 %all_to_all.32.part_ref = bf16[16,192,128]{2,1,0:T(8,128)(2,1)S(1)} all-to-all(bf16[16,192,128]{2,1,0:T(8,128)(2,1)S(1)} %attend_rest_kernel.1), channel_id=1, replica_groups=mesh['z3'=2,'z2'=2,'z1'=2,'z0'=2,'c'=2,'y1'=2,'y0'=2,'x1'=2,'x0'=2] {'y0..., dimensions={0} | all-to-all | bytes 1572864 | tf_op jit(solution)/shard_map/all_to_all | solution.py:366
  84.9 0.1 stream_kernel.1.stream_ref
  85.0 0.0 copy-start.1
  85.0 0.0 copy-start.2
  85.0 0.0 copy-start.3
  85.0 0.0 copy-start.10
  85.1 15.0 %all_to_all.33.x_ref = bf16[16,192,128]{2,1,0:T(8,128)(2,1)S(1)} all-to-all(bf16[16,192,128]{2,1,0:T(8,128)(2,1)S(1)} %stream_kernel.1.stream_ref), channel_id=1, replica_groups=mesh['z3'=2,'z2'=2,'z1'=2,'z0'=2,'c'=2,'y1'=2,'y0'=2,'x1'=2,'x0'=2] {'y0..., dimensions={0} | all-to-all | bytes 1572864 | tf_op jit(solution)/shard_map/all_to_all | solution.py:366
  100.0 0.0 copy-done.6
  100.0 0.0 copy-done.7
  100.1 1.6 %expert_kernel.1 = bf16[16,192,128]{2,1,0:T(8,128)(2,1)S(1)} custom-call(bf16[16,192,128]{2,1,0:T(8,128)(2,1)S(1)} %all_to_all.33.x_ref, bf16[192,512]{1,0:T(8,128)(2,1)S(1)} %slots_kernel.1.slot_ref, f32[1,2048]{1,0:T(1,128)S(1)} %bitcast.26, bf16[2,64,2048]{2,1,0:T(8,128)(2,1)S(1)} %bitcast.18, bf16[2,64,2048]{2,1,0:T(8,128)(2,1)S(1)} %bitcast.19, ...), custom_call_target="tpu_custom_call" | custom-call | tf_op jit(solution)/shard_map/expert_kernel/pallas_call | solution.py:354
  101.6 15.3 %all_to_all.34.part_ref = bf16[16,192,128]{2,1,0:T(8,128)(2,1)S(1)} all-to-all(bf16[16,192,128]{2,1,0:T(8,128)(2,1)S(1)} %expert_kernel.1), channel_id=1, replica_groups=mesh['z3'=2,'z2'=2,'z1'=2,'z0'=2,'c'=2,'y1'=2,'y0'=2,'x1'=2,'x0'=2] {'y0..., dimensions={0} | all-to-all | bytes 1572864 | tf_op jit(solution)/shard_map/all_to_all | solution.py:366
  116.9 0.2 give_back_kernel.1
  117.1 22.1 %all_to_all.35 = bf16[32,3,2,128]{3,2,1,0:T(2,128)(2,1)S(1)} all-to-all(bf16[32,3,2,128]{3,2,1,0:T(2,128)(2,1)S(1)} %bitcast.25), channel_id=1, replica_groups=mesh['z3'=2,'z2'=2,'z1'=2,'z0'=2,'c'=2,'y1'=2,'y0'=2,'x1'=2,'x0'=2] {'z0..., dimensions={0} | all-to-all | bytes 98304 | tf_op jit(solution)/shard_map/all_to_all | solution.py:366
  139.1 0.8 finish_kernel.1
  (11 shorter events, 0.0 us)
Async XLA Ops:
  36.3 23.2 %copy-start.4 = (bf16[512,256]{1,0:T(8,128)(2,1)S(1)}, bf16[512,256]{1,0:T(8,128)(2,1)}, u32[]{:S(2)}) copy-start(bf16[512,256]{1,0:T(8,128)(2,1)} %wide_ref.1) | copy-start | bytes 786436
  36.3 23.2 %copy-start.9 = (bf16[512,128]{1,0:T(8,128)(2,1)S(1)}, bf16[512,128]{1,0:T(8,128)(2,1)}, u32[]{:S(2)}) copy-start(bf16[512,128]{1,0:T(8,128)(2,1)} %narrow_ref.1) | copy-start | bytes 393220
  60.5 6.8 %copy-start = (bf16[128,2048]{1,0:T(8,128)(2,1)S(1)}, bf16[128,2048]{1,0:T(8,128)(2,1)}, u32[]{:S(2)}) copy-start(bf16[128,2048]{1,0:T(8,128)(2,1)} %wide_out_ref.1) | copy-start | bytes 1572868
  60.5 6.8 %copy-start.5 = (bf16[64,2048]{1,0:T(8,128)(2,1)S(1)}, bf16[64,2048]{1,0:T(8,128)(2,1)}, u32[]{:S(2)}) copy-start(bf16[64,2048]{1,0:T(8,128)(2,1)} %narrow_out_ref.1) | copy-start | bytes 786436
  60.5 6.8 %collective-permute-start = (bf16[4,1024,128]{2,1,0:T(8,128)(2,1)S(1)}, bf16[4,1024,128]{2,1,0:T(8,128)(2,1)S(1)}, u32[]{:S(2)}, u32[]{:S(2)}) collective-permute-start(bf16[4,1024,128]{2,1,0:T(8,128)(2,1)S(1)} %keys_kernel.1.kv_ref), channel_id=1, source_target_pairs={{0,16},{16,0},{1,17},{17,1},{2,18},{18,2},{3,19},{19,3},{4,20},{20... | collective-permute-start | bytes 3145736 | tf_op jit(solution)/shard_map/ppermute | solution.py:418
  84.8 15.2 %copy-start.6 = (bf16[2048,64]{0,1:T(8,128)(2,1)S(1)}, bf16[2048,64]{0,1:T(8,128)(2,1)}, u32[]{:S(2)}) copy-start(bf16[2048,64]{0,1:T(8,128)(2,1)} %param.35) | copy-start | bytes 786436
  84.9 15.2 %copy-start.7 = (bf16[2048,64]{0,1:T(8,128)(2,1)S(1)}, bf16[2048,64]{0,1:T(8,128)(2,1)}, u32[]{:S(2)}) copy-start(bf16[2048,64]{0,1:T(8,128)(2,1)} %param.36) | copy-start | bytes 786436
  84.9 15.2 %copy-start.8 = (bf16[64,2048]{1,0:T(8,128)(2,1)S(1)}, bf16[64,2048]{1,0:T(8,128)(2,1)}, u32[]{:S(2)}) copy-start(bf16[64,2048]{1,0:T(8,128)(2,1)} %sd_ref.1) | copy-start | bytes 786436
  85.0 15.0 %copy-start.1 = (bf16[2,2048,64]{1,2,0:T(8,128)(2,1)S(1)}, bf16[2,2048,64]{1,2,0:T(8,128)(2,1)}, u32[]{:S(2)}) copy-start(bf16[2,2048,64]{1,2,0:T(8,128)(2,1)} %param.32) | copy-start | bytes 1572868
  85.0 15.0 %copy-start.2 = (bf16[2,2048,64]{1,2,0:T(8,128)(2,1)S(1)}, bf16[2,2048,64]{1,2,0:T(8,128)(2,1)}, u32[]{:S(2)}) copy-start(bf16[2,2048,64]{1,2,0:T(8,128)(2,1)} %param.33) | copy-start | bytes 1572868
  85.0 15.0 %copy-start.3 = (bf16[2,64,2048]{2,1,0:T(8,128)(2,1)S(1)}, bf16[2,64,2048]{2,1,0:T(8,128)(2,1)}, u32[]{:S(2)}) copy-start(bf16[2,64,2048]{2,1,0:T(8,128)(2,1)} %param.34) | copy-start | bytes 1572868
  85.0 15.0 %copy-start.10 = (f32[2048]{0:T(1024)S(1)}, f32[2048]{0:T(1024)}, u32[]{:S(2)}) copy-start(f32[2048]{0:T(1024)} %param.29) | copy-start | bytes 24580

commit v8 on v7

--- a/solution.py
+++ b/solution.py
@@ -14,7 +14,7 @@
 FLOOR = -1e30
 MESH = ("z3", "z2", "z1", "z0", "c", "y1", "y0", "x1", "x0")
 SP, TP = MESH[:5], MESH[5:]
-SP_ORDER = ("z0", "c", "z3", "z2", "z1")
+SP_ORDER = ("c", "z1", "z0", "z3", "z2")
 TP_ORDER = ("y0", "x0", "y1", "x1")
 N_SP = 32
 N_TP = 16

time: 140 us -> 140 us (level)
  no operation moved by 1% of the time
where the time goes in v8:
time: 140 us; the launch traced here: 139 us
  blocking collectives  124 us (89%)
  Pallas kernels  9.28 us (7%)
  starting transfers between devices  5.03 us (4%)
    all_to_all x6, blocking collectives, swap_all(): return lax.all_to_all(values, axes, split_axis=0, concat_axis=0, tiled=True)  124 us
    pallas_call x10, Pallas kernels, run(): pl.pallas_call(kernel, out_shape=[pltpu.VMEM(shape, kind) for shape in ou...  9.28 us
    ppermute x1, starting transfers between devices, local(): other = lax.ppermute(own, 'c', [(0, 1), (1, 0)])  5.03 us
  transfers between devices with their start and end apart: 1, of which 1 were waited for; matrix products, arithmetic and copies ran while one was open for 0% of the time, Pallas kernels for 1%

profile of v8, /device:TPU:1, one launch (start us, length us, event | category | flops | bytes accessed | tf_op | source)
XLA Modules:
  0.0 139.3 jit_solution(13077005035945862324)
XLA Ops:
  0.1 0.1 multiply_sine_fusion
  0.2 2.0 %pack_kernel.1 = (bf16[896,128]{1,0:T(8,128)(2,1)S(1)}, bf16[192,64]{1,0:T(8,128)(2,1)S(1)}) custom-call(s32[1]{0:T(128)} %bitcast.tp_ref, bf16[64,160]{1,0:T(8,128)(2,1)} %wide_hbm.1, bf16[64,96]{1,0:T(8,128)(2,1)} %narrow_hbm.1, bf16[32,64]{1,0:T(8,128)(2,1)} %bitcast.27, bf16[64,512]{1,0:T(8,128)(2,1)} %lat_hbm.1, f32[1,512]{1,0:T(1,128)} %bitcast.28, ...), custom_call_target="tpu_custom_call" | custom-call | tf_op jit(solution)/shard_map/pack_kernel/pallas_call | solution.py:354
  2.2 32.4 %all_to_all.30 = bf16[32,14,2,128]{3,2,1,0:T(2,128)(2,1)S(1)} all-to-all(bf16[32,14,2,128]{3,2,1,0:T(2,128)(2,1)S(1)} %bitcast.23), channel_id=1, replica_groups=mesh['z3'=2,'z2'=2,'z1'=2,'z0'=2,'c'=2,'y1'=2,'y0'=2,'x1'=2,'x0'=2] {'c'..., dimensions={0} | all-to-all | bytes 458752 | tf_op jit(solution)/shard_map/all_to_all | solution.py:366
  34.5 0.5 spread_kernel.1
  35.0 0.0 copy-start.9
  35.0 22.7 %all_to_all.31.lat_ref = bf16[16,272,128]{2,1,0:T(8,128)(2,1)S(1)} all-to-all(bf16[16,272,128]{2,1,0:T(8,128)(2,1)S(1)} %spread_kernel.1), channel_id=1, replica_groups=mesh['z3'=2,'z2'=2,'z1'=2,'z0'=2,'c'=2,'y1'=2,'y0'=2,'x1'=2,'x0'=2] {'y0..., dimensions={0} | all-to-all | bytes 2228224 | tf_op jit(solution)/shard_map/all_to_all | solution.py:366
  57.7 0.0 copy-done.4
  57.8 0.0 copy-done.9
  57.8 0.9 keys_kernel.1.kv_ref
  58.7 0.0 copy-start
  58.7 0.0 copy-start.5
  58.7 5.0 %collective-permute-start = (bf16[4,1024,128]{2,1,0:T(8,128)(2,1)S(1)}, bf16[4,1024,128]{2,1,0:T(8,128)(2,1)S(1)}, u32[]{:S(2)}, u32[]{:S(2)}) collective-permute-start(bf16[4,1024,128]{2,1,0:T(8,128)(2,1)S(1)} %keys_kernel.1.kv_ref), channel_id=1, source_target_pairs={{0,16},{16,0},{1,17},{17,1},{2,18},{18,2},{3,19},{19,3},{4,20},{20... | collective-permute-start | bytes 3145736 | tf_op jit(solution)/shard_map/ppermute | solution.py:418
  63.7 0.5 slots_kernel.1.slot_ref
  64.3 1.1 attend_own_kernel.1
  65.3 0.7 collective-permute-done.kv_ref
  66.0 0.0 copy-done
  66.0 0.0 copy-done.5
  66.0 1.7 %attend_rest_kernel.1 = bf16[16,192,128]{2,1,0:T(8,128)(2,1)S(1)} custom-call(s32[1]{0:T(128)} %bitcast.5.core_ref, bf16[192,512]{1,0:T(8,128)(2,1)S(1)} %slots_kernel.1.slot_ref, bf16[4,1024,128]{2,1,0:T(8,128)(2,1)S(1)} %collective-permute-done.kv_ref, f32[2,192,128]{2,1,0:T(8,128)S(1)} %get-tuple-element.12.peak_ref, ...), custom_call_target="tpu_custom_call" | custom-call | tf_op jit(solution)/shard_map/attend_rest_kernel/pallas_call | solution.py:354
  67.7 15.8 %all_to_all.32.part_ref = bf16[16,192,128]{2,1,0:T(8,128)(2,1)S(1)} all-to-all(bf16[16,192,128]{2,1,0:T(8,128)(2,1)S(1)} %attend_rest_kernel.1), channel_id=1, replica_groups=mesh['z3'=2,'z2'=2,'z1'=2,'z0'=2,'c'=2,'y1'=2,'y0'=2,'x1'=2,'x0'=2] {'y0..., dimensions={0} | all-to-all | bytes 1572864 | tf_op jit(solution)/shard_map/all_to_all | solution.py:366
  83.6 0.1 stream_kernel.1.stream_ref
  83.7 0.0 copy-start.1
  83.7 0.0 copy-start.2
  83.7 0.0 copy-start.3
  83.8 0.0 copy-start.10
  83.8 15.0 %all_to_all.33.x_ref = bf16[16,192,128]{2,1,0:T(8,128)(2,1)S(1)} all-to-all(bf16[16,192,128]{2,1,0:T(8,128)(2,1)S(1)} %stream_kernel.1.stream_ref), channel_id=1, replica_groups=mesh['z3'=2,'z2'=2,'z1'=2,'z0'=2,'c'=2,'y1'=2,'y0'=2,'x1'=2,'x0'=2] {'y0..., dimensions={0} | all-to-all | bytes 1572864 | tf_op jit(solution)/shard_map/all_to_all | solution.py:366
  98.7 0.0 copy-done.6
  98.7 0.0 copy-done.7
  98.8 1.6 %expert_kernel.1 = bf16[16,192,128]{2,1,0:T(8,128)(2,1)S(1)} custom-call(bf16[16,192,128]{2,1,0:T(8,128)(2,1)S(1)} %all_to_all.33.x_ref, bf16[192,512]{1,0:T(8,128)(2,1)S(1)} %slots_kernel.1.slot_ref, f32[1,2048]{1,0:T(1,128)S(1)} %bitcast.26, bf16[2,64,2048]{2,1,0:T(8,128)(2,1)S(1)} %bitcast.18, bf16[2,64,2048]{2,1,0:T(8,128)(2,1)S(1)} %bitcast.19, ...), custom_call_target="tpu_custom_call" | custom-call | tf_op jit(solution)/shard_map/expert_kernel/pallas_call | solution.py:354
  100.3 15.3 %all_to_all.34.part_ref = bf16[16,192,128]{2,1,0:T(8,128)(2,1)S(1)} all-to-all(bf16[16,192,128]{2,1,0:T(8,128)(2,1)S(1)} %expert_kernel.1), channel_id=1, replica_groups=mesh['z3'=2,'z2'=2,'z1'=2,'z0'=2,'c'=2,'y1'=2,'y0'=2,'x1'=2,'x0'=2] {'y0..., dimensions={0} | all-to-all | bytes 1572864 | tf_op jit(solution)/shard_map/all_to_all | solution.py:366
  115.6 0.2 give_back_kernel.1
  115.8 22.7 %all_to_all.35 = bf16[32,3,2,128]{3,2,1,0:T(2,128)(2,1)S(1)} all-to-all(bf16[32,3,2,128]{3,2,1,0:T(2,128)(2,1)S(1)} %bitcast.25), channel_id=1, replica_groups=mesh['z3'=2,'z2'=2,'z1'=2,'z0'=2,'c'=2,'y1'=2,'y0'=2,'x1'=2,'x0'=2] {'c'..., dimensions={0} | all-to-all | bytes 98304 | tf_op jit(solution)/shard_map/all_to_all | solution.py:366
  138.5 0.8 finish_kernel.1
  (11 shorter events, 0.0 us)
Async XLA Ops:
  35.0 22.8 %copy-start.4 = (bf16[512,256]{1,0:T(8,128)(2,1)S(1)}, bf16[512,256]{1,0:T(8,128)(2,1)}, u32[]{:S(2)}) copy-start(bf16[512,256]{1,0:T(8,128)(2,1)} %wide_ref.1) | copy-start | bytes 786436
  35.0 22.8 %copy-start.9 = (bf16[512,128]{1,0:T(8,128)(2,1)S(1)}, bf16[512,128]{1,0:T(8,128)(2,1)}, u32[]{:S(2)}) copy-start(bf16[512,128]{1,0:T(8,128)(2,1)} %narrow_ref.1) | copy-start | bytes 393220
  58.7 7.3 %copy-start = (bf16[128,2048]{1,0:T(8,128)(2,1)S(1)}, bf16[128,2048]{1,0:T(8,128)(2,1)}, u32[]{:S(2)}) copy-start(bf16[128,2048]{1,0:T(8,128)(2,1)} %wide_out_ref.1) | copy-start | bytes 1572868
  58.7 7.3 %copy-start.5 = (bf16[64,2048]{1,0:T(8,128)(2,1)S(1)}, bf16[64,2048]{1,0:T(8,128)(2,1)}, u32[]{:S(2)}) copy-start(bf16[64,2048]{1,0:T(8,128)(2,1)} %narrow_out_ref.1) | copy-start | bytes 786436
  58.7 7.3 %collective-permute-start = (bf16[4,1024,128]{2,1,0:T(8,128)(2,1)S(1)}, bf16[4,1024,128]{2,1,0:T(8,128)(2,1)S(1)}, u32[]{:S(2)}, u32[]{:S(2)}) collective-permute-start(bf16[4,1024,128]{2,1,0:T(8,128)(2,1)S(1)} %keys_kernel.1.kv_ref), channel_id=1, source_target_pairs={{0,16},{16,0},{1,17},{17,1},{2,18},{18,2},{3,19},{19,3},{4,20},{20... | collective-permute-start | bytes 3145736 | tf_op jit(solution)/shard_map/ppermute | solution.py:418
  83.6 15.2 %copy-start.6 = (bf16[2048,64]{0,1:T(8,128)(2,1)S(1)}, bf16[2048,64]{0,1:T(8,128)(2,1)}, u32[]{:S(2)}) copy-start(bf16[2048,64]{0,1:T(8,128)(2,1)} %param.35) | copy-start | bytes 786436
  83.6 15.2 %copy-start.7 = (bf16[2048,64]{0,1:T(8,128)(2,1)S(1)}, bf16[2048,64]{0,1:T(8,128)(2,1)}, u32[]{:S(2)}) copy-start(bf16[2048,64]{0,1:T(8,128)(2,1)} %param.36) | copy-start | bytes 786436
  83.6 15.2 %copy-start.8 = (bf16[64,2048]{1,0:T(8,128)(2,1)S(1)}, bf16[64,2048]{1,0:T(8,128)(2,1)}, u32[]{:S(2)}) copy-start(bf16[64,2048]{1,0:T(8,128)(2,1)} %sd_ref.1) | copy-start | bytes 786436
  83.7 15.0 %copy-start.1 = (bf16[2,2048,64]{1,2,0:T(8,128)(2,1)S(1)}, bf16[2,2048,64]{1,2,0:T(8,128)(2,1)}, u32[]{:S(2)}) copy-start(bf16[2,2048,64]{1,2,0:T(8,128)(2,1)} %param.32) | copy-start | bytes 1572868
  83.7 15.0 %copy-start.2 = (bf16[2,2048,64]{1,2,0:T(8,128)(2,1)S(1)}, bf16[2,2048,64]{1,2,0:T(8,128)(2,1)}, u32[]{:S(2)}) copy-start(bf16[2,2048,64]{1,2,0:T(8,128)(2,1)} %param.33) | copy-start | bytes 1572868
  83.7 15.0 %copy-start.3 = (bf16[2,64,2048]{2,1,0:T(8,128)(2,1)S(1)}, bf16[2,64,2048]{2,1,0:T(8,128)(2,1)}, u32[]{:S(2)}) copy-start(bf16[2,64,2048]{2,1,0:T(8,128)(2,1)} %param.34) | copy-start | bytes 1572868
  83.8 15.0 %copy-start.10 = (f32[2048]{0:T(1024)S(1)}, f32[2048]{0:T(1024)}, u32[]{:S(2)}) copy-start(f32[2048]{0:T(1024)} %param.29) | copy-start | bytes 24580

commit v9 on v8

--- a/solution.py
+++ b/solution.py
@@ -251,20 +251,23 @@
     n = iota((1, N_TP * TOK), 1)
     source, taken = source_of((n & 63) >> 1), reordered(n >> 6, TP_ORDER, TP)
     allowed = source * TOK + taken * 2 + (n & 1) + half * 32 <= row_pos
-    wide = dot_nt(wide_q, jnp.concatenate([kv_ref[0], kv_ref[2]], axis=1)) * (160 ** -0.5)
-    narrow = dot_nt(narrow_q, kv_ref[2]) * (96 ** -0.5)
+    wide = dot_nt(wide_q, jnp.concatenate([kv_ref[0], kv_ref[2]], axis=1))
+    narrow = dot_nt(narrow_q, kv_ref[2])
     return [jnp.where(allowed, s, FLOOR) for s in (wide, narrow)]
 
 
-def weighed(scores, peak, values):
-    e = jnp.exp(scores - peak)
+RATES = tuple(width ** -0.5 * 1.4426950408889634 for width in (160, 96))
+
+
+def weighed(scores, peak, rate, values):
+    e = jnp.exp2((scores - peak) * rate)
     return jnp.sum(e, axis=1, keepdims=True), dot(e.astype(BF), values)
 
 
 def attend_own_kernel(core_ref, slot_ref, kv_ref, peak_ref, total_ref, sum_ref):
     for i, scores in enumerate(half_attention(core_ref[0], slot_ref, kv_ref)):
         peak = jnp.max(scores, axis=1, keepdims=True)
-        total, summed = weighed(scores, peak, kv_ref[1 + 2 * i])
+        total, summed = weighed(scores, peak, RATES[i], kv_ref[1 + 2 * i])
         peak_ref[i] = jnp.broadcast_to(peak, (SLOTS, 128))
         total_ref[i] = jnp.broadcast_to(total, (SLOTS, 128))
         sum_ref[i] = summed
@@ -275,8 +278,8 @@
     for i, scores in enumerate(half_attention(1 - core_ref[0], slot_ref, kv_ref)):
         old = peak_ref[i][:, :1]
         peak = jnp.maximum(old, jnp.max(scores, axis=1, keepdims=True))
-        total, summed = weighed(scores, peak, kv_ref[1 + 2 * i])
-        kept = jnp.exp(old - peak)
+        total, summed = weighed(scores, peak, RATES[i], kv_ref[1 + 2 * i])
+        kept = jnp.exp2((old - peak) * RATES[i])
         attended.append(((summed + kept * sum_ref[i]) / (total + kept * total_ref[i][:, :1])).astype(BF))
     wide_att, narrow_att = attended[0], attended[1][:, :64]
     for pair in range(N_TP // 2):

time: 140 us -> 140 us (level)
  no operation moved by 1% of the time
where the time goes in v9:
time: 140 us; the launch traced here: 139 us
  blocking collectives  124 us (89%)
  Pallas kernels  9.18 us (7%)
  starting transfers between devices  5.03 us (4%)
    all_to_all x6, blocking collectives, swap_all(): return lax.all_to_all(values, axes, split_axis=0, concat_axis=0, tiled=True)  124 us
    pallas_call x10, Pallas kernels, run(): pl.pallas_call(kernel, out_shape=[pltpu.VMEM(shape, kind) for shape in ou...  9.18 us
    ppermute x1, starting transfers between devices, local(): other = lax.ppermute(own, 'c', [(0, 1), (1, 0)])  5.03 us
  transfers between devices with their start and end apart: 1, of which 1 were waited for; matrix products, arithmetic and copies ran while one was open for 0% of the time, Pallas kernels for 1%

profile of v9, /device:TPU:1, one launch (start us, length us, event | category | flops | bytes accessed | tf_op | source)
XLA Modules:
  0.0 139.2 jit_solution(16960261029878414428)
XLA Ops:
  0.1 0.1 multiply_sine_fusion
  0.2 2.0 %pack_kernel.1 = (bf16[896,128]{1,0:T(8,128)(2,1)S(1)}, bf16[192,64]{1,0:T(8,128)(2,1)S(1)}) custom-call(s32[1]{0:T(128)} %bitcast.tp_ref, bf16[64,160]{1,0:T(8,128)(2,1)} %wide_hbm.1, bf16[64,96]{1,0:T(8,128)(2,1)} %narrow_hbm.1, bf16[32,64]{1,0:T(8,128)(2,1)} %bitcast.27, bf16[64,512]{1,0:T(8,128)(2,1)} %lat_hbm.1, f32[1,512]{1,0:T(1,128)} %bitcast.28, ...), custom_call_target="tpu_custom_call" | custom-call | tf_op jit(solution)/shard_map/pack_kernel/pallas_call | solution.py:357
  2.2 32.4 %all_to_all.30 = bf16[32,14,2,128]{3,2,1,0:T(2,128)(2,1)S(1)} all-to-all(bf16[32,14,2,128]{3,2,1,0:T(2,128)(2,1)S(1)} %bitcast.23), channel_id=1, replica_groups=mesh['z3'=2,'z2'=2,'z1'=2,'z0'=2,'c'=2,'y1'=2,'y0'=2,'x1'=2,'x0'=2] {'c'..., dimensions={0} | all-to-all | bytes 458752 | tf_op jit(solution)/shard_map/all_to_all | solution.py:369
  34.5 0.5 spread_kernel.1
  35.0 0.0 copy-start.9
  35.0 22.7 %all_to_all.31.lat_ref = bf16[16,272,128]{2,1,0:T(8,128)(2,1)S(1)} all-to-all(bf16[16,272,128]{2,1,0:T(8,128)(2,1)S(1)} %spread_kernel.1), channel_id=1, replica_groups=mesh['z3'=2,'z2'=2,'z1'=2,'z0'=2,'c'=2,'y1'=2,'y0'=2,'x1'=2,'x0'=2] {'y0..., dimensions={0} | all-to-all | bytes 2228224 | tf_op jit(solution)/shard_map/all_to_all | solution.py:369
  57.7 0.0 copy-done.4
  57.8 0.0 copy-done.9
  57.8 0.9 keys_kernel.1.kv_ref
  58.7 0.0 copy-start
  58.7 0.0 copy-start.5
  58.7 5.0 %collective-permute-start = (bf16[4,1024,128]{2,1,0:T(8,128)(2,1)S(1)}, bf16[4,1024,128]{2,1,0:T(8,128)(2,1)S(1)}, u32[]{:S(2)}, u32[]{:S(2)}) collective-permute-start(bf16[4,1024,128]{2,1,0:T(8,128)(2,1)S(1)} %keys_kernel.1.kv_ref), channel_id=1, source_target_pairs={{0,16},{16,0},{1,17},{17,1},{2,18},{18,2},{3,19},{19,3},{4,20},{20... | collective-permute-start | bytes 3145736 | tf_op jit(solution)/shard_map/ppermute | solution.py:421
  63.7 0.5 slots_kernel.1.slot_ref
  64.3 1.0 attend_own_kernel.1
  65.3 0.7 collective-permute-done.kv_ref
  66.0 0.0 copy-done
  66.0 0.0 copy-done.5
  66.0 1.6 %attend_rest_kernel.1 = bf16[16,192,128]{2,1,0:T(8,128)(2,1)S(1)} custom-call(s32[1]{0:T(128)} %bitcast.5.core_ref, bf16[192,512]{1,0:T(8,128)(2,1)S(1)} %slots_kernel.1.slot_ref, bf16[4,1024,128]{2,1,0:T(8,128)(2,1)S(1)} %collective-permute-done.kv_ref, f32[2,192,128]{2,1,0:T(8,128)S(1)} %get-tuple-element.12.peak_ref, ...), custom_call_target="tpu_custom_call" | custom-call | tf_op jit(solution)/shard_map/attend_rest_kernel/pallas_call | solution.py:357
  67.7 15.9 %all_to_all.32.part_ref = bf16[16,192,128]{2,1,0:T(8,128)(2,1)S(1)} all-to-all(bf16[16,192,128]{2,1,0:T(8,128)(2,1)S(1)} %attend_rest_kernel.1), channel_id=1, replica_groups=mesh['z3'=2,'z2'=2,'z1'=2,'z0'=2,'c'=2,'y1'=2,'y0'=2,'x1'=2,'x0'=2] {'y0..., dimensions={0} | all-to-all | bytes 1572864 | tf_op jit(solution)/shard_map/all_to_all | solution.py:369
  83.5 0.1 stream_kernel.1.stream_ref
  83.7 0.0 copy-start.1
  83.7 0.0 copy-start.2
  83.7 0.0 copy-start.3
  83.7 0.0 copy-start.10
  83.7 14.9 %all_to_all.33.x_ref = bf16[16,192,128]{2,1,0:T(8,128)(2,1)S(1)} all-to-all(bf16[16,192,128]{2,1,0:T(8,128)(2,1)S(1)} %stream_kernel.1.stream_ref), channel_id=1, replica_groups=mesh['z3'=2,'z2'=2,'z1'=2,'z0'=2,'c'=2,'y1'=2,'y0'=2,'x1'=2,'x0'=2] {'y0..., dimensions={0} | all-to-all | bytes 1572864 | tf_op jit(solution)/shard_map/all_to_all | solution.py:369
  98.7 0.0 copy-done.6
  98.7 0.0 copy-done.7
  98.7 1.6 %expert_kernel.1 = bf16[16,192,128]{2,1,0:T(8,128)(2,1)S(1)} custom-call(bf16[16,192,128]{2,1,0:T(8,128)(2,1)S(1)} %all_to_all.33.x_ref, bf16[192,512]{1,0:T(8,128)(2,1)S(1)} %slots_kernel.1.slot_ref, f32[1,2048]{1,0:T(1,128)S(1)} %bitcast.26, bf16[2,64,2048]{2,1,0:T(8,128)(2,1)S(1)} %bitcast.18, bf16[2,64,2048]{2,1,0:T(8,128)(2,1)S(1)} %bitcast.19, ...), custom_call_target="tpu_custom_call" | custom-call | tf_op jit(solution)/shard_map/expert_kernel/pallas_call | solution.py:357
  100.3 15.3 %all_to_all.34.part_ref = bf16[16,192,128]{2,1,0:T(8,128)(2,1)S(1)} all-to-all(bf16[16,192,128]{2,1,0:T(8,128)(2,1)S(1)} %expert_kernel.1), channel_id=1, replica_groups=mesh['z3'=2,'z2'=2,'z1'=2,'z0'=2,'c'=2,'y1'=2,'y0'=2,'x1'=2,'x0'=2] {'y0..., dimensions={0} | all-to-all | bytes 1572864 | tf_op jit(solution)/shard_map/all_to_all | solution.py:369
  115.6 0.2 give_back_kernel.1
  115.7 22.7 %all_to_all.35 = bf16[32,3,2,128]{3,2,1,0:T(2,128)(2,1)S(1)} all-to-all(bf16[32,3,2,128]{3,2,1,0:T(2,128)(2,1)S(1)} %bitcast.25), channel_id=1, replica_groups=mesh['z3'=2,'z2'=2,'z1'=2,'z0'=2,'c'=2,'y1'=2,'y0'=2,'x1'=2,'x0'=2] {'c'..., dimensions={0} | all-to-all | bytes 98304 | tf_op jit(solution)/shard_map/all_to_all | solution.py:369
  138.4 0.8 finish_kernel.1
  (11 shorter events, 0.0 us)
Async XLA Ops:
  35.0 22.8 %copy-start.4 = (bf16[512,256]{1,0:T(8,128)(2,1)S(1)}, bf16[512,256]{1,0:T(8,128)(2,1)}, u32[]{:S(2)}) copy-start(bf16[512,256]{1,0:T(8,128)(2,1)} %wide_ref.1) | copy-start | bytes 786436
  35.0 22.8 %copy-start.9 = (bf16[512,128]{1,0:T(8,128)(2,1)S(1)}, bf16[512,128]{1,0:T(8,128)(2,1)}, u32[]{:S(2)}) copy-start(bf16[512,128]{1,0:T(8,128)(2,1)} %narrow_ref.1) | copy-start | bytes 393220
  58.7 7.3 %copy-start = (bf16[128,2048]{1,0:T(8,128)(2,1)S(1)}, bf16[128,2048]{1,0:T(8,128)(2,1)}, u32[]{:S(2)}) copy-start(bf16[128,2048]{1,0:T(8,128)(2,1)} %wide_out_ref.1) | copy-start | bytes 1572868
  58.7 7.3 %copy-start.5 = (bf16[64,2048]{1,0:T(8,128)(2,1)S(1)}, bf16[64,2048]{1,0:T(8,128)(2,1)}, u32[]{:S(2)}) copy-start(bf16[64,2048]{1,0:T(8,128)(2,1)} %narrow_out_ref.1) | copy-start | bytes 786436
  58.7 7.3 %collective-permute-start = (bf16[4,1024,128]{2,1,0:T(8,128)(2,1)S(1)}, bf16[4,1024,128]{2,1,0:T(8,128)(2,1)S(1)}, u32[]{:S(2)}, u32[]{:S(2)}) collective-permute-start(bf16[4,1024,128]{2,1,0:T(8,128)(2,1)S(1)} %keys_kernel.1.kv_ref), channel_id=1, source_target_pairs={{0,16},{16,0},{1,17},{17,1},{2,18},{18,2},{3,19},{19,3},{4,20},{20... | collective-permute-start | bytes 3145736 | tf_op jit(solution)/shard_map/ppermute | solution.py:421
  83.5 15.1 %copy-start.6 = (bf16[2048,64]{0,1:T(8,128)(2,1)S(1)}, bf16[2048,64]{0,1:T(8,128)(2,1)}, u32[]{:S(2)}) copy-start(bf16[2048,64]{0,1:T(8,128)(2,1)} %param.35) | copy-start | bytes 786436
  83.5 15.1 %copy-start.7 = (bf16[2048,64]{0,1:T(8,128)(2,1)S(1)}, bf16[2048,64]{0,1:T(8,128)(2,1)}, u32[]{:S(2)}) copy-start(bf16[2048,64]{0,1:T(8,128)(2,1)} %param.36) | copy-start | bytes 786436
  83.5 15.1 %copy-start.8 = (bf16[64,2048]{1,0:T(8,128)(2,1)S(1)}, bf16[64,2048]{1,0:T(8,128)(2,1)}, u32[]{:S(2)}) copy-start(bf16[64,2048]{1,0:T(8,128)(2,1)} %sd_ref.1) | copy-start | bytes 786436
  83.7 15.0 %copy-start.1 = (bf16[2,2048,64]{1,2,0:T(8,128)(2,1)S(1)}, bf16[2,2048,64]{1,2,0:T(8,128)(2,1)}, u32[]{:S(2)}) copy-start(bf16[2,2048,64]{1,2,0:T(8,128)(2,1)} %param.32) | copy-start | bytes 1572868
  83.7 15.0 %copy-start.2 = (bf16[2,2048,64]{1,2,0:T(8,128)(2,1)S(1)}, bf16[2,2048,64]{1,2,0:T(8,128)(2,1)}, u32[]{:S(2)}) copy-start(bf16[2,2048,64]{1,2,0:T(8,128)(2,1)} %param.33) | copy-start | bytes 1572868
  83.7 15.0 %copy-start.3 = (bf16[2,64,2048]{2,1,0:T(8,128)(2,1)S(1)}, bf16[2,64,2048]{2,1,0:T(8,128)(2,1)}, u32[]{:S(2)}) copy-start(bf16[2,64,2048]{2,1,0:T(8,128)(2,1)} %param.34) | copy-start | bytes 1572868
  83.7 15.0 %copy-start.10 = (f32[2048]{0:T(1024)S(1)}, f32[2048]{0:T(1024)}, u32[]{:S(2)}) copy-start(f32[2048]{0:T(1024)} %param.29) | copy-start | bytes 24580
